TPU v7x, 256 devices: a whole 4x4x8 slice. The times are simulated.
256 devices in a mesh: sp: 64 (over z, y, core), tp: 4 (over x).
Axes of the slice: x: 4, y: 4, z: 8, core: 2. Of those that a mesh axis runs over, the one named last changes fastest.
Arguments:
- tokens: bfloat16 [16384, 2048], P('sp', 'tp'), may hold values from -19 to 250
- in_gain: bfloat16 [2048], replicated, may hold values from 0.099609375 to 1.8984375
- w_glu_value: bfloat16 [2048, 512], P(None, 'tp'), may hold values from -0.125 to 0.125
- w_glu_gate: bfloat16 [2048, 512], P(None, 'tp'), may hold values from -0.125 to 0.125
- w_query: bfloat16 [2048, 1024], P(None, 'tp'), may hold values from -1 to 1
- w_key: bfloat16 [2048, 512], P(None, 'tp'), may hold values from -1 to 1
- w_value: bfloat16 [2048, 512], P(None, 'tp'), may hold values from -0.125 to 0.125
- w_gate_conv: bfloat16 [2048, 512], P(None, 'tp'), may hold values from -0.125 to 0.125
- w_gate_attn: bfloat16 [2048, 1024], P(None, 'tp'), may hold values from -0.125 to 0.125
- conv_weight: bfloat16 [31, 512], P(None, 'tp'), may hold values from -4.6 to 4.6
- conv_gain: float32 [512], P('tp'), may hold values from 0.1 to 1.9
- lam: float32 [8], P('tp'), may hold values from 0.3 to 0.8
- head_gain: float32 [128], replicated, may hold values from 0.1 to 1.9
- out_conv: bfloat16 [512, 2048], P('tp'), may hold values from -0.15625 to 0.15625
- out_attn: bfloat16 [1024, 2048], P('tp'), may hold values from -0.15625 to 0.15625
Outputs:
- mixed: bfloat16 [16384, 2048], P(('sp', 'tp'))
All inputs are finite; a program needn't handle non-finite values.
Results may differ from a plain program's by a relative error of at most 0.017.
The roundings to bfloat16 on the way count: a program that leaves them out, or rounds other values in their place, can miss the bound.
Values may be sent and summed in bfloat16 or wider, within the bound.
No kernel may reach another device: no remote copies, remote signals or barrier semaphores. Data moves between devices by JAX's collectives and lax.ppermute only.
A program may use at most 128 MiB of HBM per device.

v0:
```python
import functools

import jax
import jax.numpy as jnp
from jax import lax
from jax.experimental import pallas as pl
from jax.experimental.pallas import tpu as pltpu
from jax.sharding import PartitionSpec as P


D = 2048
CONV = 512
QK = 64
VDIM = 128
WIDTH = 31
ROWS = 256
ACC = VDIM + 16
MSG = 4 * VDIM + 16

EPSILON = 1e-06
NEG_BIG = -1e30
HEAD_SCALE = 0.8


F32 = jnp.float32
BF16 = jnp.bfloat16
VM = pl.BlockSpec(memory_space=pltpu.VMEM)
OUT = pl.BlockSpec()
SM = pl.BlockSpec(memory_space=pltpu.SMEM)
ANY = pl.BlockSpec(memory_space=pltpu.MemorySpace.HBM)
BIG = pltpu.CompilerParams(vmem_limit_bytes=56 * 1024 * 1024)
SHIFTS = (1, -1, 2)
DEPTH = 3
LOG2E = 1.4426950408889634


def place(s):
    return s // 8, (s // 2) % 4, s % 2


def along_sp(x, move):
    pairs = []
    for s in range(64):
        z, y, c = place(s)
        z, y, c = move(z, y, c)
        pairs.append((s, z * 8 + y * 2 + c))
    return lax.ppermute(x, "sp", pairs)


def z_shift(x, by):
    return along_sp(x, lambda z, y, c: ((z + by) % 8, y, c))


def y_shift(x, by):
    return along_sp(x, lambda z, y, c: (z, (y + by) % 4, c))


def core_swap(x):
    return along_sp(x, lambda z, y, c: (z, y, 1 - c))


def tp_shift(x, by):
    return lax.ppermute(x, "tp", [(i, (i + by) % 4) for i in range(4)])


def dot(a, b):
    return jnp.dot(a, b, preferred_element_type=F32)


def fetch(pairs, sems):
    copies = [pltpu.make_async_copy(src, dst, sems.at[i]) for i, (src, dst) in enumerate(pairs)]
    for copy in copies:
        copy.start()
    return copies


def project_kernel(t0, t1, t2, t3, gain, wq, wk, wv, qt, kv, scaled, inv_out, tok, vq, vk, vv, sems):
    x = lax.axis_index("tp")
    copies = fetch([(t, tok.at[i]) for i, t in enumerate((t0, t1, t2, t3))] + [(wk, vk), (wv, vv), (wq, vq)], sems)
    squares = jnp.zeros((ROWS, 128), F32)
    for i, by in enumerate((0,) + SHIFTS):
        j = lax.rem(x - by + 4, 4)
        copies[i].wait()
        wide = tok[i].astype(F32)
        scaled[j] = (wide * gain[pl.ds(j, 1), :]).astype(BF16)
        sq = wide * wide
        squares += (sq[:, 0:128] + sq[:, 128:256]) + (sq[:, 256:384] + sq[:, 384:512])
    inv = lax.rsqrt(jnp.sum(squares, axis=1, keepdims=True) / D + EPSILON)
    inv_out[...] = jnp.broadcast_to(inv, (ROWS, 128))
    rows = jnp.concatenate([scaled[j] for j in range(4)], axis=1)
    copies[4].wait()
    copies[5].wait()
    both = dot(rows, jnp.concatenate([vk[...], vv[...]], axis=1)) * inv
    kv[0:256, :] = both[:, 0:128].astype(BF16)
    vt = jnp.transpose(both[:, 128:256]).astype(BF16)
    kv[256:384, :] = vt[:, 0:128]
    kv[384:512, :] = vt[:, 128:256]
    copies[6].wait()
    q = dot(rows, vq[...]) * inv
    qt[...] = jnp.transpose(q * (QK ** -0.5)).astype(BF16)


def rest_kernel(scaled, inv_in, wgv, wgg, wgc, wga, glued, tail, gates):
    inv = inv_in[...]
    wide = jnp.concatenate([inv, inv], axis=1)
    rows = jnp.concatenate([scaled[j] for j in range(4)], axis=1)
    glu = (dot(rows, jnp.concatenate([wgv[...], wgg[...]], axis=1)) * wide).astype(BF16).astype(F32)
    g = (glu[:, 0:128] * jax.nn.sigmoid(glu[:, 128:256])).astype(BF16)
    glued[...] = g
    tail[...] = g[ROWS - 32 :, :]
    gates[:, 0:128] = (dot(rows, wgc[...]) * inv).astype(BF16)
    gates[:, 128:384] = (dot(rows, wga[...]) * wide).astype(BF16)


def conv_kernel(glued, before, weight, conv, squares, padded):
    padded[0:32, :] = before[...].astype(F32)
    padded[32 : 32 + ROWS, :] = glued[...].astype(F32)
    taps = weight[...].astype(F32)
    total = jnp.zeros((ROWS, 128), F32)
    for j in range(WIDTH):
        total += padded[j + 2 : j + 2 + ROWS, :] * taps[j : j + 1, :]
    conv[...] = total
    squares[...] = jnp.sum(jnp.transpose(total * total), axis=0, keepdims=True)


def gate_kernel(conv, s0, s1, s2, s3, gain, gates, y_conv):
    total = (s0[...] + s1[...]) + (s2[...] + s3[...])
    inv = lax.rsqrt(total / CONV + EPSILON)
    inv = jnp.transpose(jnp.broadcast_to(inv, (128, ROWS)))
    normed = conv[...] * inv * gain[...]
    y_conv[...] = (jax.nn.silu(normed) * jax.nn.silu(gates[:, 0:128].astype(F32))).astype(BF16)


def attend(tiles, kv, slot, queries, maxima, acc, mask=None):
    keys = jnp.concatenate([kv[slot, 0, 0:256, :], kv[slot, 1, 0:256, :]], axis=0)
    keys = jnp.concatenate([keys, keys], axis=1)
    values = jnp.concatenate(
        [
            kv[slot, 0, 256:384, :],
            kv[slot, 0, 384:512, :],
            kv[slot, 1, 256:384, :],
            kv[slot, 1, 384:512, :],
        ],
        axis=1,
    )
    values = jnp.concatenate([values, jnp.ones((ACC - VDIM, 512), BF16)], axis=0)
    ahead = [dot(keys, queries[t]) for t in tiles[:DEPTH]]
    for i, t in enumerate(tiles):
        scores = ahead.pop(0)
        if i + DEPTH < len(tiles):
            ahead.append(dot(keys, queries[tiles[i + DEPTH]]))
        if mask is not None:
            scores = jnp.where(mask, scores, NEG_BIG)
        old = maxima[t]
        new = jnp.maximum(old, jnp.max(scores, axis=0, keepdims=True))
        factor = jnp.exp2(old - new)
        expd = jnp.exp2(scores - new).astype(BF16)
        acc[t] = acc[t] * factor + dot(values, expd)
        maxima[t] = new


def lay_queries(q_refs, queries):
    none = jnp.zeros((64, ROWS), BF16)
    for b, ref in enumerate(q_refs):
        for t in range(4):
            g, m = t // 2, t % 2
            part = ref[g * 128 + m * 64 : g * 128 + m * 64 + 64, :].astype(F32) * LOG2E
            high = part.astype(BF16)
            low = (part - high.astype(F32)).astype(BF16)
            for i, rows in enumerate((high, low)):
                at = i * 128
                queries[b * 4 + t, at + m * 64 : at + m * 64 + 64, :] = rows
                queries[b * 4 + t, at + (1 - m) * 64 : at + (1 - m) * 64 + 64, :] = none


def write_part(out, first, maxima, acc):
    lines = []
    for t in range(4):
        i = first + t
        length = acc[i, VDIM : VDIM + 1, :]
        some = length > 0.0
        safe = jnp.where(some, length, 1.0)
        out[t * VDIM : (t + 1) * VDIM, :] = (acc[i, 0:VDIM, :] * (1.0 / safe)).astype(BF16)
        log = jnp.where(some, maxima[i] + jnp.log2(safe), NEG_BIG)
        for _ in range(3):
            piece = log.astype(BF16).astype(F32)
            lines.append(piece)
            log = log - piece
    lines.append(jnp.zeros((4, ROWS), F32))
    out[4 * VDIM : MSG, :] = jnp.concatenate(lines, axis=0).astype(BF16)


def position():
    s = lax.axis_index("sp")
    return s // 8, lax.rem(s // 2, 4), lax.rem(s, 2)


def kv_pairs(refs, kv, slots, core):
    pairs = []
    for ref, slot in zip(refs, slots):
        if isinstance(ref, tuple):
            pairs += [(ref[0], kv.at[slot, core, 0:256]), (ref[1], kv.at[slot, core, 256:512])]
        else:
            pairs.append((ref, kv.at[slot, core]))
    return pairs


def loop_over(tiles, kv, count, first, queries, maxima, acc):
    def visit(i, carry):
        attend(tiles, kv, first + i, queries, maxima, acc)
        return carry

    lax.fori_loop(0, count, visit, 0)


def early_kernel(*refs):
    q_refs, own, other = refs[0:3], refs[3:8], refs[8:13]
    max_out, acc_out, kv, queries, maxima, sems = refs[13:]
    acc = acc_out
    z, y, c = position()
    slots = (0, 1, 4, 2, 3)
    copies = fetch(kv_pairs(own, kv, slots, c) + kv_pairs(other, kv, slots, 1 - c), sems)
    lay_queries(q_refs, queries)
    maxima[...] = jnp.full(maxima.shape, NEG_BIG, F32)
    acc[...] = jnp.zeros(acc.shape, F32)
    for copy in copies:
        copy.wait()
    for b, by in enumerate(SHIFTS):

        @pl.when(lax.rem(y - by + 4, 4) > y)
        def _(b=b):
            attend(range(4 * b, 4 * b + 4), kv, 0, queries, maxima, acc)

    count = jnp.minimum(z, 2) + jnp.where(z >= 6, 1, 0) + jnp.where(z >= 7, 1, 0)
    loop_over(range(12), kv, count, 1, queries, maxima, acc)
    max_out[...] = maxima[...]


def late_kernel(*refs, blocks):
    n = len(blocks)
    q_refs, own, other = refs[0:n], refs[n : n + 4], refs[n + 4 : n + 8]
    max_in, acc_in = refs[n + 8 : n + 10]
    outs = refs[n + 10 : 2 * n + 10]
    kv, queries, maxima, acc, sems = refs[2 * n + 10 :]
    z, _, c = position()
    pairs = [((own[2], own[3])), ((other[2], other[3]))]
    slots = (0, 2, 1)
    copies = fetch(
        kv_pairs((own[0], own[1], pairs[0]), kv, slots, c)
        + kv_pairs((other[0], other[1], pairs[1]), kv, slots, 1 - c)
        + [(max_in.at[4 * b : 4 * b + 4], maxima.at[4 * i : 4 * i + 4]) for i, b in enumerate(blocks)]
        + [(acc_in.at[4 * b : 4 * b + 4], acc.at[4 * i : 4 * i + 4]) for i, b in enumerate(blocks)],
        sems,
    )
    lay_queries(q_refs, queries)
    for copy in copies:
        copy.wait()
    loop_over(range(4 * n), kv, jnp.clip(z - 2, 0, 3), 0, queries, maxima, acc)
    for i in range(n):
        write_part(outs[i], 4 * i, maxima, acc)


def self_kernel(*refs):
    q_ref, own, other, out = refs[0], refs[1:10], refs[10:19], refs[19]
    kv, queries, maxima, acc, sems = refs[20:]
    z, _, c = position()
    slots = (0, 1, 7, 2, 6, 3, 5, 4)
    copies = fetch(
        kv_pairs(own[0:7] + ((own[7], own[8]),), kv, slots, c)
        + kv_pairs(other[0:7] + ((other[7], other[8]),), kv, slots, 1 - c),
        sems,
    )
    lay_queries((q_ref,), queries)
    maxima[...] = jnp.full(maxima.shape, NEG_BIG, F32)
    acc[...] = jnp.zeros(acc.shape, F32)
    for copy in copies:
        copy.wait()
    key_row = lax.broadcasted_iota(jnp.int32, (512, ROWS), 0)
    query_row = lax.broadcasted_iota(jnp.int32, (512, ROWS), 1) + c * ROWS
    attend(range(4), kv, 0, queries, maxima, acc, key_row <= query_row)
    loop_over(range(4), kv, z, 1, queries, maxima, acc)
    write_part(out, 0, maxima, acc)


def output_kernel(m0, m1, m2, m3, y_conv, gates, lam, gain, out_conv, out_attn, o0, o1, o2, o3, rows):
    x = lax.axis_index("tp")
    logs = []
    for ref in (m0, m1, m2, m3):
        stats = ref[4 * VDIM : MSG, :].astype(F32)
        logs.append([(stats[3 * t : 3 * t + 1] + stats[3 * t + 1 : 3 * t + 2]) + stats[3 * t + 2 : 3 * t + 3] for t in range(4)])
    for j in range(4):
        rows[j, :, 0:128] = y_conv[64 * j : 64 * j + 64, :]
    for g in range(2):
        maps = []
        for m in range(2):
            t = 2 * g + m
            top = functools.reduce(jnp.maximum, [l[t] for l in logs])
            weights = [jnp.exp2(l[t] - top) for l in logs]
            norm = 1.0 / functools.reduce(jnp.add, weights)
            part = [r[t * VDIM : (t + 1) * VDIM, :].astype(F32) * (w * norm) for r, w in zip((m0, m1, m2, m3), weights)]
            maps.append((part[0] + part[1]) + (part[2] + part[3]))
        o = maps[0] - lam[g] * maps[1]
        o = o * lax.rsqrt(jnp.mean(o * o, axis=0, keepdims=True) + EPSILON)
        o = jnp.transpose(o) * gain[...] * HEAD_SCALE
        gate = gates[:, 128 + g * 128 : 256 + g * 128].astype(F32)
        o = (o * jax.nn.silu(gate)).astype(BF16)
        for j in range(4):
            rows[j, :, 128 + g * 128 : 256 + g * 128] = o[64 * j : 64 * j + 64, :]
    order = [lax.rem(x + by + 4, 4) for by in (0,) + SHIFTS]
    ordered = jnp.concatenate([rows[j] for j in order], axis=0)
    total = dot(ordered[:, 0:128], out_conv[...]) + dot(ordered[:, 128:384], out_attn[...])
    for i, ref in enumerate((o0, o1, o2, o3)):
        ref[...] = total[64 * i : 64 * i + 64, :].astype(BF16)


def in_hbm(arrays):
    return [pltpu.with_memory_space_constraint(a, pltpu.MemorySpace.HBM) for a in arrays]


def shape(dims, kind=BF16):
    return jax.ShapeDtypeStruct(dims, kind)


def sent(dims, kind=BF16):
    return pltpu.MemorySpace.HBM(dims, kind)


def local(
    tokens,
    in_gain,
    w_glu_value,
    w_glu_gate,
    w_query,
    w_key,
    w_value,
    w_gate_conv,
    w_gate_attn,
    conv_weight,
    conv_gain,
    lam,
    head_gain,
    out_conv,
    out_attn,
):
    pieces = [tokens] + [tp_shift(tokens, by) for by in SHIFTS]
    gain = in_gain.astype(F32).reshape(4, 512)
    qt, kv, scaled, inv = pl.pallas_call(
        project_kernel,
        out_shape=[sent((256, ROWS)), sent((512, 128)), shape((4, ROWS, 512)), shape((ROWS, 128), F32)],
        in_specs=[ANY] * 4 + [VM] + [ANY] * 3,
        out_specs=[OUT] * 2 + [VM] * 2,
        scratch_shapes=[
            pltpu.VMEM((4, ROWS, 512), BF16),
            pltpu.VMEM((D, 256), BF16),
            pltpu.VMEM((D, 128), BF16),
            pltpu.VMEM((D, 128), BF16),
            pltpu.SemaphoreType.DMA((7,)),
        ],
        compiler_params=BIG,
        name="project",
    )(*in_hbm(pieces), gain, *in_hbm([w_query, w_key, w_value]))

    p2, m2, p1, m1 = [z_shift(kv, by) for by in (2, -2, 1, -1)]
    kv_s = core_swap(kv)
    q_blocks = [y_shift(qt, by) for by in SHIFTS]

    glued, tail, gates = pl.pallas_call(
        rest_kernel,
        out_shape=[shape((ROWS, 128)), sent((32, 128)), shape((ROWS, 384))],
        in_specs=[VM] * 6,
        out_specs=[VM, OUT, VM],
        compiler_params=BIG,
        name="rest",
    )(scaled, inv, w_glu_value, w_glu_gate, w_gate_conv, w_gate_attn)
    before = lax.ppermute(tail, "sp", [(i, i + 1) for i in range(63)])
    conv, squares = pl.pallas_call(
        conv_kernel,
        out_shape=[shape((ROWS, 128), F32), sent((1, ROWS), F32)],
        in_specs=[VM] * 3,
        out_specs=[VM, OUT],
        scratch_shapes=[pltpu.VMEM((32 + ROWS, 128), F32)],
        name="conv",
    )(glued, before, conv_weight)
    sums = [squares] + [tp_shift(squares, by) for by in SHIFTS]

    (p1, m1, p2, m2), squares = lax.optimization_barrier(((p1, m1, p2, m2), squares))
    p3, m3 = z_shift(p2, 1), z_shift(m2, -1)
    p4, m4 = z_shift(p2[0:256], 2), z_shift(m2[256:512], -2)
    near = [kv, p1, m1, p2, m2]
    near_s = [kv_s] + [core_swap(k) for k in near[1:]]

    y_conv = pl.pallas_call(
        gate_kernel,
        out_shape=shape((ROWS, 128)),
        in_specs=[VM] * 7,
        out_specs=VM,
        name="gate",
    )(conv, *sums, conv_gain.reshape(1, 128), gates)
    y_conv, near_s = lax.optimization_barrier((y_conv, near_s))

    def scratch(slots, tiles, held, copies):
        return (
            [pltpu.VMEM((slots, 2, 512, 128), BF16), pltpu.VMEM((tiles, 256, ROWS), BF16), pltpu.VMEM((tiles, 1, ROWS), F32)]
            + ([pltpu.VMEM((tiles, ACC, ROWS), F32)] if held else [])
            + [pltpu.SemaphoreType.DMA((copies,))]
        )

    maxima, acc = pl.pallas_call(
        early_kernel,
        out_shape=[shape((12, 1, ROWS), F32), shape((12, ACC, ROWS), F32)],
        in_specs=[VM] * 3 + [ANY] * 10,
        out_specs=[VM] * 2,
        scratch_shapes=scratch(5, 12, False, 10),
        compiler_params=BIG,
        name="early",
    )(*q_blocks, *in_hbm(near), *in_hbm(near_s))

    (p3, m3, p4, m4), acc = lax.optimization_barrier(((p3, m3, p4, m4), acc))
    far = [p3, m3, p4, m4]
    far_s = [core_swap(k) for k in far]

    def late(blocks, acc):
        n = len(blocks)
        return pl.pallas_call(
            functools.partial(late_kernel, blocks=blocks),
            out_shape=[sent((MSG, ROWS))] * n,
            in_specs=[VM] * n + [ANY] * 8 + [pl.BlockSpec(memory_space=pl.ANY)] * 2,
            out_specs=[OUT] * n,
            scratch_shapes=scratch(3, 4 * n, True, 8 + 2 * n),
            compiler_params=BIG,
        )(*[q_blocks[b] for b in blocks], *in_hbm(far), *in_hbm(far_s), maxima, acc)

    (part2,) = late((2,), acc)
    part2, acc = lax.optimization_barrier((part2, acc))
    back2 = y_shift(part2, -2)
    part0, part1 = late((0, 1), acc)
    back0, back1 = y_shift(part0, -1), y_shift(part1, 1)
    (part0, qt) = lax.optimization_barrier((part0, qt))
    part = pl.pallas_call(
        self_kernel,
        out_shape=shape((MSG, ROWS)),
        in_specs=[VM] + [ANY] * 18,
        out_specs=VM,
        scratch_shapes=scratch(8, 4, True, 18),
        compiler_params=BIG,
        name="self",
    )(qt, *in_hbm(near), *in_hbm(far), *in_hbm(near_s), *in_hbm(far_s))
    merged = [part, back0, back1, back2]

    outs = pl.pallas_call(
        output_kernel,
        out_shape=[sent((64, D))] * 4,
        in_specs=[VM] * 6 + [SM] + [VM] * 3,
        out_specs=[OUT] * 4,
        scratch_shapes=[pltpu.VMEM((4, 64, 384), BF16)],
        compiler_params=BIG,
        name="output",
    )(*merged, y_conv, gates, lam, head_gain.reshape(1, 128), out_conv, out_attn)
    sums = [outs[0]] + [tp_shift(o, by) for o, by in zip(outs[1:], SHIFTS)]
    a, b, c, d = [o.astype(F32) for o in sums]
    return ((a + b) + (c + d)).astype(BF16)


def solution(mesh):
    in_specs = (
        P("sp", "tp"),
        P(),
        P(None, "tp"),
        P(None, "tp"),
        P(None, "tp"),
        P(None, "tp"),
        P(None, "tp"),
        P(None, "tp"),
        P(None, "tp"),
        P(None, "tp"),
        P("tp"),
        P("tp"),
        P(),
        P("tp", None),
        P("tp", None),
    )
    out_specs = P(("sp", "tp"), None)

    return jax.shard_map(local, mesh=mesh, in_specs=in_specs, out_specs=out_specs, check_vma=False)
```

profile of v0, /device:TPU:230, one launch (start us, length us, event | category | flops | bytes accessed | tf_op | source)
XLA Modules:
  0.0 135.2 jit_solution(12815788068110070337)
XLA Ops:
  0.8 2.4 %collective-permute-start = (bf16[256,512]{1,0:T(8,128)(2,1)}, bf16[256,512]{1,0:T(8,128)(2,1)S(1)}, u32[]{:S(2)}, u32[]{:S(2)}) collective-permute-start(bf16[256,512]{1,0:T(8,128)(2,1)} %t0.1), channel_id=1, source_target_pairs={{0,1},{1,2},{2,3},{3,0},{4,5},{5,6},{6,7},{7,4},{8,9},{9,10},{10,1... | collective-permute-start | bytes 786440 | tf_op jit(solution)/shard_map/ppermute | solution.py:63
  3.4 1.3 reshape.16.gain
  4.7 10.4 %collective-permute-done.1.t2 = bf16[256,512]{1,0:T(8,128)(2,1)S(1)} collective-permute-done((bf16[256,512]{1,0:T(8,128)(2,1)}, bf16[256,512]{1,0:T(8,128)(2,1)S(1)}, u32[]{:S(2)}, u32[]{:S(2)}) %collective-permute-start.1) | collective-permute-done | bytes 262176 | tf_op jit(solution)/shard_map/ppermute | solution.py:63
  16.6 4.5 %project.1 = (bf16[256,256]{1,0:T(8,128)(2,1)}, bf16[512,128]{1,0:T(8,128)(2,1)}, bf16[4,256,512]{2,1,0:T(8,128)(2,1)}, f32[256,128]{1,0:T(8,128)}) custom-call(bf16[256,512]{1,0:T(8,128)(2,1)} %t0.1, bf16[256,512]{1,0:T(8,128)(2,1)} %copy-done.26, bf16[256,512]{1,0:T(8,128)(2,1)} %copy-done.25, bf16[256,512]{1,0:T(8,128)(2,1)} %copy-done.27, ...), custom_call_target="tpu_custom_call" | custom-call | tf_op jit(solution)/shard_map/project/pallas_call | solution.py:347
  21.1 1.5 %collective-permute-start.8 = (bf16[512,128]{1,0:T(8,128)(2,1)}, bf16[512,128]{1,0:T(8,128)(2,1)S(1)}, u32[]{:S(2)}, u32[]{:S(2)}) collective-permute-start(bf16[512,128]{1,0:T(8,128)(2,1)} %get-tuple-element.41.refs_3_.refs_1_), channel_id=1, source_target_pairs={{0,192},{4,196},{8,200},{12,204},{16,208},{20,212},{24,216},{28,22... | collective-permute-start | bytes 393224 | tf_op jit(solution)/shard_map/ppermute | solution.py:47
  22.6 2.7 %collective-permute-start.7 = (bf16[512,128]{1,0:T(8,128)(2,1)}, bf16[512,128]{1,0:T(8,128)(2,1)S(1)}, u32[]{:S(2)}, u32[]{:S(2)}) collective-permute-start(bf16[512,128]{1,0:T(8,128)(2,1)} %get-tuple-element.41.refs_3_.refs_1_), channel_id=1, source_target_pairs={{0,64},{4,68},{8,72},{12,76},{16,80},{20,84},{24,88},{28,92},{32,9... | collective-permute-start | bytes 393224 | tf_op jit(solution)/shard_map/ppermute | solution.py:47
  25.3 1.0 collective-permute-start.6
  26.3 2.2 %collective-permute-start.5 = (bf16[512,128]{1,0:T(8,128)(2,1)}, bf16[512,128]{1,0:T(8,128)(2,1)S(1)}, u32[]{:S(2)}, u32[]{:S(2)}) collective-permute-start(bf16[512,128]{1,0:T(8,128)(2,1)} %get-tuple-element.41.refs_3_.refs_1_), channel_id=1, source_target_pairs={{0,32},{4,36},{8,40},{12,44},{16,48},{20,52},{24,56},{28,60},{32,6... | collective-permute-start | bytes 393224 | tf_op jit(solution)/shard_map/ppermute | solution.py:47
  28.5 3.8 %rest.1 = (bf16[256,128]{1,0:T(8,128)(2,1)}, bf16[32,128]{1,0:T(8,128)(2,1)}, bf16[256,384]{1,0:T(8,128)(2,1)}) custom-call(bf16[4,256,512]{2,1,0:T(8,128)(2,1)} %get-tuple-element.42.scaled, f32[256,128]{1,0:T(8,128)} %get-tuple-element.43.inv_in, bf16[2048,128]{1,0:T(8,128)(2,1)} %wgv.1, bf16[2048,128]{1,0:T(8,128)(2,1)} %wgg.1, bf16[2048,128]{1,0:T(8,128)(2,1)} %wgc.1, ...), custom_call_target="tpu_custom_call" | custom-call | tf_op jit(solution)/shard_map/rest/pallas_call | solution.py:367
  32.3 1.9 %collective-permute-start.9 = (bf16[32,128]{1,0:T(8,128)(2,1)}, bf16[32,128]{1,0:T(8,128)(2,1)S(1)}, u32[]{:S(2)}, u32[]{:S(2)}) collective-permute-start(bf16[32,128]{1,0:T(8,128)(2,1)} %get-tuple-element.45), channel_id=1, source_target_pairs={{0,4},{4,8},{8,12},{12,16},{16,20},{20,24},{24,28},{28,32},{32,36}... | collective-permute-start | bytes 24584 | tf_op jit(solution)/shard_map/ppermute | solution.py:375
  34.2 5.4 %collective-permute-done.9.before = bf16[32,128]{1,0:T(8,128)(2,1)S(1)} collective-permute-done((bf16[32,128]{1,0:T(8,128)(2,1)}, bf16[32,128]{1,0:T(8,128)(2,1)S(1)}, u32[]{:S(2)}, u32[]{:S(2)}) %collective-permute-start.9) | collective-permute-done | bytes 8224 | tf_op jit(solution)/shard_map/ppermute | solution.py:375
  40.2 1.8 %conv.1 = (f32[256,128]{1,0:T(8,128)}, f32[1,256]{1,0:T(1,128)}) custom-call(bf16[256,128]{1,0:T(8,128)(2,1)} %get-tuple-element.44.glued, bf16[32,128]{1,0:T(8,128)(2,1)} %copy-done.29, bf16[31,128]{1,0:T(8,128)(2,1)} %weight.1), custom_call_target="tpu_custom_call" | custom-call | tf_op jit(solution)/shard_map/conv/pallas_call | solution.py:376
  42.3 4.9 %collective-permute-done.17.s3 = f32[1,256]{1,0:T(1,128)S(1)} collective-permute-done((f32[1,256]{1,0:T(1,128)}, f32[1,256]{1,0:T(1,128)S(1)}, u32[]{:S(2)}, u32[]{:S(2)}) %collective-permute-start.17) | collective-permute-done | bytes 1056 | tf_op jit(solution)/shard_map/ppermute | solution.py:63
  47.3 1.1 collective-permute-start.14
  48.4 1.1 collective-permute-start.4
  49.7 3.0 %collective-permute-start.15 = (f32[1,256]{1,0:T(1,128)}, f32[1,256]{1,0:T(1,128)S(1)}, u32[]{:S(2)}, u32[]{:S(2)}) collective-permute-start(f32[1,256]{1,0:T(1,128)} %get-tuple-element.46.s0), channel_id=1, source_target_pairs={{0,1},{1,2},{2,3},{3,0},{4,5},{5,6},{6,7},{7,4},{8,9},{9,10},{10,1... | collective-permute-start | bytes 3080 | tf_op jit(solution)/shard_map/ppermute | solution.py:63
  52.8 1.6 %collective-permute-done.16.s2 = f32[1,256]{1,0:T(1,128)S(1)} collective-permute-done((f32[1,256]{1,0:T(1,128)}, f32[1,256]{1,0:T(1,128)S(1)}, u32[]{:S(2)}, u32[]{:S(2)}) %collective-permute-start.16) | collective-permute-done | bytes 1056 | tf_op jit(solution)/shard_map/ppermute | solution.py:63
  56.5 2.0 %collective-permute-start.11 = (bf16[512,128]{1,0:T(8,128)(2,1)S(1)}, bf16[512,128]{1,0:T(8,128)(2,1)S(1)}, u32[]{:S(2)}, u32[]{:S(2)}) collective-permute-start(bf16[512,128]{1,0:T(8,128)(2,1)S(1)} %collective-permute-done.8.refs_7_.refs_5_), channel_id=1, source_target_pairs={{0,224},{4,228},{8,232},{12,236},{16,240},{20,244},{24,248},{28,25... | collective-permute-start | bytes 393224 | tf_op jit(solution)/shard_map/ppermute | solution.py:47
  58.6 4.1 %collective-permute-start.12 = (bf16[256,128]{1,0:T(8,128)(2,1)S(1)}, bf16[256,128]{1,0:T(8,128)(2,1)S(1)}, u32[]{:S(2)}, u32[]{:S(2)}) collective-permute-start(bf16[256,128]{1,0:T(8,128)(2,1)S(1)} %slice.6), channel_id=1, source_target_pairs={{0,64},{4,68},{8,72},{12,76},{16,80},{20,84},{24,88},{28,92},{32,9... | collective-permute-start | bytes 196616 | tf_op jit(solution)/shard_map/ppermute | solution.py:47
  62.8 1.8 %gate.1.y_conv = bf16[256,128]{1,0:T(8,128)(2,1)} custom-call(f32[256,128]{1,0:T(8,128)} %get-tuple-element.51.conv, f32[1,256]{1,0:T(1,128)} %get-tuple-element.46.s0, f32[1,256]{1,0:T(1,128)} %copy-done.32, f32[1,256]{1,0:T(1,128)} %copy-done.31, f32[1,256]{1,0:T(1,128)} %copy-done.30, f32[1,128]{1,0:T(1,128)} %bitcast.2, ...), custom_call_target="tpu_custom_call" | custom-call | tf_op jit(solution)/shard_map/gate/pallas_call | solution.py:392
  65.3 13.7 %early.1 = (f32[12,1,256]{2,1,0:T(1,128)}, f32[12,144,256]{2,1,0:T(8,128)}) custom-call(bf16[256,256]{1,0:T(8,128)(2,1)} %copy-done.20, bf16[256,256]{1,0:T(8,128)(2,1)} %copy-done.15, bf16[256,256]{1,0:T(8,128)(2,1)} %copy-done.13, bf16[512,128]{1,0:T(8,128)(2,1)} %get-tuple-element.41.refs_3_.refs_1_, bf16[512,128]{1,0:T(8,128)(2,1)} %copy-done.12, ...), custom_call_target="tpu_custom_call" | custom-call | tf_op jit(solution)/shard_map/early/pallas_call | solution.py:408
  81.9 5.7 %shard_map.145 = bf16[528,256]{1,0:T(8,128)(2,1)} custom-call(bf16[256,256]{1,0:T(8,128)(2,1)} %copy-done.13, bf16[512,128]{1,0:T(8,128)(2,1)} %copy-done, bf16[512,128]{1,0:T(8,128)(2,1)} %copy-done.1, bf16[256,128]{1,0:T(8,128)(2,1)} %copy-done.7, bf16[256,128]{1,0:T(8,128)(2,1)} %copy-done.6, bf16[512,128]{1,0:T(8,128)(2,1)} %copy-done.2, ...), custom_call_target="tpu_custom_call" | custom-call | tf_op jit(solution)/shard_map/pallas_call | solution.py:424
  87.6 7.7 %shard_map.146 = (bf16[528,256]{1,0:T(8,128)(2,1)}, bf16[528,256]{1,0:T(8,128)(2,1)}) custom-call(bf16[256,256]{1,0:T(8,128)(2,1)} %copy-done.20, bf16[256,256]{1,0:T(8,128)(2,1)} %copy-done.15, bf16[512,128]{1,0:T(8,128)(2,1)} %copy-done, bf16[512,128]{1,0:T(8,128)(2,1)} %copy-done.1, bf16[256,128]{1,0:T(8,128)(2,1)} %copy-done.7, ...), custom_call_target="tpu_custom_call" | custom-call | tf_op jit(solution)/shard_map/pallas_call | solution.py:424
  95.4 3.2 %collective-permute-start.27 = (bf16[528,256]{1,0:T(8,128)(2,1)}, bf16[528,256]{1,0:T(8,128)(2,1)S(1)}, u32[]{:S(2)}, u32[]{:S(2)}) collective-permute-start(bf16[528,256]{1,0:T(8,128)(2,1)} %get-tuple-element.66), channel_id=1, source_target_pairs={{0,24},{4,28},{8,0},{12,4},{16,8},{20,12},{24,16},{28,20},{32,56},... | collective-permute-start | bytes 811016 | tf_op jit(solution)/shard_map/ppermute | solution.py:47
  98.7 10.3 %self.1.m0 = bf16[528,256]{1,0:T(8,128)(2,1)} custom-call(bf16[256,256]{1,0:T(8,128)(2,1)} %get-tuple-element.67.refs_0_, bf16[512,128]{1,0:T(8,128)(2,1)} %get-tuple-element.41.refs_3_.refs_1_, bf16[512,128]{1,0:T(8,128)(2,1)} %copy-done.12, bf16[512,128]{1,0:T(8,128)(2,1)} %copy-done.11, bf16[512,128]{1,0:T(8,128)(2,1)} %copy-done.5, ...), custom_call_target="tpu_custom_call" | custom-call | tf_op jit(solution)/shard_map/self/pallas_call | solution.py:439
  108.9 2.4 %collective-permute-done.28.m2 = bf16[528,256]{1,0:T(8,128)(2,1)S(1)} collective-permute-done((bf16[528,256]{1,0:T(8,128)(2,1)}, bf16[528,256]{1,0:T(8,128)(2,1)S(1)}, u32[]{:S(2)}, u32[]{:S(2)}) %collective-permute-start.28) | collective-permute-done | bytes 270368 | tf_op jit(solution)/shard_map/ppermute | solution.py:47
  112.3 3.9 %output.1 = (bf16[64,2048]{1,0:T(8,128)(2,1)}, bf16[64,2048]{1,0:T(8,128)(2,1)}, bf16[64,2048]{1,0:T(8,128)(2,1)}, bf16[64,2048]{1,0:T(8,128)(2,1)}) custom-call(bf16[528,256]{1,0:T(8,128)(2,1)} %self.1.m0, bf16[528,256]{1,0:T(8,128)(2,1)} %copy-done.23, bf16[528,256]{1,0:T(8,128)(2,1)} %copy-done.22, bf16[528,256]{1,0:T(8,128)(2,1)} %copy-done.24, ...), custom_call_target="tpu_custom_call" | custom-call | tf_op jit(solution)/shard_map/output/pallas_call | solution.py:450
  116.1 2.8 %collective-permute-start.30 = (bf16[64,2048]{1,0:T(8,128)(2,1)}, bf16[64,2048]{1,0:T(8,128)(2,1)S(1)}, u32[]{:S(2)}, u32[]{:S(2)}) collective-permute-start(bf16[64,2048]{1,0:T(8,128)(2,1)} %get-tuple-element.72), channel_id=1, source_target_pairs={{0,1},{1,2},{2,3},{3,0},{4,5},{5,6},{6,7},{7,4},{8,9},{9,10},{10,1... | collective-permute-start | bytes 786440 | tf_op jit(solution)/shard_map/ppermute | solution.py:63
  119.0 1.9 %collective-permute-start.32 = (bf16[64,2048]{1,0:T(8,128)(2,1)}, bf16[64,2048]{1,0:T(8,128)(2,1)S(1)}, u32[]{:S(2)}, u32[]{:S(2)}) collective-permute-start(bf16[64,2048]{1,0:T(8,128)(2,1)} %get-tuple-element.74), channel_id=1, source_target_pairs={{0,2},{1,3},{2,0},{3,1},{4,6},{5,7},{6,4},{7,5},{8,10},{9,11},{10,... | collective-permute-start | bytes 786440 | tf_op jit(solution)/shard_map/ppermute | solution.py:63
  120.9 9.2 %collective-permute-done.30 = bf16[64,2048]{1,0:T(8,128)(2,1)S(1)} collective-permute-done((bf16[64,2048]{1,0:T(8,128)(2,1)}, bf16[64,2048]{1,0:T(8,128)(2,1)S(1)}, u32[]{:S(2)}, u32[]{:S(2)}) %collective-permute-start.30) | collective-permute-done | bytes 262176 | tf_op jit(solution)/shard_map/ppermute | solution.py:63
  130.1 3.3 %collective-permute-done.31 = bf16[64,2048]{1,0:T(8,128)(2,1)S(1)} collective-permute-done((bf16[64,2048]{1,0:T(8,128)(2,1)}, bf16[64,2048]{1,0:T(8,128)(2,1)S(1)}, u32[]{:S(2)}, u32[]{:S(2)}) %collective-permute-start.31) | collective-permute-done | bytes 262176 | tf_op jit(solution)/shard_map/ppermute | solution.py:63
  133.4 1.8 %add_convert_fusion = bf16[64,2048]{1,0:T(8,128)(2,1)} fusion(bf16[64,2048]{1,0:T(8,128)(2,1)S(1)} %collective-permute-done.32, bf16[64,2048]{1,0:T(8,128)(2,1)S(1)} %collective-permute-done.31, bf16[64,2048]{1,0:T(8,128)(2,1)S(1)} %collective-permute-done.30, bf16[64,2048]{1,0:T(8,128)(2,1)} %get-tuple-element.71), kind=kLoop, calls=%fused_computation | loop fusion | flops 1048576 | bytes 1310720 | tf_op jit(solution)/shard_map/convert_element_type | solution.py:461
  (113 shorter events, 10.3 us)
Async XLA Ops:
  0.0 15.1 %collective-permute-start.1 = (bf16[256,512]{1,0:T(8,128)(2,1)}, bf16[256,512]{1,0:T(8,128)(2,1)S(1)}, u32[]{:S(2)}, u32[]{:S(2)}) collective-permute-start(bf16[256,512]{1,0:T(8,128)(2,1)} %t0.1), channel_id=1, source_target_pairs={{0,3},{1,0},{2,1},{3,2},{4,7},{5,4},{6,5},{7,6},{8,11},{9,8},{10,9... | collective-permute-start | bytes 786440 | tf_op jit(solution)/shard_map/ppermute | solution.py:63
  0.8 14.3 %collective-permute-start = (bf16[256,512]{1,0:T(8,128)(2,1)}, bf16[256,512]{1,0:T(8,128)(2,1)S(1)}, u32[]{:S(2)}, u32[]{:S(2)}) collective-permute-start(bf16[256,512]{1,0:T(8,128)(2,1)} %t0.1), channel_id=1, source_target_pairs={{0,1},{1,2},{2,3},{3,0},{4,5},{5,6},{6,7},{7,4},{8,9},{9,10},{10,1... | collective-permute-start | bytes 786440 | tf_op jit(solution)/shard_map/ppermute | solution.py:63
  3.2 11.9 %collective-permute-start.2 = (bf16[256,512]{1,0:T(8,128)(2,1)}, bf16[256,512]{1,0:T(8,128)(2,1)S(1)}, u32[]{:S(2)}, u32[]{:S(2)}) collective-permute-start(bf16[256,512]{1,0:T(8,128)(2,1)} %t0.1), channel_id=1, source_target_pairs={{0,2},{1,3},{2,0},{3,1},{4,6},{5,7},{6,4},{7,5},{8,10},{9,11},{10,... | collective-permute-start | bytes 786440 | tf_op jit(solution)/shard_map/ppermute | solution.py:63
  21.1 27.3 %collective-permute-start.8 = (bf16[512,128]{1,0:T(8,128)(2,1)}, bf16[512,128]{1,0:T(8,128)(2,1)S(1)}, u32[]{:S(2)}, u32[]{:S(2)}) collective-permute-start(bf16[512,128]{1,0:T(8,128)(2,1)} %get-tuple-element.41.refs_3_.refs_1_), channel_id=1, source_target_pairs={{0,192},{4,196},{8,200},{12,204},{16,208},{20,212},{24,216},{28,22... | collective-permute-start | bytes 393224 | tf_op jit(solution)/shard_map/ppermute | solution.py:47
  22.6 26.9 %collective-permute-start.7 = (bf16[512,128]{1,0:T(8,128)(2,1)}, bf16[512,128]{1,0:T(8,128)(2,1)S(1)}, u32[]{:S(2)}, u32[]{:S(2)}) collective-permute-start(bf16[512,128]{1,0:T(8,128)(2,1)} %get-tuple-element.41.refs_3_.refs_1_), channel_id=1, source_target_pairs={{0,64},{4,68},{8,72},{12,76},{16,80},{20,84},{24,88},{28,92},{32,9... | collective-permute-start | bytes 393224 | tf_op jit(solution)/shard_map/ppermute | solution.py:47
  25.3 24.4 %collective-permute-start.6 = (bf16[512,128]{1,0:T(8,128)(2,1)}, bf16[512,128]{1,0:T(8,128)(2,1)S(1)}, u32[]{:S(2)}, u32[]{:S(2)}) collective-permute-start(bf16[512,128]{1,0:T(8,128)(2,1)} %get-tuple-element.41.refs_3_.refs_1_), channel_id=1, source_target_pairs={{0,224},{4,228},{8,232},{12,236},{16,240},{20,244},{24,248},{28,25... | collective-permute-start | bytes 393224 | tf_op jit(solution)/shard_map/ppermute | solution.py:47
  26.3 26.4 %collective-permute-start.5 = (bf16[512,128]{1,0:T(8,128)(2,1)}, bf16[512,128]{1,0:T(8,128)(2,1)S(1)}, u32[]{:S(2)}, u32[]{:S(2)}) collective-permute-start(bf16[512,128]{1,0:T(8,128)(2,1)} %get-tuple-element.41.refs_3_.refs_1_), channel_id=1, source_target_pairs={{0,32},{4,36},{8,40},{12,44},{16,48},{20,52},{24,56},{28,60},{32,6... | collective-permute-start | bytes 393224 | tf_op jit(solution)/shard_map/ppermute | solution.py:47
  32.3 7.3 %collective-permute-start.9 = (bf16[32,128]{1,0:T(8,128)(2,1)}, bf16[32,128]{1,0:T(8,128)(2,1)S(1)}, u32[]{:S(2)}, u32[]{:S(2)}) collective-permute-start(bf16[32,128]{1,0:T(8,128)(2,1)} %get-tuple-element.45), channel_id=1, source_target_pairs={{0,4},{4,8},{8,12},{12,16},{16,20},{20,24},{24,28},{28,32},{32,36}... | collective-permute-start | bytes 24584 | tf_op jit(solution)/shard_map/ppermute | solution.py:375
  42.0 5.3 %collective-permute-start.17 = (f32[1,256]{1,0:T(1,128)}, f32[1,256]{1,0:T(1,128)S(1)}, u32[]{:S(2)}, u32[]{:S(2)}) collective-permute-start(f32[1,256]{1,0:T(1,128)} %get-tuple-element.46.s0), channel_id=1, source_target_pairs={{0,2},{1,3},{2,0},{3,1},{4,6},{5,7},{6,4},{7,5},{8,10},{9,11},{10,... | collective-permute-start | bytes 3080 | tf_op jit(solution)/shard_map/ppermute | solution.py:63
  47.3 7.7 %collective-permute-start.14 = (bf16[256,256]{1,0:T(8,128)(2,1)S(1)}, bf16[256,256]{1,0:T(8,128)(2,1)S(1)}, u32[]{:S(2)}, u32[]{:S(2)}) collective-permute-start(bf16[256,256]{1,0:T(8,128)(2,1)S(1)} %copy-done.28), channel_id=1, source_target_pairs={{0,16},{4,20},{8,24},{12,28},{16,0},{20,4},{24,8},{28,12},{32,48},... | collective-permute-start | bytes 393224 | tf_op jit(solution)/shard_map/ppermute | solution.py:47
  48.4 6.7 %collective-permute-start.4 = (bf16[256,256]{1,0:T(8,128)(2,1)S(1)}, bf16[256,256]{1,0:T(8,128)(2,1)S(1)}, u32[]{:S(2)}, u32[]{:S(2)}) collective-permute-start(bf16[256,256]{1,0:T(8,128)(2,1)S(1)} %copy-done.28), channel_id=1, source_target_pairs={{0,24},{4,28},{8,0},{12,4},{16,8},{20,12},{24,16},{28,20},{32,56},... | collective-permute-start | bytes 393224 | tf_op jit(solution)/shard_map/ppermute | solution.py:47
  49.4 5.0 %collective-permute-start.16 = (f32[1,256]{1,0:T(1,128)}, f32[1,256]{1,0:T(1,128)S(1)}, u32[]{:S(2)}, u32[]{:S(2)}) collective-permute-start(f32[1,256]{1,0:T(1,128)} %get-tuple-element.46.s0), channel_id=1, source_target_pairs={{0,3},{1,0},{2,1},{3,2},{4,7},{5,4},{6,5},{7,6},{8,11},{9,8},{10,9... | collective-permute-start | bytes 3080 | tf_op jit(solution)/shard_map/ppermute | solution.py:63
  49.7 4.8 %collective-permute-start.15 = (f32[1,256]{1,0:T(1,128)}, f32[1,256]{1,0:T(1,128)S(1)}, u32[]{:S(2)}, u32[]{:S(2)}) collective-permute-start(f32[1,256]{1,0:T(1,128)} %get-tuple-element.46.s0), channel_id=1, source_target_pairs={{0,1},{1,2},{2,3},{3,0},{4,5},{5,6},{6,7},{7,4},{8,9},{9,10},{10,1... | collective-permute-start | bytes 3080 | tf_op jit(solution)/shard_map/ppermute | solution.py:63
  52.7 2.8 %collective-permute-start.18 = (bf16[512,128]{1,0:T(8,128)(2,1)S(1)}, bf16[512,128]{1,0:T(8,128)(2,1)S(1)}, u32[]{:S(2)}, u32[]{:S(2)}) collective-permute-start(bf16[512,128]{1,0:T(8,128)(2,1)S(1)} %copy-done.10), channel_id=1, source_target_pairs={{0,4},{4,0},{8,12},{12,8},{16,20},{20,16},{24,28},{28,24},{32,36},... | collective-permute-start | bytes 393224 | tf_op jit(solution)/shard_map/ppermute | solution.py:47
  54.4 2.0 %collective-permute-start.19 = (bf16[512,128]{1,0:T(8,128)(2,1)S(1)}, bf16[512,128]{1,0:T(8,128)(2,1)S(1)}, u32[]{:S(2)}, u32[]{:S(2)}) collective-permute-start(bf16[512,128]{1,0:T(8,128)(2,1)S(1)} %collective-permute-done.5.refs_4_.refs_2_), channel_id=1, source_target_pairs={{0,4},{4,0},{8,12},{12,8},{16,20},{20,16},{24,28},{28,24},{32,36},... | collective-permute-start | bytes 393224 | tf_op jit(solution)/shard_map/ppermute | solution.py:47
  54.5 2.0 %collective-permute-start.20 = (bf16[512,128]{1,0:T(8,128)(2,1)S(1)}, bf16[512,128]{1,0:T(8,128)(2,1)S(1)}, u32[]{:S(2)}, u32[]{:S(2)}) collective-permute-start(bf16[512,128]{1,0:T(8,128)(2,1)S(1)} %collective-permute-done.6.refs_5_.refs_3_), channel_id=1, source_target_pairs={{0,4},{4,0},{8,12},{12,8},{16,20},{20,16},{24,28},{28,24},{32,36},... | collective-permute-start | bytes 393224 | tf_op jit(solution)/shard_map/ppermute | solution.py:47
  55.0 3.5 %collective-permute-start.21 = (bf16[512,128]{1,0:T(8,128)(2,1)S(1)}, bf16[512,128]{1,0:T(8,128)(2,1)S(1)}, u32[]{:S(2)}, u32[]{:S(2)}) collective-permute-start(bf16[512,128]{1,0:T(8,128)(2,1)S(1)} %collective-permute-done.7.refs_6_.refs_4_), channel_id=1, source_target_pairs={{0,4},{4,0},{8,12},{12,8},{16,20},{20,16},{24,28},{28,24},{32,36},... | collective-permute-start | bytes 393224 | tf_op jit(solution)/shard_map/ppermute | solution.py:47
  55.1 3.5 %collective-permute-start.22 = (bf16[512,128]{1,0:T(8,128)(2,1)S(1)}, bf16[512,128]{1,0:T(8,128)(2,1)S(1)}, u32[]{:S(2)}, u32[]{:S(2)}) collective-permute-start(bf16[512,128]{1,0:T(8,128)(2,1)S(1)} %collective-permute-done.8.refs_7_.refs_5_), channel_id=1, source_target_pairs={{0,4},{4,0},{8,12},{12,8},{16,20},{20,16},{24,28},{28,24},{32,36},... | collective-permute-start | bytes 393224 | tf_op jit(solution)/shard_map/ppermute | solution.py:47
  55.5 9.1 %collective-permute-start.3 = (bf16[256,256]{1,0:T(8,128)(2,1)S(1)}, bf16[256,256]{1,0:T(8,128)(2,1)S(1)}, u32[]{:S(2)}, u32[]{:S(2)}) collective-permute-start(bf16[256,256]{1,0:T(8,128)(2,1)S(1)} %copy-done.28), channel_id=1, source_target_pairs={{0,8},{4,12},{8,16},{12,20},{16,24},{20,28},{24,0},{28,4},{32,40},... | collective-permute-start | bytes 393224 | tf_op jit(solution)/shard_map/ppermute | solution.py:47
  56.5 22.6 %collective-permute-start.10 = (bf16[512,128]{1,0:T(8,128)(2,1)S(1)}, bf16[512,128]{1,0:T(8,128)(2,1)S(1)}, u32[]{:S(2)}, u32[]{:S(2)}) collective-permute-start(bf16[512,128]{1,0:T(8,128)(2,1)S(1)} %collective-permute-done.7.refs_6_.refs_4_), channel_id=1, source_target_pairs={{0,32},{4,36},{8,40},{12,44},{16,48},{20,52},{24,56},{28,60},{32,6... | collective-permute-start | bytes 393224 | tf_op jit(solution)/shard_map/ppermute | solution.py:47
  56.5 22.6 %collective-permute-start.11 = (bf16[512,128]{1,0:T(8,128)(2,1)S(1)}, bf16[512,128]{1,0:T(8,128)(2,1)S(1)}, u32[]{:S(2)}, u32[]{:S(2)}) collective-permute-start(bf16[512,128]{1,0:T(8,128)(2,1)S(1)} %collective-permute-done.8.refs_7_.refs_5_), channel_id=1, source_target_pairs={{0,224},{4,228},{8,232},{12,236},{16,240},{20,244},{24,248},{28,25... | collective-permute-start | bytes 393224 | tf_op jit(solution)/shard_map/ppermute | solution.py:47
  58.5 20.5 %collective-permute-start.13 = (bf16[256,128]{1,0:T(8,128)(2,1)S(1)}, bf16[256,128]{1,0:T(8,128)(2,1)S(1)}, u32[]{:S(2)}, u32[]{:S(2)}) collective-permute-start(bf16[256,128]{1,0:T(8,128)(2,1)S(1)} %slice.7), channel_id=1, source_target_pairs={{0,192},{4,196},{8,200},{12,204},{16,208},{20,212},{24,216},{28,22... | collective-permute-start | bytes 196616 | tf_op jit(solution)/shard_map/ppermute | solution.py:47
  58.6 20.4 %collective-permute-start.12 = (bf16[256,128]{1,0:T(8,128)(2,1)S(1)}, bf16[256,128]{1,0:T(8,128)(2,1)S(1)}, u32[]{:S(2)}, u32[]{:S(2)}) collective-permute-start(bf16[256,128]{1,0:T(8,128)(2,1)S(1)} %slice.6), channel_id=1, source_target_pairs={{0,64},{4,68},{8,72},{12,76},{16,80},{20,84},{24,88},{28,92},{32,9... | collective-permute-start | bytes 196616 | tf_op jit(solution)/shard_map/ppermute | solution.py:47
  79.1 2.0 %collective-permute-start.23 = (bf16[512,128]{1,0:T(8,128)(2,1)S(1)}, bf16[512,128]{1,0:T(8,128)(2,1)S(1)}, u32[]{:S(2)}, u32[]{:S(2)}) collective-permute-start(bf16[512,128]{1,0:T(8,128)(2,1)S(1)} %collective-permute-done.10.refs_1_.refs_2_.refs_6_), channel_id=1, source_target_pairs={{0,4},{4,0},{8,12},{12,8},{16,20},{20,16},{24,28},{28,24},{32,36},... | collective-permute-start | bytes 393224 | tf_op jit(solution)/shard_map/ppermute | solution.py:47
  79.2 1.9 %collective-permute-start.24 = (bf16[512,128]{1,0:T(8,128)(2,1)S(1)}, bf16[512,128]{1,0:T(8,128)(2,1)S(1)}, u32[]{:S(2)}, u32[]{:S(2)}) collective-permute-start(bf16[512,128]{1,0:T(8,128)(2,1)S(1)} %collective-permute-done.11.refs_2_.refs_3_.refs_7_), channel_id=1, source_target_pairs={{0,4},{4,0},{8,12},{12,8},{16,20},{20,16},{24,28},{28,24},{32,36},... | collective-permute-start | bytes 393224 | tf_op jit(solution)/shard_map/ppermute | solution.py:47
  79.8 1.3 collective-permute-start.26
  95.3 16.0 %collective-permute-start.28 = (bf16[528,256]{1,0:T(8,128)(2,1)}, bf16[528,256]{1,0:T(8,128)(2,1)S(1)}, u32[]{:S(2)}, u32[]{:S(2)}) collective-permute-start(bf16[528,256]{1,0:T(8,128)(2,1)} %get-tuple-element.68), channel_id=1, source_target_pairs={{0,8},{4,12},{8,16},{12,20},{16,24},{20,28},{24,0},{28,4},{32,40},... | collective-permute-start | bytes 811016 | tf_op jit(solution)/shard_map/ppermute | solution.py:47
  95.4 15.9 %collective-permute-start.27 = (bf16[528,256]{1,0:T(8,128)(2,1)}, bf16[528,256]{1,0:T(8,128)(2,1)S(1)}, u32[]{:S(2)}, u32[]{:S(2)}) collective-permute-start(bf16[528,256]{1,0:T(8,128)(2,1)} %get-tuple-element.66), channel_id=1, source_target_pairs={{0,24},{4,28},{8,0},{12,4},{16,8},{20,12},{24,16},{28,20},{32,56},... | collective-permute-start | bytes 811016 | tf_op jit(solution)/shard_map/ppermute | solution.py:47
  98.7 12.7 %collective-permute-start.29 = (bf16[528,256]{1,0:T(8,128)(2,1)S(1)}, bf16[528,256]{1,0:T(8,128)(2,1)S(1)}, u32[]{:S(2)}, u32[]{:S(2)}) collective-permute-start(bf16[528,256]{1,0:T(8,128)(2,1)S(1)} %copy-done.21), channel_id=1, source_target_pairs={{0,16},{4,20},{8,24},{12,28},{16,0},{20,4},{24,8},{28,12},{32,48},... | collective-permute-start | bytes 811016 | tf_op jit(solution)/shard_map/ppermute | solution.py:47
  116.1 14.0 %collective-permute-start.30 = (bf16[64,2048]{1,0:T(8,128)(2,1)}, bf16[64,2048]{1,0:T(8,128)(2,1)S(1)}, u32[]{:S(2)}, u32[]{:S(2)}) collective-permute-start(bf16[64,2048]{1,0:T(8,128)(2,1)} %get-tuple-element.72), channel_id=1, source_target_pairs={{0,1},{1,2},{2,3},{3,0},{4,5},{5,6},{6,7},{7,4},{8,9},{9,10},{10,1... | collective-permute-start | bytes 786440 | tf_op jit(solution)/shard_map/ppermute | solution.py:63
  119.0 14.5 %collective-permute-start.31 = (bf16[64,2048]{1,0:T(8,128)(2,1)}, bf16[64,2048]{1,0:T(8,128)(2,1)S(1)}, u32[]{:S(2)}, u32[]{:S(2)}) collective-permute-start(bf16[64,2048]{1,0:T(8,128)(2,1)} %get-tuple-element.73), channel_id=1, source_target_pairs={{0,3},{1,0},{2,1},{3,2},{4,7},{5,4},{6,5},{7,6},{8,11},{9,8},{10,9... | collective-permute-start | bytes 786440 | tf_op jit(solution)/shard_map/ppermute | solution.py:63
  119.0 14.5 %collective-permute-start.32 = (bf16[64,2048]{1,0:T(8,128)(2,1)}, bf16[64,2048]{1,0:T(8,128)(2,1)S(1)}, u32[]{:S(2)}, u32[]{:S(2)}) collective-permute-start(bf16[64,2048]{1,0:T(8,128)(2,1)} %get-tuple-element.74), channel_id=1, source_target_pairs={{0,2},{1,3},{2,0},{3,1},{4,6},{5,7},{6,4},{7,5},{8,10},{9,11},{10,... | collective-permute-start | bytes 786440 | tf_op jit(solution)/shard_map/ppermute | solution.py:63
  (34 other events, 219.0 us)
where the time goes:
time: 136 us; the launch traced here: 135 us
  Pallas kernels  53.1 us (39%)
  waiting for transfers between devices  38.2 us (28%)
  starting transfers between devices  35.9 us (26%)
  local copies, waits for them, and re-layouts  5.72 us (4%)
  other arithmetic  1.79 us (1%)
    ppermute x9, waiting for transfers between devices, tp_shift(): return lax.ppermute(x, 'tp', [(i, (i + by) % 4) for i in range(4)])  29.5 us
    ppermute x23, starting transfers between devices, along_sp(): return lax.ppermute(x, 'sp', pairs)  22.3 us
    pallas_call x1, Pallas kernels, local(): pl.pallas_call(early_kernel, out_shape=[shape((12, 1, ROWS), F32), shape(...  13.7 us
    pallas_call x2, Pallas kernels, late(): pl.pallas_call(functools.partial(late_kernel, blocks=blocks), out_shape=[...  13.4 us
    ppermute x9, starting transfers between devices, tp_shift(): return lax.ppermute(x, 'tp', [(i, (i + by) % 4) for i in range(4)])  11.8 us
    pallas_call x1, Pallas kernels, local(): pl.pallas_call(self_kernel, out_shape=shape((MSG, ROWS)), in_specs=[VM] +...  10.3 us
    ppermute x1, waiting for transfers between devices, local(): before = lax.ppermute(tail, 'sp', [(i, i + 1) for i in range(63)])  5.36 us
    pallas_call x1, Pallas kernels, local(): pl.pallas_call(project_kernel, out_shape=[sent((256, ROWS)), sent((512, 1...  4.46 us
  transfers between devices with their start and end apart: 33, of which 9 were waited for; matrix products, arithmetic and copies ran while one was open for 1% of the time, Pallas kernels for 23%

commit v1 on v0

v1 whole, which is shorter than its diff:
```python
import functools

import jax
import jax.numpy as jnp
from jax import lax
from jax.experimental import pallas as pl
from jax.experimental.pallas import tpu as pltpu
from jax.sharding import PartitionSpec as P


D = 2048
CONV = 512
QK = 64
VDIM = 128
WIDTH = 31
ROWS = 256
ACC = VDIM + 16
MSG = 4 * VDIM + 16

EPSILON = 1e-06
NEG_BIG = -1e30
HEAD_SCALE = 0.8


F32 = jnp.float32
BF16 = jnp.bfloat16
VM = pl.BlockSpec(memory_space=pltpu.VMEM)
OUT = pl.BlockSpec()
SM = pl.BlockSpec(memory_space=pltpu.SMEM)
ANY = pl.BlockSpec(memory_space=pltpu.MemorySpace.HBM)
BIG = pltpu.CompilerParams(vmem_limit_bytes=56 * 1024 * 1024)
SHIFTS = (1, -1, 2)
DEPTH = 3
LOG2E = 1.4426950408889634


def place(s):
    return s // 8, (s // 2) % 4, s % 2


def along_sp(x, move):
    pairs = []
    for s in range(64):
        z, y, c = place(s)
        z, y, c = move(z, y, c)
        pairs.append((s, z * 8 + y * 2 + c))
    return lax.ppermute(x, "sp", pairs)


def y_shift(x, by):
    return along_sp(x, lambda z, y, c: (z, (y + by) % 4, c))


def core_swap(x):
    return along_sp(x, lambda z, y, c: (z, y, 1 - c))


def tp_shift(x, by):
    return lax.ppermute(x, "tp", [(i, (i + by) % 4) for i in range(4)])


def dot(a, b):
    return jnp.dot(a, b, preferred_element_type=F32)


def fetch(pairs, sems):
    copies = [pltpu.make_async_copy(src, dst, sems.at[i]) for i, (src, dst) in enumerate(pairs)]
    for copy in copies:
        copy.start()
    return copies


def project_kernel(t0, t1, t2, t3, gain, wq, wk, wv, qt, kv, scaled, inv_out, tok, vq, vk, vv, sems):
    x = lax.axis_index("tp")
    copies = fetch([(t, tok.at[i]) for i, t in enumerate((t0, t1, t2, t3))] + [(wk, vk), (wv, vv), (wq, vq)], sems)
    squares = jnp.zeros((ROWS, 128), F32)
    for i, by in enumerate((0,) + SHIFTS):
        j = lax.rem(x - by + 4, 4)
        copies[i].wait()
        wide = tok[i].astype(F32)
        scaled[j] = (wide * gain[pl.ds(j, 1), :]).astype(BF16)
        sq = wide * wide
        squares += (sq[:, 0:128] + sq[:, 128:256]) + (sq[:, 256:384] + sq[:, 384:512])
    inv = lax.rsqrt(jnp.sum(squares, axis=1, keepdims=True) / D + EPSILON)
    inv_out[...] = jnp.broadcast_to(inv, (ROWS, 128))
    rows = jnp.concatenate([scaled[j] for j in range(4)], axis=1)
    copies[4].wait()
    copies[5].wait()
    both = dot(rows, jnp.concatenate([vk[...], vv[...]], axis=1)) * inv
    k = both[:, 0:128].astype(BF16)
    vt = jnp.transpose(both[:, 128:256]).astype(BF16)
    for z in range(8):
        kv[z, 0:256, :] = k
        kv[z, 256:384, :] = vt[:, 0:128]
        kv[z, 384:512, :] = vt[:, 128:256]
    copies[6].wait()
    q = dot(rows, vq[...]) * inv
    qt[...] = jnp.transpose(q * (QK ** -0.5)).astype(BF16)


def rest_kernel(scaled, inv_in, wgv, wgg, wgc, wga, glued, tail, gates):
    inv = inv_in[...]
    wide = jnp.concatenate([inv, inv], axis=1)
    rows = jnp.concatenate([scaled[j] for j in range(4)], axis=1)
    glu = (dot(rows, jnp.concatenate([wgv[...], wgg[...]], axis=1)) * wide).astype(BF16).astype(F32)
    g = (glu[:, 0:128] * jax.nn.sigmoid(glu[:, 128:256])).astype(BF16)
    glued[...] = g
    tail[...] = g[ROWS - 32 :, :]
    gates[:, 0:128] = (dot(rows, wgc[...]) * inv).astype(BF16)
    gates[:, 128:384] = (dot(rows, wga[...]) * wide).astype(BF16)


def conv_kernel(glued, before, weight, conv, squares, padded):
    padded[0:32, :] = before[...].astype(F32)
    padded[32 : 32 + ROWS, :] = glued[...].astype(F32)
    taps = weight[...].astype(F32)
    total = jnp.zeros((ROWS, 128), F32)
    for j in range(WIDTH):
        total += padded[j + 2 : j + 2 + ROWS, :] * taps[j : j + 1, :]
    conv[...] = total
    squares[...] = jnp.sum(jnp.transpose(total * total), axis=0, keepdims=True)


def attend(tiles, kv, slot, queries, maxima, acc, mask=None):
    keys = jnp.concatenate([kv[0, slot, 0:256, :], kv[1, slot, 0:256, :]], axis=0)
    keys = jnp.concatenate([keys, keys], axis=1)
    values = jnp.concatenate(
        [
            kv[0, slot, 256:384, :],
            kv[0, slot, 384:512, :],
            kv[1, slot, 256:384, :],
            kv[1, slot, 384:512, :],
        ],
        axis=1,
    )
    values = jnp.concatenate([values, jnp.ones((ACC - VDIM, 512), BF16)], axis=0)
    ahead = [dot(keys, queries[t]) for t in tiles[:DEPTH]]
    for i, t in enumerate(tiles):
        scores = ahead.pop(0)
        if i + DEPTH < len(tiles):
            ahead.append(dot(keys, queries[tiles[i + DEPTH]]))
        if mask is not None:
            scores = jnp.where(mask, scores, NEG_BIG)
        old = maxima[t]
        new = jnp.maximum(old, jnp.max(scores, axis=0, keepdims=True))
        factor = jnp.exp2(old - new)
        expd = jnp.exp2(scores - new).astype(BF16)
        acc[t] = acc[t] * factor + dot(values, expd)
        maxima[t] = new


def lay_queries(q_refs, queries):
    none = jnp.zeros((64, ROWS), BF16)
    for b, ref in enumerate(q_refs):
        for t in range(4):
            g, m = t // 2, t % 2
            part = ref[g * 128 + m * 64 : g * 128 + m * 64 + 64, :].astype(F32) * LOG2E
            high = part.astype(BF16)
            low = (part - high.astype(F32)).astype(BF16)
            for i, rows in enumerate((high, low)):
                at = i * 128
                queries[b * 4 + t, at + m * 64 : at + m * 64 + 64, :] = rows
                queries[b * 4 + t, at + (1 - m) * 64 : at + (1 - m) * 64 + 64, :] = none


def write_part(out, first, maxima, acc):
    lines = []
    for t in range(4):
        i = first + t
        length = acc[i, VDIM : VDIM + 1, :]
        some = length > 0.0
        safe = jnp.where(some, length, 1.0)
        out[t * VDIM : (t + 1) * VDIM, :] = (acc[i, 0:VDIM, :] * (1.0 / safe)).astype(BF16)
        log = jnp.where(some, maxima[i] + jnp.log2(safe), NEG_BIG)
        for _ in range(3):
            piece = log.astype(BF16).astype(F32)
            lines.append(piece)
            log = log - piece
    lines.append(jnp.zeros((4, ROWS), F32))
    out[4 * VDIM : MSG, :] = jnp.concatenate(lines, axis=0).astype(BF16)


def position():
    s = lax.axis_index("sp")
    return s // 8, lax.rem(s // 2, 4), lax.rem(s, 2)


def bring(own, other, kv, sems):
    c = lax.rem(lax.axis_index("sp"), 2)
    return fetch([(own, kv.at[c]), (other, kv.at[1 - c])], sems)


def start_state(maxima, acc):
    maxima[...] = jnp.full(maxima.shape, NEG_BIG, F32)
    acc[...] = jnp.zeros(acc.shape, F32)


def remote_kernel(q0, q1, q2, own, other, o0, o1, o2, kv, queries, maxima, acc, sems):
    copies = bring(own, other, kv, sems)
    z, y, _ = position()
    lay_queries((q0, q1, q2), queries)
    start_state(maxima, acc)
    for copy in copies:
        copy.wait()

    def visit(i, carry):
        attend(range(12), kv, i, queries, maxima, acc)
        return carry

    lax.fori_loop(0, z, visit, 0)
    for b, by in enumerate(SHIFTS):

        @pl.when(lax.rem(y - by + 4, 4) > y)
        def _(b=b):
            attend(range(4 * b, 4 * b + 4), kv, z, queries, maxima, acc)

    for b, out in enumerate((o0, o1, o2)):
        write_part(out, 4 * b, maxima, acc)


def self_kernel(q0, own, other, out, kv, queries, maxima, acc, sems):
    copies = bring(own, other, kv, sems)
    z, _, c = position()
    lay_queries((q0,), queries)
    start_state(maxima, acc)
    for copy in copies:
        copy.wait()
    key_row = lax.broadcasted_iota(jnp.int32, (512, ROWS), 0)
    query_row = lax.broadcasted_iota(jnp.int32, (512, ROWS), 1) + c * ROWS
    attend(range(4), kv, z, queries, maxima, acc, key_row <= query_row)

    def visit(i, carry):
        attend(range(4), kv, i, queries, maxima, acc)
        return carry

    lax.fori_loop(0, z, visit, 0)
    write_part(out, 0, maxima, acc)


def merge_kernel(m0, m1, m2, m3, conv, s0, s1, s2, s3, c_gain, gates, lam, gain, y0, y1, y2, y3, rows):
    x = lax.axis_index("tp")
    total = (s0[...] + s1[...]) + (s2[...] + s3[...])
    inv = lax.rsqrt(total / CONV + EPSILON)
    inv = jnp.transpose(jnp.broadcast_to(inv, (128, ROWS)))
    normed = conv[...] * inv * c_gain[...]
    y_conv = (jax.nn.silu(normed) * jax.nn.silu(gates[:, 0:128].astype(F32))).astype(BF16)
    for j in range(4):
        rows[j, :, 0:128] = y_conv[64 * j : 64 * j + 64, :]
    logs = []
    for ref in (m0, m1, m2, m3):
        stats = ref[4 * VDIM : MSG, :].astype(F32)
        logs.append([(stats[3 * t : 3 * t + 1] + stats[3 * t + 1 : 3 * t + 2]) + stats[3 * t + 2 : 3 * t + 3] for t in range(4)])
    for g in range(2):
        maps = []
        for m in range(2):
            t = 2 * g + m
            top = functools.reduce(jnp.maximum, [l[t] for l in logs])
            weights = [jnp.exp2(l[t] - top) for l in logs]
            norm = 1.0 / functools.reduce(jnp.add, weights)
            part = [r[t * VDIM : (t + 1) * VDIM, :].astype(F32) * (w * norm) for r, w in zip((m0, m1, m2, m3), weights)]
            maps.append((part[0] + part[1]) + (part[2] + part[3]))
        o = maps[0] - lam[g] * maps[1]
        o = o * lax.rsqrt(jnp.mean(o * o, axis=0, keepdims=True) + EPSILON)
        o = jnp.transpose(o) * gain[...] * HEAD_SCALE
        gate = gates[:, 128 + g * 128 : 256 + g * 128].astype(F32)
        o = (o * jax.nn.silu(gate)).astype(BF16)
        for j in range(4):
            rows[j, :, 128 + g * 128 : 256 + g * 128] = o[64 * j : 64 * j + 64, :]
    for ref, by in zip((y0, y1, y2, y3), (0,) + SHIFTS):
        ref[...] = rows[lax.rem(x + by + 4, 4)]


def output_kernel(y0, y1, y2, y3, w_conv, w_attn, a1, a2, a3, b1, b2, b3, out, held, sems):
    c = lax.rem(lax.axis_index("sp"), 2)
    copies = fetch([(a, held.at[c, i]) for i, a in enumerate((a1, a2, a3))] + [(b, held.at[1 - c, i]) for i, b in enumerate((b1, b2, b3))], sems)
    y = y0[...]
    mine = [dot(y[:, 0:128], w_conv[:, h]) + dot(y[:, 128:384], w_attn[:, h]) for h in (slice(0, 1024), slice(1024, 2048))]
    for copy in copies:
        copy.wait()
    theirs = jnp.concatenate([y1[...], y2[...], y3[...]], axis=1)
    for h in range(2):
        weights = jnp.concatenate([held[h, i] for i in range(3)], axis=0)
        out[:, h * 1024 : (h + 1) * 1024] = (mine[h] + dot(theirs, weights)).astype(BF16)


def shape(dims, kind=BF16):
    return jax.ShapeDtypeStruct(dims, kind)


def sent(dims, kind=BF16):
    return pltpu.MemorySpace.HBM(dims, kind)


def local(
    tokens,
    in_gain,
    w_glu_value,
    w_glu_gate,
    w_query,
    w_key,
    w_value,
    w_gate_conv,
    w_gate_attn,
    conv_weight,
    conv_gain,
    lam,
    head_gain,
    out_conv,
    out_attn,
):
    c = lax.rem(lax.axis_index("sp"), 2)
    half = lax.dynamic_slice_in_dim(jnp.concatenate([out_conv, out_attn], axis=0), c * 1024, 1024, 1)
    pieces = [tokens] + [tp_shift(tokens, by) for by in SHIFTS]
    gain = in_gain.astype(F32).reshape(4, 512)
    qt, kv, scaled, inv = pl.pallas_call(
        project_kernel,
        out_shape=[sent((256, ROWS)), sent((8, 512, 128)), shape((4, ROWS, 512)), shape((ROWS, 128), F32)],
        in_specs=[ANY] * 4 + [VM] + [ANY] * 3,
        out_specs=[OUT] * 2 + [VM] * 2,
        scratch_shapes=[
            pltpu.VMEM((4, ROWS, 512), BF16),
            pltpu.VMEM((D, 256), BF16),
            pltpu.VMEM((D, 128), BF16),
            pltpu.VMEM((D, 128), BF16),
            pltpu.SemaphoreType.DMA((7,)),
        ],
        compiler_params=BIG,
        name="project",
    )(*pieces, gain, w_query, w_key, w_value)

    groups = [[z * 8 + r for z in range(8)] for r in range(8)]
    gathered = lax.all_to_all(kv, "sp", 0, 0, tiled=True, axis_index_groups=groups)
    q_blocks = [y_shift(qt, by) for by in SHIFTS]
    half, scaled = lax.optimization_barrier((half, scaled))
    weights = [tp_shift(half, by) for by in SHIFTS]

    glued, tail, gates = pl.pallas_call(
        rest_kernel,
        out_shape=[shape((ROWS, 128)), sent((32, 128)), shape((ROWS, 384))],
        in_specs=[VM] * 6,
        out_specs=[VM, OUT, VM],
        compiler_params=BIG,
        name="rest",
    )(scaled, inv, w_glu_value, w_glu_gate, w_gate_conv, w_gate_attn)
    before = lax.ppermute(tail, "sp", [(i, i + 1) for i in range(63)])
    conv, squares = pl.pallas_call(
        conv_kernel,
        out_shape=[shape((ROWS, 128), F32), sent((1, ROWS), F32)],
        in_specs=[VM] * 3,
        out_specs=[VM, OUT],
        scratch_shapes=[pltpu.VMEM((32 + ROWS, 128), F32)],
        name="conv",
    )(glued, before, conv_weight)
    sums = [squares] + [tp_shift(squares, by) for by in SHIFTS]

    swapped = core_swap(gathered)

    def scratch(tiles):
        return [
            pltpu.VMEM((2, 8, 512, 128), BF16),
            pltpu.VMEM((tiles, 256, ROWS), BF16),
            pltpu.VMEM((tiles, 1, ROWS), F32),
            pltpu.VMEM((tiles, ACC, ROWS), F32),
            pltpu.SemaphoreType.DMA((2,)),
        ]

    parts = pl.pallas_call(
        remote_kernel,
        out_shape=[sent((MSG, ROWS))] * 3,
        in_specs=[VM] * 3 + [ANY] * 2,
        out_specs=[OUT] * 3,
        scratch_shapes=scratch(12),
        compiler_params=BIG,
        name="remote",
    )(*q_blocks, gathered, swapped)
    back = [y_shift(part, -by) for part, by in zip(parts, SHIFTS)]
    parts, qt, weights = lax.optimization_barrier((parts, qt, weights))
    weights_s = [core_swap(w) for w in weights]
    part = pl.pallas_call(
        self_kernel,
        out_shape=shape((MSG, ROWS)),
        in_specs=[VM] + [ANY] * 2,
        out_specs=VM,
        scratch_shapes=scratch(4),
        compiler_params=BIG,
        name="self",
    )(qt, gathered, swapped)

    rows = pl.pallas_call(
        merge_kernel,
        out_shape=[shape((64, 384))] + [sent((64, 384))] * 3,
        in_specs=[VM] * 11 + [SM, VM],
        out_specs=[VM] + [OUT] * 3,
        scratch_shapes=[pltpu.VMEM((4, 64, 384), BF16)],
        compiler_params=BIG,
        name="merge",
    )(part, *back, conv, *sums, conv_gain.reshape(1, 128), gates, lam, head_gain.reshape(1, 128))
    rows = [rows[0]] + [tp_shift(r, by) for r, by in zip(rows[1:], SHIFTS)]
    return pl.pallas_call(
        output_kernel,
        out_shape=shape((64, D)),
        in_specs=[VM] * 6 + [ANY] * 6,
        out_specs=VM,
        scratch_shapes=[pltpu.VMEM((2, 3, 384, 1024), BF16), pltpu.SemaphoreType.DMA((6,))],
        compiler_params=BIG,
        name="output",
    )(*rows, out_conv, out_attn, *weights, *weights_s)


def solution(mesh):
    in_specs = (
        P("sp", "tp"),
        P(),
        P(None, "tp"),
        P(None, "tp"),
        P(None, "tp"),
        P(None, "tp"),
        P(None, "tp"),
        P(None, "tp"),
        P(None, "tp"),
        P(None, "tp"),
        P("tp"),
        P("tp"),
        P(),
        P("tp", None),
        P("tp", None),
    )
    out_specs = P(("sp", "tp"), None)

    return jax.shard_map(local, mesh=mesh, in_specs=in_specs, out_specs=out_specs, check_vma=False)
```

time: 136 us -> 160 us (1.18)
  the two profiles are of different devices: /device:TPU:230 before, /device:TPU:32 now
where the time goes in v1:
time: 160 us
  waiting for transfers between devices  57 us (36%)
  blocking collectives  33.2 us (21%)
  Pallas kernels  31.3 us (20%)
  starting transfers between devices  29.4 us (18%)
  local copies, waits for them, and re-layouts  6.88 us (4%)
    ppermute x12, waiting for transfers between devices, tp_shift(): return lax.ppermute(x, 'tp', [(i, (i + by) % 4) for i in range(4)])  35.1 us
    all_to_all x1, blocking collectives, local(): lax.all_to_all(kv, 'sp', 0, 0, tiled=True, axis_index_groups=groups)  33.2 us
    ppermute x10, waiting for transfers between devices, along_sp(): return lax.ppermute(x, 'sp', pairs)  16.8 us
    ppermute x12, starting transfers between devices, tp_shift(): return lax.ppermute(x, 'tp', [(i, (i + by) % 4) for i in range(4)])  16.3 us
    ppermute x10, starting transfers between devices, along_sp(): return lax.ppermute(x, 'sp', pairs)  10.9 us
    pallas_call x1, Pallas kernels, local(): pl.pallas_call(remote_kernel, out_shape=[sent((MSG, ROWS))] * 3, in_specs...  8.13 us
    unnamed x50, local copies, waits for them, and re-layouts  5.59 us
    pallas_call x1, Pallas kernels, local(): pl.pallas_call(output_kernel, out_shape=shape((64, D)), in_specs=[VM] * 6...  5.53 us
  transfers between devices with their start and end apart: 23, of which 14 were waited for; matrix products, arithmetic and copies ran while one was open for 2% of the time, Pallas kernels for 13%

profile of v1, /device:TPU:32, one launch (start us, length us, event | category | flops | bytes accessed | tf_op | source)
XLA Modules:
  0.0 159.6 jit_solution(6140193597176760043)
XLA Ops:
  0.0 2.8 %collective-permute-start.1 = (bf16[256,512]{1,0:T(8,128)(2,1)}, bf16[256,512]{1,0:T(8,128)(2,1)S(1)}, u32[]{:S(2)}, u32[]{:S(2)}) collective-permute-start(bf16[256,512]{1,0:T(8,128)(2,1)} %t0.1), channel_id=1, source_target_pairs={{0,3},{1,0},{2,1},{3,2},{4,7},{5,4},{6,5},{7,6},{8,11},{9,8},{10,9... | collective-permute-start | bytes 786440 | tf_op jit(solution)/shard_map/ppermute | solution.py:59
  2.8 2.3 %collective-permute-start.2 = (bf16[256,512]{1,0:T(8,128)(2,1)}, bf16[256,512]{1,0:T(8,128)(2,1)S(1)}, u32[]{:S(2)}, u32[]{:S(2)}) collective-permute-start(bf16[256,512]{1,0:T(8,128)(2,1)} %t0.1), channel_id=1, source_target_pairs={{0,2},{1,3},{2,0},{3,1},{4,6},{5,7},{6,4},{7,5},{8,10},{9,11},{10,... | collective-permute-start | bytes 786440 | tf_op jit(solution)/shard_map/ppermute | solution.py:59
  6.3 7.9 %collective-permute-done.1.t2 = bf16[256,512]{1,0:T(8,128)(2,1)S(1)} collective-permute-done((bf16[256,512]{1,0:T(8,128)(2,1)}, bf16[256,512]{1,0:T(8,128)(2,1)S(1)}, u32[]{:S(2)}, u32[]{:S(2)}) %collective-permute-start.1) | collective-permute-done | bytes 262176 | tf_op jit(solution)/shard_map/ppermute | solution.py:59
  14.3 3.3 %collective-permute-done.t1 = bf16[256,512]{1,0:T(8,128)(2,1)S(1)} collective-permute-done((bf16[256,512]{1,0:T(8,128)(2,1)}, bf16[256,512]{1,0:T(8,128)(2,1)S(1)}, u32[]{:S(2)}, u32[]{:S(2)}) %collective-permute-start) | collective-permute-done | bytes 262176 | tf_op jit(solution)/shard_map/ppermute | solution.py:59
  19.0 4.5 %project.1 = (bf16[256,256]{1,0:T(8,128)(2,1)}, bf16[8,512,128]{2,1,0:T(8,128)(2,1)}, bf16[4,256,512]{2,1,0:T(8,128)(2,1)}, f32[256,128]{1,0:T(8,128)}) custom-call(bf16[256,512]{1,0:T(8,128)(2,1)} %t0.1, bf16[256,512]{1,0:T(8,128)(2,1)} %copy-done.10, bf16[256,512]{1,0:T(8,128)(2,1)} %copy-done.9, bf16[256,512]{1,0:T(8,128)(2,1)} %copy-done.11, ...), custom_call_target="tpu_custom_call" | custom-call | tf_op jit(solution)/shard_map/project/pallas_call | solution.py:315
  23.5 33.2 %all_to_all.5.own = bf16[8,512,128]{2,1,0:T(8,128)(2,1)S(1)} all-to-all(bf16[8,512,128]{2,1,0:T(8,128)(2,1)} %get-tuple-element.28), channel_id=1, replica_groups={{0,32,64,96,128,160,192,224},{4,36,68,100,132,164,196,228},{8,40,72,104..., dimensions={0} | all-to-all | bytes 2097152 | tf_op jit(solution)/shard_map/all_to_all | solution.py:332
  56.7 1.3 fusion
  58.1 1.9 %collective-permute-start.9 = (bf16[384,1024]{1,0:T(8,128)(2,1)S(1)}, bf16[384,1024]{1,0:T(8,128)(2,1)S(1)}, u32[]{:S(2)}, u32[]{:S(2)}) collective-permute-start(bf16[384,1024]{1,0:T(8,128)(2,1)S(1)} %fusion), channel_id=1, source_target_pairs={{0,2},{1,3},{2,0},{3,1},{4,6},{5,7},{6,4},{7,5},{8,10},{9,11},{10,... | collective-permute-start | bytes 2359304 | tf_op jit(solution)/shard_map/ppermute | solution.py:59
  62.0 3.2 %collective-permute-start.5 = (bf16[256,256]{1,0:T(8,128)(2,1)S(1)}, bf16[256,256]{1,0:T(8,128)(2,1)S(1)}, u32[]{:S(2)}, u32[]{:S(2)}) collective-permute-start(bf16[256,256]{1,0:T(8,128)(2,1)S(1)} %copy-done.12), channel_id=1, source_target_pairs={{0,16},{4,20},{8,24},{12,28},{16,0},{20,4},{24,8},{28,12},{32,48},... | collective-permute-start | bytes 393224 | tf_op jit(solution)/shard_map/ppermute | solution.py:47
  65.2 3.3 %collective-permute-done.5.q2 = bf16[256,256]{1,0:T(8,128)(2,1)S(1)} collective-permute-done((bf16[256,256]{1,0:T(8,128)(2,1)S(1)}, bf16[256,256]{1,0:T(8,128)(2,1)S(1)}, u32[]{:S(2)}, u32[]{:S(2)}) %collective-permute-start.5) | collective-permute-done | bytes 131104 | tf_op jit(solution)/shard_map/ppermute | solution.py:47
  68.5 3.0 %collective-permute-start.4 = (bf16[256,256]{1,0:T(8,128)(2,1)S(1)}, bf16[256,256]{1,0:T(8,128)(2,1)S(1)}, u32[]{:S(2)}, u32[]{:S(2)}) collective-permute-start(bf16[256,256]{1,0:T(8,128)(2,1)S(1)} %copy-done.12), channel_id=1, source_target_pairs={{0,24},{4,28},{8,0},{12,4},{16,8},{20,12},{24,16},{28,20},{32,56},... | collective-permute-start | bytes 393224 | tf_op jit(solution)/shard_map/ppermute | solution.py:47
  71.5 2.5 %collective-permute-done.4.q1 = bf16[256,256]{1,0:T(8,128)(2,1)S(1)} collective-permute-done((bf16[256,256]{1,0:T(8,128)(2,1)S(1)}, bf16[256,256]{1,0:T(8,128)(2,1)S(1)}, u32[]{:S(2)}, u32[]{:S(2)}) %collective-permute-start.4) | collective-permute-done | bytes 131104 | tf_op jit(solution)/shard_map/ppermute | solution.py:47
  75.0 5.6 %collective-permute-done.3.q0 = bf16[256,256]{1,0:T(8,128)(2,1)S(1)} collective-permute-done((bf16[256,256]{1,0:T(8,128)(2,1)S(1)}, bf16[256,256]{1,0:T(8,128)(2,1)S(1)}, u32[]{:S(2)}, u32[]{:S(2)}) %collective-permute-start.3) | collective-permute-done | bytes 131104 | tf_op jit(solution)/shard_map/ppermute | solution.py:47
  82.2 8.1 %remote.1 = (bf16[528,256]{1,0:T(8,128)(2,1)}, bf16[528,256]{1,0:T(8,128)(2,1)}, bf16[528,256]{1,0:T(8,128)(2,1)}) custom-call(bf16[256,256]{1,0:T(8,128)(2,1)} %copy-done.15, bf16[256,256]{1,0:T(8,128)(2,1)} %copy-done.14, bf16[256,256]{1,0:T(8,128)(2,1)} %copy-done.13, bf16[8,512,128]{2,1,0:T(8,128)(2,1)} %copy-done, bf16[8,512,128]{2,1,0:T(8,128)(2,1)} %copy-done.2), custom_call_target="tpu_custom_call" | custom-call | tf_op jit(solution)/shard_map/remote/pallas_call | solution.py:367
  90.4 5.5 %collective-permute-done.8.a2 = bf16[384,1024]{1,0:T(8,128)(2,1)} collective-permute-done((bf16[384,1024]{1,0:T(8,128)(2,1)S(1)}, bf16[384,1024]{1,0:T(8,128)(2,1)}, u32[]{:S(2)}, u32[]{:S(2)}) %collective-permute-start.8) | collective-permute-done | bytes 786464 | tf_op jit(solution)/shard_map/ppermute | solution.py:59
  96.8 3.0 %collective-permute-start.10 = (bf16[528,256]{1,0:T(8,128)(2,1)}, bf16[528,256]{1,0:T(8,128)(2,1)S(1)}, u32[]{:S(2)}, u32[]{:S(2)}) collective-permute-start(bf16[528,256]{1,0:T(8,128)(2,1)} %get-tuple-element.29), channel_id=1, source_target_pairs={{0,24},{4,28},{8,0},{12,4},{16,8},{20,12},{24,16},{28,20},{32,56},... | collective-permute-start | bytes 811016 | tf_op jit(solution)/shard_map/ppermute | solution.py:47
  99.8 3.8 %rest.1 = (bf16[256,128]{1,0:T(8,128)(2,1)}, bf16[32,128]{1,0:T(8,128)(2,1)}, bf16[256,384]{1,0:T(8,128)(2,1)}) custom-call(bf16[4,256,512]{2,1,0:T(8,128)(2,1)} %get-tuple-element.35.scaled, f32[256,128]{1,0:T(8,128)} %get-tuple-element.36.inv_in, bf16[2048,128]{1,0:T(8,128)(2,1)} %wgv.1, bf16[2048,128]{1,0:T(8,128)(2,1)} %wgg.1, bf16[2048,128]{1,0:T(8,128)(2,1)} %wgc.1, ...), custom_call_target="tpu_custom_call" | custom-call | tf_op jit(solution)/shard_map/rest/pallas_call | solution.py:337
  103.6 2.1 %collective-permute-start.13 = (bf16[32,128]{1,0:T(8,128)(2,1)}, bf16[32,128]{1,0:T(8,128)(2,1)S(1)}, u32[]{:S(2)}, u32[]{:S(2)}) collective-permute-start(bf16[32,128]{1,0:T(8,128)(2,1)} %get-tuple-element.38), channel_id=1, source_target_pairs={{0,4},{4,8},{8,12},{12,16},{16,20},{20,24},{24,28},{28,32},{32,36}... | collective-permute-start | bytes 24584 | tf_op jit(solution)/shard_map/ppermute | solution.py:345
  105.7 5.2 %collective-permute-done.13.before = bf16[32,128]{1,0:T(8,128)(2,1)S(1)} collective-permute-done((bf16[32,128]{1,0:T(8,128)(2,1)}, bf16[32,128]{1,0:T(8,128)(2,1)S(1)}, u32[]{:S(2)}, u32[]{:S(2)}) %collective-permute-start.13) | collective-permute-done | bytes 8224 | tf_op jit(solution)/shard_map/ppermute | solution.py:345
  111.5 1.8 %conv.1 = (f32[256,128]{1,0:T(8,128)}, f32[1,256]{1,0:T(1,128)}) custom-call(bf16[256,128]{1,0:T(8,128)(2,1)} %get-tuple-element.37.glued, bf16[32,128]{1,0:T(8,128)(2,1)} %copy-done.19, bf16[31,128]{1,0:T(8,128)(2,1)} %weight.1), custom_call_target="tpu_custom_call" | custom-call | tf_op jit(solution)/shard_map/conv/pallas_call | solution.py:346
  113.3 1.8 %collective-permute-start.16 = (f32[1,256]{1,0:T(1,128)}, f32[1,256]{1,0:T(1,128)S(1)}, u32[]{:S(2)}, u32[]{:S(2)}) collective-permute-start(f32[1,256]{1,0:T(1,128)} %get-tuple-element.40.s0), channel_id=1, source_target_pairs={{0,2},{1,3},{2,0},{3,1},{4,6},{5,7},{6,4},{7,5},{8,10},{9,11},{10,... | collective-permute-start | bytes 3080 | tf_op jit(solution)/shard_map/ppermute | solution.py:59
  115.1 3.5 %collective-permute-done.16.s3 = f32[1,256]{1,0:T(1,128)S(1)} collective-permute-done((f32[1,256]{1,0:T(1,128)}, f32[1,256]{1,0:T(1,128)S(1)}, u32[]{:S(2)}, u32[]{:S(2)}) %collective-permute-start.16) | collective-permute-done | bytes 1056 | tf_op jit(solution)/shard_map/ppermute | solution.py:59
  118.6 2.0 %collective-permute-start.15 = (f32[1,256]{1,0:T(1,128)}, f32[1,256]{1,0:T(1,128)S(1)}, u32[]{:S(2)}, u32[]{:S(2)}) collective-permute-start(f32[1,256]{1,0:T(1,128)} %get-tuple-element.40.s0), channel_id=1, source_target_pairs={{0,3},{1,0},{2,1},{3,2},{4,7},{5,4},{6,5},{7,6},{8,11},{9,8},{10,9... | collective-permute-start | bytes 3080 | tf_op jit(solution)/shard_map/ppermute | solution.py:59
  120.6 1.8 %collective-permute-done.15.s2 = f32[1,256]{1,0:T(1,128)S(1)} collective-permute-done((f32[1,256]{1,0:T(1,128)}, f32[1,256]{1,0:T(1,128)S(1)}, u32[]{:S(2)}, u32[]{:S(2)}) %collective-permute-start.15) | collective-permute-done | bytes 1056 | tf_op jit(solution)/shard_map/ppermute | solution.py:59
  122.7 4.7 %collective-permute-done.14.s1 = f32[1,256]{1,0:T(1,128)S(1)} collective-permute-done((f32[1,256]{1,0:T(1,128)}, f32[1,256]{1,0:T(1,128)S(1)}, u32[]{:S(2)}, u32[]{:S(2)}) %collective-permute-start.14) | collective-permute-done | bytes 1056 | tf_op jit(solution)/shard_map/ppermute | solution.py:59
  127.6 5.0 %self.1.m0 = bf16[528,256]{1,0:T(8,128)(2,1)} custom-call(bf16[256,256]{1,0:T(8,128)(2,1)} %get-tuple-element.34.q0, bf16[8,512,128]{2,1,0:T(8,128)(2,1)} %copy-done, bf16[8,512,128]{2,1,0:T(8,128)(2,1)} %copy-done.2), custom_call_target="tpu_custom_call" | custom-call | tf_op jit(solution)/shard_map/self/pallas_call | solution.py:379
  132.7 5.4 %collective-permute-done.11.m2 = bf16[528,256]{1,0:T(8,128)(2,1)S(1)} collective-permute-done((bf16[528,256]{1,0:T(8,128)(2,1)S(1)}, bf16[528,256]{1,0:T(8,128)(2,1)S(1)}, u32[]{:S(2)}, u32[]{:S(2)}) %collective-permute-start.11) | collective-permute-done | bytes 270368 | tf_op jit(solution)/shard_map/ppermute | solution.py:47
  138.8 2.6 %merge.1 = (bf16[64,384]{1,0:T(8,128)(2,1)}, bf16[64,384]{1,0:T(8,128)(2,1)}, bf16[64,384]{1,0:T(8,128)(2,1)}, bf16[64,384]{1,0:T(8,128)(2,1)}) custom-call(bf16[528,256]{1,0:T(8,128)(2,1)} %self.1.m0, bf16[528,256]{1,0:T(8,128)(2,1)} %copy-done.6, bf16[528,256]{1,0:T(8,128)(2,1)} %copy-done.7, bf16[528,256]{1,0:T(8,128)(2,1)} %copy-done.8, ...), custom_call_target="tpu_custom_call" | custom-call | tf_op jit(solution)/shard_map/merge/pallas_call | solution.py:389
  141.4 3.2 %collective-permute-start.18 = (bf16[64,384]{1,0:T(8,128)(2,1)}, bf16[64,384]{1,0:T(8,128)(2,1)S(1)}, u32[]{:S(2)}, u32[]{:S(2)}) collective-permute-start(bf16[64,384]{1,0:T(8,128)(2,1)} %get-tuple-element.44), channel_id=1, source_target_pairs={{0,3},{1,0},{2,1},{3,2},{4,7},{5,4},{6,5},{7,6},{8,11},{9,8},{10,9... | collective-permute-start | bytes 147464 | tf_op jit(solution)/shard_map/ppermute | solution.py:59
  144.6 2.3 %collective-permute-done.17.y1 = bf16[64,384]{1,0:T(8,128)(2,1)S(1)} collective-permute-done((bf16[64,384]{1,0:T(8,128)(2,1)}, bf16[64,384]{1,0:T(8,128)(2,1)S(1)}, u32[]{:S(2)}, u32[]{:S(2)}) %collective-permute-start.17) | collective-permute-done | bytes 49184 | tf_op jit(solution)/shard_map/ppermute | solution.py:59
  146.9 5.8 %collective-permute-done.19.y3 = bf16[64,384]{1,0:T(8,128)(2,1)S(1)} collective-permute-done((bf16[64,384]{1,0:T(8,128)(2,1)}, bf16[64,384]{1,0:T(8,128)(2,1)S(1)}, u32[]{:S(2)}, u32[]{:S(2)}) %collective-permute-start.19) | collective-permute-done | bytes 49184 | tf_op jit(solution)/shard_map/ppermute | solution.py:59
  153.9 5.5 %output.1 = bf16[64,2048]{1,0:T(8,128)(2,1)} custom-call(bf16[64,384]{1,0:T(8,128)(2,1)} %get-tuple-element.42.y0, bf16[64,384]{1,0:T(8,128)(2,1)} %copy-done.16, bf16[64,384]{1,0:T(8,128)(2,1)} %copy-done.17, bf16[64,384]{1,0:T(8,128)(2,1)} %copy-done.18, bf16[128,2048]{1,0:T(8,128)(2,1)} %w_conv.1, bf16[256,2048]{1,0:T(8,128)(2,1)} %w_attn.1, ...), custom_call_target="tpu_custom_call" | custom-call | tf_op jit(solution)/shard_map/output/pallas_call | solution.py:399
  (74 shorter events, 11.3 us)
Async XLA Ops:
  0.0 14.3 %collective-permute-start.1 = (bf16[256,512]{1,0:T(8,128)(2,1)}, bf16[256,512]{1,0:T(8,128)(2,1)S(1)}, u32[]{:S(2)}, u32[]{:S(2)}) collective-permute-start(bf16[256,512]{1,0:T(8,128)(2,1)} %t0.1), channel_id=1, source_target_pairs={{0,3},{1,0},{2,1},{3,2},{4,7},{5,4},{6,5},{7,6},{8,11},{9,8},{10,9... | collective-permute-start | bytes 786440 | tf_op jit(solution)/shard_map/ppermute | solution.py:59
  2.8 14.8 %collective-permute-start = (bf16[256,512]{1,0:T(8,128)(2,1)}, bf16[256,512]{1,0:T(8,128)(2,1)S(1)}, u32[]{:S(2)}, u32[]{:S(2)}) collective-permute-start(bf16[256,512]{1,0:T(8,128)(2,1)} %t0.1), channel_id=1, source_target_pairs={{0,1},{1,2},{2,3},{3,0},{4,5},{5,6},{6,7},{7,4},{8,9},{9,10},{10,1... | collective-permute-start | bytes 786440 | tf_op jit(solution)/shard_map/ppermute | solution.py:59
  2.8 14.8 %collective-permute-start.2 = (bf16[256,512]{1,0:T(8,128)(2,1)}, bf16[256,512]{1,0:T(8,128)(2,1)S(1)}, u32[]{:S(2)}, u32[]{:S(2)}) collective-permute-start(bf16[256,512]{1,0:T(8,128)(2,1)} %t0.1), channel_id=1, source_target_pairs={{0,2},{1,3},{2,0},{3,1},{4,6},{5,7},{6,4},{7,5},{8,10},{9,11},{10,... | collective-permute-start | bytes 786440 | tf_op jit(solution)/shard_map/ppermute | solution.py:59
  23.5 33.3 %copy-start.1 = (bf16[256,2048]{1,0:T(8,128)(2,1)S(1)}, bf16[256,2048]{1,0:T(8,128)(2,1)}, u32[]{:S(2)}) copy-start(bf16[256,2048]{1,0:T(8,128)(2,1)} %w_attn.1) | copy-start | bytes 3145732
  56.7 23.9 %collective-permute-start.6 = (bf16[8,512,128]{2,1,0:T(8,128)(2,1)S(1)}, bf16[8,512,128]{2,1,0:T(8,128)(2,1)S(1)}, u32[]{:S(2)}, u32[]{:S(2)}) collective-permute-start(bf16[8,512,128]{2,1,0:T(8,128)(2,1)S(1)} %all_to_all.5.own), channel_id=1, source_target_pairs={{0,4},{4,0},{8,12},{12,8},{16,20},{20,16},{24,28},{28,24},{32,36},... | collective-permute-start | bytes 3145736 | tf_op jit(solution)/shard_map/ppermute | solution.py:47
  58.1 32.3 %collective-permute-start.9 = (bf16[384,1024]{1,0:T(8,128)(2,1)S(1)}, bf16[384,1024]{1,0:T(8,128)(2,1)S(1)}, u32[]{:S(2)}, u32[]{:S(2)}) collective-permute-start(bf16[384,1024]{1,0:T(8,128)(2,1)S(1)} %fusion), channel_id=1, source_target_pairs={{0,2},{1,3},{2,0},{3,1},{4,6},{5,7},{6,4},{7,5},{8,10},{9,11},{10,... | collective-permute-start | bytes 2359304 | tf_op jit(solution)/shard_map/ppermute | solution.py:59
  60.0 36.0 %collective-permute-start.8 = (bf16[384,1024]{1,0:T(8,128)(2,1)S(1)}, bf16[384,1024]{1,0:T(8,128)(2,1)}, u32[]{:S(2)}, u32[]{:S(2)}) collective-permute-start(bf16[384,1024]{1,0:T(8,128)(2,1)S(1)} %fusion), channel_id=1, source_target_pairs={{0,3},{1,0},{2,1},{3,2},{4,7},{5,4},{6,5},{7,6},{8,11},{9,8},{10,9... | collective-permute-start | bytes 2359304 | tf_op jit(solution)/shard_map/ppermute | solution.py:59
  60.7 35.5 %collective-permute-start.7 = (bf16[384,1024]{1,0:T(8,128)(2,1)S(1)}, bf16[384,1024]{1,0:T(8,128)(2,1)}, u32[]{:S(2)}, u32[]{:S(2)}) collective-permute-start(bf16[384,1024]{1,0:T(8,128)(2,1)S(1)} %fusion), channel_id=1, source_target_pairs={{0,1},{1,2},{2,3},{3,0},{4,5},{5,6},{6,7},{7,4},{8,9},{9,10},{10,1... | collective-permute-start | bytes 2359304 | tf_op jit(solution)/shard_map/ppermute | solution.py:59
  62.0 6.5 %collective-permute-start.5 = (bf16[256,256]{1,0:T(8,128)(2,1)S(1)}, bf16[256,256]{1,0:T(8,128)(2,1)S(1)}, u32[]{:S(2)}, u32[]{:S(2)}) collective-permute-start(bf16[256,256]{1,0:T(8,128)(2,1)S(1)} %copy-done.12), channel_id=1, source_target_pairs={{0,16},{4,20},{8,24},{12,28},{16,0},{20,4},{24,8},{28,12},{32,48},... | collective-permute-start | bytes 393224 | tf_op jit(solution)/shard_map/ppermute | solution.py:47
  68.5 12.2 %copy-start.13 = (bf16[256,256]{1,0:T(8,128)(2,1)}, bf16[256,256]{1,0:T(8,128)(2,1)S(1)}, u32[]{:S(2)}) copy-start(bf16[256,256]{1,0:T(8,128)(2,1)S(1)} %collective-permute-done.5.q2) | copy-start | bytes 393220
  68.5 5.5 %collective-permute-start.4 = (bf16[256,256]{1,0:T(8,128)(2,1)S(1)}, bf16[256,256]{1,0:T(8,128)(2,1)S(1)}, u32[]{:S(2)}, u32[]{:S(2)}) collective-permute-start(bf16[256,256]{1,0:T(8,128)(2,1)S(1)} %copy-done.12), channel_id=1, source_target_pairs={{0,24},{4,28},{8,0},{12,4},{16,8},{20,12},{24,16},{28,20},{32,56},... | collective-permute-start | bytes 393224 | tf_op jit(solution)/shard_map/ppermute | solution.py:47
  74.0 6.6 %copy-start.14 = (bf16[256,256]{1,0:T(8,128)(2,1)}, bf16[256,256]{1,0:T(8,128)(2,1)S(1)}, u32[]{:S(2)}) copy-start(bf16[256,256]{1,0:T(8,128)(2,1)S(1)} %collective-permute-done.4.q1) | copy-start | bytes 393220
  74.0 6.6 %collective-permute-start.3 = (bf16[256,256]{1,0:T(8,128)(2,1)S(1)}, bf16[256,256]{1,0:T(8,128)(2,1)S(1)}, u32[]{:S(2)}, u32[]{:S(2)}) collective-permute-start(bf16[256,256]{1,0:T(8,128)(2,1)S(1)} %copy-done.12), channel_id=1, source_target_pairs={{0,8},{4,12},{8,16},{12,20},{16,24},{20,28},{24,0},{28,4},{32,40},... | collective-permute-start | bytes 393224 | tf_op jit(solution)/shard_map/ppermute | solution.py:47
  90.4 13.2 %copy-start.3 = (bf16[384,1024]{1,0:T(8,128)(2,1)}, bf16[384,1024]{1,0:T(8,128)(2,1)S(1)}, u32[]{:S(2)}) copy-start(bf16[384,1024]{1,0:T(8,128)(2,1)S(1)} %collective-permute-done.9.a3) | copy-start | bytes 2359300
  96.3 56.4 %collective-permute-start.20 = (bf16[384,1024]{1,0:T(8,128)(2,1)}, bf16[384,1024]{1,0:T(8,128)(2,1)S(1)}, u32[]{:S(2)}, u32[]{:S(2)}) collective-permute-start(bf16[384,1024]{1,0:T(8,128)(2,1)} %collective-permute-done.7.a1), channel_id=1, source_target_pairs={{0,4},{4,0},{8,12},{12,8},{16,20},{20,16},{24,28},{28,24},{32,36},... | collective-permute-start | bytes 2359304 | tf_op jit(solution)/shard_map/ppermute | solution.py:47
  96.3 56.4 %collective-permute-start.21 = (bf16[384,1024]{1,0:T(8,128)(2,1)}, bf16[384,1024]{1,0:T(8,128)(2,1)S(1)}, u32[]{:S(2)}, u32[]{:S(2)}) collective-permute-start(bf16[384,1024]{1,0:T(8,128)(2,1)} %collective-permute-done.8.a2), channel_id=1, source_target_pairs={{0,4},{4,0},{8,12},{12,8},{16,20},{20,16},{24,28},{28,24},{32,36},... | collective-permute-start | bytes 2359304 | tf_op jit(solution)/shard_map/ppermute | solution.py:47
  96.8 55.9 %collective-permute-start.22 = (bf16[384,1024]{1,0:T(8,128)(2,1)S(1)}, bf16[384,1024]{1,0:T(8,128)(2,1)}, u32[]{:S(2)}, u32[]{:S(2)}) collective-permute-start(bf16[384,1024]{1,0:T(8,128)(2,1)S(1)} %collective-permute-done.9.a3), channel_id=1, source_target_pairs={{0,4},{4,0},{8,12},{12,8},{16,20},{20,16},{24,28},{28,24},{32,36},... | collective-permute-start | bytes 2359304 | tf_op jit(solution)/shard_map/ppermute | solution.py:47
  96.8 30.6 %collective-permute-start.10 = (bf16[528,256]{1,0:T(8,128)(2,1)}, bf16[528,256]{1,0:T(8,128)(2,1)S(1)}, u32[]{:S(2)}, u32[]{:S(2)}) collective-permute-start(bf16[528,256]{1,0:T(8,128)(2,1)} %get-tuple-element.29), channel_id=1, source_target_pairs={{0,24},{4,28},{8,0},{12,4},{16,8},{20,12},{24,16},{28,20},{32,56},... | collective-permute-start | bytes 811016 | tf_op jit(solution)/shard_map/ppermute | solution.py:47
  99.8 27.6 %copy-start.24 = (bf16[528,256]{1,0:T(8,128)(2,1)S(1)}, bf16[528,256]{1,0:T(8,128)(2,1)}, u32[]{:S(2)}) copy-start(bf16[528,256]{1,0:T(8,128)(2,1)} %get-tuple-element.30) | copy-start | bytes 811012
  99.8 27.6 %copy-start.23 = (bf16[528,256]{1,0:T(8,128)(2,1)S(1)}, bf16[528,256]{1,0:T(8,128)(2,1)}, u32[]{:S(2)}) copy-start(bf16[528,256]{1,0:T(8,128)(2,1)} %get-tuple-element.31) | copy-start | bytes 811012
  103.6 7.3 %collective-permute-start.13 = (bf16[32,128]{1,0:T(8,128)(2,1)}, bf16[32,128]{1,0:T(8,128)(2,1)S(1)}, u32[]{:S(2)}, u32[]{:S(2)}) collective-permute-start(bf16[32,128]{1,0:T(8,128)(2,1)} %get-tuple-element.38), channel_id=1, source_target_pairs={{0,4},{4,8},{8,12},{12,16},{16,20},{20,24},{24,28},{28,32},{32,36}... | collective-permute-start | bytes 24584 | tf_op jit(solution)/shard_map/ppermute | solution.py:345
  113.3 5.3 %collective-permute-start.16 = (f32[1,256]{1,0:T(1,128)}, f32[1,256]{1,0:T(1,128)S(1)}, u32[]{:S(2)}, u32[]{:S(2)}) collective-permute-start(f32[1,256]{1,0:T(1,128)} %get-tuple-element.40.s0), channel_id=1, source_target_pairs={{0,2},{1,3},{2,0},{3,1},{4,6},{5,7},{6,4},{7,5},{8,10},{9,11},{10,... | collective-permute-start | bytes 3080 | tf_op jit(solution)/shard_map/ppermute | solution.py:59
  118.6 14.0 %copy-start.20 = (f32[1,256]{1,0:T(1,128)}, f32[1,256]{1,0:T(1,128)S(1)}, u32[]{:S(2)}) copy-start(f32[1,256]{1,0:T(1,128)S(1)} %collective-permute-done.16.s3) | copy-start | bytes 3076
  118.6 3.8 %collective-permute-start.15 = (f32[1,256]{1,0:T(1,128)}, f32[1,256]{1,0:T(1,128)S(1)}, u32[]{:S(2)}, u32[]{:S(2)}) collective-permute-start(f32[1,256]{1,0:T(1,128)} %get-tuple-element.40.s0), channel_id=1, source_target_pairs={{0,3},{1,0},{2,1},{3,2},{4,7},{5,4},{6,5},{7,6},{8,11},{9,8},{10,9... | collective-permute-start | bytes 3080 | tf_op jit(solution)/shard_map/ppermute | solution.py:59
  122.4 10.3 %copy-start.21 = (f32[1,256]{1,0:T(1,128)}, f32[1,256]{1,0:T(1,128)S(1)}, u32[]{:S(2)}) copy-start(f32[1,256]{1,0:T(1,128)S(1)} %collective-permute-done.15.s2) | copy-start | bytes 3076
  122.4 5.0 %collective-permute-start.14 = (f32[1,256]{1,0:T(1,128)}, f32[1,256]{1,0:T(1,128)S(1)}, u32[]{:S(2)}, u32[]{:S(2)}) collective-permute-start(f32[1,256]{1,0:T(1,128)} %get-tuple-element.40.s0), channel_id=1, source_target_pairs={{0,1},{1,2},{2,3},{3,0},{4,5},{5,6},{6,7},{7,4},{8,9},{9,10},{10,1... | collective-permute-start | bytes 3080 | tf_op jit(solution)/shard_map/ppermute | solution.py:59
  127.4 10.6 %collective-permute-start.11 = (bf16[528,256]{1,0:T(8,128)(2,1)S(1)}, bf16[528,256]{1,0:T(8,128)(2,1)S(1)}, u32[]{:S(2)}, u32[]{:S(2)}) collective-permute-start(bf16[528,256]{1,0:T(8,128)(2,1)S(1)} %copy-done.24), channel_id=1, source_target_pairs={{0,8},{4,12},{8,16},{12,20},{16,24},{20,28},{24,0},{28,4},{32,40},... | collective-permute-start | bytes 811016 | tf_op jit(solution)/shard_map/ppermute | solution.py:47
  127.4 10.6 %collective-permute-start.12 = (bf16[528,256]{1,0:T(8,128)(2,1)S(1)}, bf16[528,256]{1,0:T(8,128)(2,1)S(1)}, u32[]{:S(2)}, u32[]{:S(2)}) collective-permute-start(bf16[528,256]{1,0:T(8,128)(2,1)S(1)} %copy-done.23), channel_id=1, source_target_pairs={{0,16},{4,20},{8,24},{12,28},{16,0},{20,4},{24,8},{28,12},{32,48},... | collective-permute-start | bytes 811016 | tf_op jit(solution)/shard_map/ppermute | solution.py:47
  141.4 5.5 %collective-permute-start.17 = (bf16[64,384]{1,0:T(8,128)(2,1)}, bf16[64,384]{1,0:T(8,128)(2,1)S(1)}, u32[]{:S(2)}, u32[]{:S(2)}) collective-permute-start(bf16[64,384]{1,0:T(8,128)(2,1)} %get-tuple-element.43), channel_id=1, source_target_pairs={{0,1},{1,2},{2,3},{3,0},{4,5},{5,6},{6,7},{7,4},{8,9},{9,10},{10,1... | collective-permute-start | bytes 147464 | tf_op jit(solution)/shard_map/ppermute | solution.py:59
  141.4 5.5 %collective-permute-start.18 = (bf16[64,384]{1,0:T(8,128)(2,1)}, bf16[64,384]{1,0:T(8,128)(2,1)S(1)}, u32[]{:S(2)}, u32[]{:S(2)}) collective-permute-start(bf16[64,384]{1,0:T(8,128)(2,1)} %get-tuple-element.44), channel_id=1, source_target_pairs={{0,3},{1,0},{2,1},{3,2},{4,7},{5,4},{6,5},{7,6},{8,11},{9,8},{10,9... | collective-permute-start | bytes 147464 | tf_op jit(solution)/shard_map/ppermute | solution.py:59
  146.9 5.8 %copy-start.16 = (bf16[64,384]{1,0:T(8,128)(2,1)}, bf16[64,384]{1,0:T(8,128)(2,1)S(1)}, u32[]{:S(2)}) copy-start(bf16[64,384]{1,0:T(8,128)(2,1)S(1)} %collective-permute-done.17.y1) | copy-start | bytes 147460
  146.9 5.8 %collective-permute-start.19 = (bf16[64,384]{1,0:T(8,128)(2,1)}, bf16[64,384]{1,0:T(8,128)(2,1)S(1)}, u32[]{:S(2)}, u32[]{:S(2)}) collective-permute-start(bf16[64,384]{1,0:T(8,128)(2,1)} %get-tuple-element.45), channel_id=1, source_target_pairs={{0,2},{1,3},{2,0},{3,1},{4,6},{5,7},{6,4},{7,5},{8,10},{9,11},{10,... | collective-permute-start | bytes 147464 | tf_op jit(solution)/shard_map/ppermute | solution.py:59
  (16 other events, 34.0 us)

commit v2 on v1

--- a/solution.py
+++ b/solution.py
@@ -63,51 +63,39 @@
     return jnp.dot(a, b, preferred_element_type=F32)
 
 
-def fetch(pairs, sems):
-    copies = [pltpu.make_async_copy(src, dst, sems.at[i]) for i, (src, dst) in enumerate(pairs)]
-    for copy in copies:
-        copy.start()
-    return copies
-
-
-def project_kernel(t0, t1, t2, t3, gain, wq, wk, wv, qt, kv, scaled, inv_out, tok, vq, vk, vv, sems):
+def project_kernel(t0, t1, t2, t3, gain, weights, qt, kv, scaled, inv_out):
     x = lax.axis_index("tp")
-    copies = fetch([(t, tok.at[i]) for i, t in enumerate((t0, t1, t2, t3))] + [(wk, vk), (wv, vv), (wq, vq)], sems)
     squares = jnp.zeros((ROWS, 128), F32)
-    for i, by in enumerate((0,) + SHIFTS):
+    for ref, by in zip((t0, t1, t2, t3), (0,) + SHIFTS):
         j = lax.rem(x - by + 4, 4)
-        copies[i].wait()
-        wide = tok[i].astype(F32)
+        wide = ref[...].astype(F32)
         scaled[j] = (wide * gain[pl.ds(j, 1), :]).astype(BF16)
         sq = wide * wide
         squares += (sq[:, 0:128] + sq[:, 128:256]) + (sq[:, 256:384] + sq[:, 384:512])
     inv = lax.rsqrt(jnp.sum(squares, axis=1, keepdims=True) / D + EPSILON)
     inv_out[...] = jnp.broadcast_to(inv, (ROWS, 128))
     rows = jnp.concatenate([scaled[j] for j in range(4)], axis=1)
-    copies[4].wait()
-    copies[5].wait()
-    both = dot(rows, jnp.concatenate([vk[...], vv[...]], axis=1)) * inv
+    both = dot(rows, weights[:, 256:512]) * inv
     k = both[:, 0:128].astype(BF16)
     vt = jnp.transpose(both[:, 128:256]).astype(BF16)
     for z in range(8):
         kv[z, 0:256, :] = k
         kv[z, 256:384, :] = vt[:, 0:128]
         kv[z, 384:512, :] = vt[:, 128:256]
-    copies[6].wait()
-    q = dot(rows, vq[...]) * inv
+    q = dot(rows, weights[:, 0:256]) * inv
     qt[...] = jnp.transpose(q * (QK ** -0.5)).astype(BF16)
 
 
-def rest_kernel(scaled, inv_in, wgv, wgg, wgc, wga, glued, tail, gates):
+def rest_kernel(scaled, inv_in, weights, glued, tail, gates):
     inv = inv_in[...]
     wide = jnp.concatenate([inv, inv], axis=1)
     rows = jnp.concatenate([scaled[j] for j in range(4)], axis=1)
-    glu = (dot(rows, jnp.concatenate([wgv[...], wgg[...]], axis=1)) * wide).astype(BF16).astype(F32)
+    glu = (dot(rows, weights[:, 0:256]) * wide).astype(BF16).astype(F32)
     g = (glu[:, 0:128] * jax.nn.sigmoid(glu[:, 128:256])).astype(BF16)
     glued[...] = g
     tail[...] = g[ROWS - 32 :, :]
-    gates[:, 0:128] = (dot(rows, wgc[...]) * inv).astype(BF16)
-    gates[:, 128:384] = (dot(rows, wga[...]) * wide).astype(BF16)
+    gates[:, 128:384] = (dot(rows, weights[:, 256:512]) * wide).astype(BF16)
+    gates[:, 0:128] = (dot(rows, weights[:, 512:640]) * inv).astype(BF16)
 
 
 def conv_kernel(glued, before, weight, conv, squares, padded):
@@ -121,15 +109,15 @@
     squares[...] = jnp.sum(jnp.transpose(total * total), axis=0, keepdims=True)
 
 
-def attend(tiles, kv, slot, queries, maxima, acc, mask=None):
-    keys = jnp.concatenate([kv[0, slot, 0:256, :], kv[1, slot, 0:256, :]], axis=0)
+def attend(tiles, own, other, slot, queries, maxima, acc, mask=None):
+    keys = jnp.concatenate([own[slot, 0:256, :], other[slot, 0:256, :]], axis=0)
     keys = jnp.concatenate([keys, keys], axis=1)
     values = jnp.concatenate(
         [
-            kv[0, slot, 256:384, :],
-            kv[0, slot, 384:512, :],
-            kv[1, slot, 256:384, :],
-            kv[1, slot, 384:512, :],
+            own[slot, 256:384, :],
+            own[slot, 384:512, :],
+            other[slot, 256:384, :],
+            other[slot, 384:512, :],
         ],
         axis=1,
     )
@@ -185,26 +173,18 @@
     return s // 8, lax.rem(s // 2, 4), lax.rem(s, 2)
 
 
-def bring(own, other, kv, sems):
-    c = lax.rem(lax.axis_index("sp"), 2)
-    return fetch([(own, kv.at[c]), (other, kv.at[1 - c])], sems)
-
-
 def start_state(maxima, acc):
     maxima[...] = jnp.full(maxima.shape, NEG_BIG, F32)
     acc[...] = jnp.zeros(acc.shape, F32)
 
 
-def remote_kernel(q0, q1, q2, own, other, o0, o1, o2, kv, queries, maxima, acc, sems):
-    copies = bring(own, other, kv, sems)
+def remote_kernel(q0, q1, q2, own, other, o0, o1, o2, queries, maxima, acc):
     z, y, _ = position()
     lay_queries((q0, q1, q2), queries)
     start_state(maxima, acc)
-    for copy in copies:
-        copy.wait()
 
     def visit(i, carry):
-        attend(range(12), kv, i, queries, maxima, acc)
+        attend(range(12), own, other, i, queries, maxima, acc)
         return carry
 
     lax.fori_loop(0, z, visit, 0)
@@ -212,25 +192,23 @@
 
         @pl.when(lax.rem(y - by + 4, 4) > y)
         def _(b=b):
-            attend(range(4 * b, 4 * b + 4), kv, z, queries, maxima, acc)
+            attend(range(4 * b, 4 * b + 4), own, other, z, queries, maxima, acc)
 
     for b, out in enumerate((o0, o1, o2)):
         write_part(out, 4 * b, maxima, acc)
 
 
-def self_kernel(q0, own, other, out, kv, queries, maxima, acc, sems):
-    copies = bring(own, other, kv, sems)
+def self_kernel(q0, own, other, out, queries, maxima, acc):
     z, _, c = position()
     lay_queries((q0,), queries)
     start_state(maxima, acc)
-    for copy in copies:
-        copy.wait()
-    key_row = lax.broadcasted_iota(jnp.int32, (512, ROWS), 0)
+    row = lax.broadcasted_iota(jnp.int32, (512, ROWS), 0)
+    key_row = jnp.where(row < ROWS, row + c * ROWS, row - c * ROWS)
     query_row = lax.broadcasted_iota(jnp.int32, (512, ROWS), 1) + c * ROWS
-    attend(range(4), kv, z, queries, maxima, acc, key_row <= query_row)
+    attend(range(4), own, other, z, queries, maxima, acc, key_row <= query_row)
 
     def visit(i, carry):
-        attend(range(4), kv, i, queries, maxima, acc)
+        attend(range(4), own, other, i, queries, maxima, acc)
         return carry
 
     lax.fori_loop(0, z, visit, 0)
@@ -270,17 +248,15 @@
         ref[...] = rows[lax.rem(x + by + 4, 4)]
 
 
-def output_kernel(y0, y1, y2, y3, w_conv, w_attn, a1, a2, a3, b1, b2, b3, out, held, sems):
+def output_kernel(y0, y1, y2, y3, w_conv, w_attn, a1, a2, a3, b1, b2, b3, out):
     c = lax.rem(lax.axis_index("sp"), 2)
-    copies = fetch([(a, held.at[c, i]) for i, a in enumerate((a1, a2, a3))] + [(b, held.at[1 - c, i]) for i, b in enumerate((b1, b2, b3))], sems)
     y = y0[...]
-    mine = [dot(y[:, 0:128], w_conv[:, h]) + dot(y[:, 128:384], w_attn[:, h]) for h in (slice(0, 1024), slice(1024, 2048))]
-    for copy in copies:
-        copy.wait()
     theirs = jnp.concatenate([y1[...], y2[...], y3[...]], axis=1)
-    for h in range(2):
-        weights = jnp.concatenate([held[h, i] for i in range(3)], axis=0)
-        out[:, h * 1024 : (h + 1) * 1024] = (mine[h] + dot(theirs, weights)).astype(BF16)
+    for half, refs in ((c, (a1, a2, a3)), (1 - c, (b1, b2, b3))):
+        at = pl.ds(pl.multiple_of(half * 1024, 1024), 1024)
+        mine = dot(y[:, 0:128], w_conv[:, at]) + dot(y[:, 128:384], w_attn[:, at])
+        weights = jnp.concatenate([r[...] for r in refs], axis=0)
+        out[:, at] = (mine + dot(theirs, weights)).astype(BF16)
 
 
 def shape(dims, kind=BF16):
@@ -312,36 +288,30 @@
     half = lax.dynamic_slice_in_dim(jnp.concatenate([out_conv, out_attn], axis=0), c * 1024, 1024, 1)
     pieces = [tokens] + [tp_shift(tokens, by) for by in SHIFTS]
     gain = in_gain.astype(F32).reshape(4, 512)
+    first = jnp.concatenate([w_query, w_key, w_value], axis=1)
+    second = jnp.concatenate([w_glu_value, w_glu_gate, w_gate_attn, w_gate_conv], axis=1)
     qt, kv, scaled, inv = pl.pallas_call(
         project_kernel,
         out_shape=[sent((256, ROWS)), sent((8, 512, 128)), shape((4, ROWS, 512)), shape((ROWS, 128), F32)],
-        in_specs=[ANY] * 4 + [VM] + [ANY] * 3,
+        in_specs=[VM] * 6,
         out_specs=[OUT] * 2 + [VM] * 2,
-        scratch_shapes=[
-            pltpu.VMEM((4, ROWS, 512), BF16),
-            pltpu.VMEM((D, 256), BF16),
-            pltpu.VMEM((D, 128), BF16),
-            pltpu.VMEM((D, 128), BF16),
-            pltpu.SemaphoreType.DMA((7,)),
-        ],
         compiler_params=BIG,
         name="project",
-    )(*pieces, gain, w_query, w_key, w_value)
+    )(*pieces, gain, first)
 
     groups = [[z * 8 + r for z in range(8)] for r in range(8)]
     gathered = lax.all_to_all(kv, "sp", 0, 0, tiled=True, axis_index_groups=groups)
     q_blocks = [y_shift(qt, by) for by in SHIFTS]
-    half, scaled = lax.optimization_barrier((half, scaled))
     weights = [tp_shift(half, by) for by in SHIFTS]
 
     glued, tail, gates = pl.pallas_call(
         rest_kernel,
         out_shape=[shape((ROWS, 128)), sent((32, 128)), shape((ROWS, 384))],
-        in_specs=[VM] * 6,
+        in_specs=[VM] * 3,
         out_specs=[VM, OUT, VM],
         compiler_params=BIG,
         name="rest",
-    )(scaled, inv, w_glu_value, w_glu_gate, w_gate_conv, w_gate_attn)
+    )(scaled, inv, second)
     before = lax.ppermute(tail, "sp", [(i, i + 1) for i in range(63)])
     conv, squares = pl.pallas_call(
         conv_kernel,
@@ -357,17 +327,15 @@
 
     def scratch(tiles):
         return [
-            pltpu.VMEM((2, 8, 512, 128), BF16),
             pltpu.VMEM((tiles, 256, ROWS), BF16),
             pltpu.VMEM((tiles, 1, ROWS), F32),
             pltpu.VMEM((tiles, ACC, ROWS), F32),
-            pltpu.SemaphoreType.DMA((2,)),
         ]
 
     parts = pl.pallas_call(
         remote_kernel,
         out_shape=[sent((MSG, ROWS))] * 3,
-        in_specs=[VM] * 3 + [ANY] * 2,
+        in_specs=[VM] * 5,
         out_specs=[OUT] * 3,
         scratch_shapes=scratch(12),
         compiler_params=BIG,
@@ -379,7 +347,7 @@
     part = pl.pallas_call(
         self_kernel,
         out_shape=shape((MSG, ROWS)),
-        in_specs=[VM] + [ANY] * 2,
+        in_specs=[VM] * 3,
         out_specs=VM,
         scratch_shapes=scratch(4),
         compiler_params=BIG,
@@ -399,9 +367,8 @@
     return pl.pallas_call(
         output_kernel,
         out_shape=shape((64, D)),
-        in_specs=[VM] * 6 + [ANY] * 6,
+        in_specs=[VM] * 12,
         out_specs=VM,
-        scratch_shapes=[pltpu.VMEM((2, 3, 384, 1024), BF16), pltpu.SemaphoreType.DMA((6,))],
         compiler_params=BIG,
         name="output",
     )(*rows, out_conv, out_attn, *weights, *weights_s)

time: 160 us -> 160 us (level)
  other arithmetic: 1.32 us -> 6.14 us
  Pallas kernels: 31.3 us -> 29 us
  starting transfers between devices: 29.4 us -> 27.2 us
  blocking collectives: 33.2 us -> 35.1 us
    concatenate x0 -> x2, other arithmetic: none -> 4.72 us  [the longest x1 3.08 us: local(): first = jnp.concatenate([w_query, w_key, w_value], axis=1)]
    ppermute x12, waiting for transfers between devices: 35.1 us -> 31.8 us  [tp_shift(): return lax.ppermute(x, 'tp', [(i, (i + by) % 4) for i in range(4)])]
    ppermute x10, waiting for transfers between devices: 16.8 us -> 18.8 us  [along_sp(): return lax.ppermute(x, 'sp', pairs)]
    all_to_all x1, blocking collectives: 33.2 us -> 35.1 us  [local(): lax.all_to_all(kv, 'sp', 0, 0, tiled=True, axis_index_groups=groups)]
    ppermute x10, starting transfers between devices: 10.9 us -> 9.1 us  [along_sp(): return lax.ppermute(x, 'sp', pairs)]
    pallas_call x2, Pallas kernels: 10.6 us -> 8.93 us  [the longest x1 4.79 us: local(): pl.pallas_call(output_kernel, out_shape=shape((64, D)), in_specs=[VM] * 1...]
    unnamed x50 -> x58, local copies, waits for them, and re-layouts: 5.59 us -> 4.92 us
  transfers between devices with their start and end apart: 23 -> 23, of which waited for: 14 -> 14; matrix products, arithmetic and copies ran while one was open for 2% -> 5% of each run, Pallas kernels for 13% -> 13%
where the time goes in v2:
time: 160 us
  waiting for transfers between devices  55.8 us (35%)
  blocking collectives  35.1 us (22%)
  Pallas kernels  29 us (18%)
  starting transfers between devices  27.2 us (17%)
  local copies, waits for them, and re-layouts  6.21 us (4%)
  other arithmetic  6.14 us (4%)
    all_to_all x1, blocking collectives, local(): lax.all_to_all(kv, 'sp', 0, 0, tiled=True, axis_index_groups=groups)  35.1 us
    ppermute x12, waiting for transfers between devices, tp_shift(): return lax.ppermute(x, 'tp', [(i, (i + by) % 4) for i in range(4)])  31.8 us
    ppermute x10, waiting for transfers between devices, along_sp(): return lax.ppermute(x, 'sp', pairs)  18.8 us
    ppermute x12, starting transfers between devices, tp_shift(): return lax.ppermute(x, 'tp', [(i, (i + by) % 4) for i in range(4)])  16 us
    ppermute x10, starting transfers between devices, along_sp(): return lax.ppermute(x, 'sp', pairs)  9.1 us
    pallas_call x1, Pallas kernels, local(): pl.pallas_call(remote_kernel, out_shape=[sent((MSG, ROWS))] * 3, in_specs...  7.61 us
    ppermute x1, waiting for transfers between devices, local(): before = lax.ppermute(tail, 'sp', [(i, i + 1) for i in range(63)])  5.24 us
    unnamed x58, local copies, waits for them, and re-layouts  4.92 us
  transfers between devices with their start and end apart: 23, of which 14 were waited for; matrix products, arithmetic and copies ran while one was open for 5% of the time, Pallas kernels for 13%

profile of v2, /device:TPU:32, one launch (start us, length us, event | category | flops | bytes accessed | tf_op | source)
XLA Modules:
  0.0 159.7 jit_solution(5310754168710705204)
XLA Ops:
  1.5 1.7 %collective-permute-start.1 = (bf16[256,512]{1,0:T(8,128)(2,1)}, bf16[256,512]{1,0:T(8,128)(2,1)S(1)}, u32[]{:S(2)}, u32[]{:S(2)}) collective-permute-start(bf16[256,512]{1,0:T(8,128)(2,1)} %t0.1), channel_id=1, source_target_pairs={{0,3},{1,0},{2,1},{3,2},{4,7},{5,4},{6,5},{7,6},{8,11},{9,8},{10,9... | collective-permute-start | bytes 786440 | tf_op jit(solution)/shard_map/ppermute | solution.py:59
  3.2 1.8 %collective-permute-start.2 = (bf16[256,512]{1,0:T(8,128)(2,1)}, bf16[256,512]{1,0:T(8,128)(2,1)S(1)}, u32[]{:S(2)}, u32[]{:S(2)}) collective-permute-start(bf16[256,512]{1,0:T(8,128)(2,1)} %t0.1), channel_id=1, source_target_pairs={{0,2},{1,3},{2,0},{3,1},{4,6},{5,7},{6,4},{7,5},{8,10},{9,11},{10,... | collective-permute-start | bytes 786440 | tf_op jit(solution)/shard_map/ppermute | solution.py:59
  6.3 3.1 %pad_maximum_fusion.1.weights = bf16[2048,512]{1,0:T(8,128)(2,1)} fusion(bf16[2048,128]{1,0:T(8,128)(2,1)} %param.21, bf16[2048,128]{1,0:T(8,128)(2,1)} %param.20, bf16[2048,256]{1,0:T(8,128)(2,1)} %param.19), kind=kLoop, calls=%fused_computation.1 | loop fusion | flops 6291456 | bytes 4194304 | tf_op jit(solution)/shard_map/concatenate | solution.py:291
  9.6 4.9 %collective-permute-done.1.t2 = bf16[256,512]{1,0:T(8,128)(2,1)S(1)} collective-permute-done((bf16[256,512]{1,0:T(8,128)(2,1)}, bf16[256,512]{1,0:T(8,128)(2,1)S(1)}, u32[]{:S(2)}, u32[]{:S(2)}) %collective-permute-start.1) | collective-permute-done | bytes 262176 | tf_op jit(solution)/shard_map/ppermute | solution.py:59
  14.5 1.6 collective-permute-done.2.t3
  16.8 4.3 %project.1 = (bf16[256,256]{1,0:T(8,128)(2,1)}, bf16[8,512,128]{2,1,0:T(8,128)(2,1)}, bf16[4,256,512]{2,1,0:T(8,128)(2,1)}, f32[256,128]{1,0:T(8,128)}) custom-call(bf16[256,512]{1,0:T(8,128)(2,1)} %t0.1, bf16[256,512]{1,0:T(8,128)(2,1)} %copy-done.13, bf16[256,512]{1,0:T(8,128)(2,1)} %copy-done.14, bf16[256,512]{1,0:T(8,128)(2,1)} %copy-done.15, ...), custom_call_target="tpu_custom_call" | custom-call | tf_op jit(solution)/shard_map/project/pallas_call | solution.py:293
  21.0 35.1 %all_to_all.5.own = bf16[8,512,128]{2,1,0:T(8,128)(2,1)S(1)} all-to-all(bf16[8,512,128]{2,1,0:T(8,128)(2,1)} %get-tuple-element.26), channel_id=1, replica_groups={{0,32,64,96,128,160,192,224},{4,36,68,100,132,164,196,228},{8,40,72,104..., dimensions={0} | all-to-all | bytes 2097152 | tf_op jit(solution)/shard_map/all_to_all | solution.py:303
  58.6 2.4 %collective-permute-start.8 = (bf16[384,1024]{1,0:T(8,128)(2,1)S(1)}, bf16[384,1024]{1,0:T(8,128)(2,1)}, u32[]{:S(2)}, u32[]{:S(2)}) collective-permute-start(bf16[384,1024]{1,0:T(8,128)(2,1)S(1)} %fusion), channel_id=1, source_target_pairs={{0,3},{1,0},{2,1},{3,2},{4,7},{5,4},{6,5},{7,6},{8,11},{9,8},{10,9... | collective-permute-start | bytes 2359304 | tf_op jit(solution)/shard_map/ppermute | solution.py:59
  62.5 4.8 %collective-permute-done.3.q0 = bf16[256,256]{1,0:T(8,128)(2,1)S(1)} collective-permute-done((bf16[256,256]{1,0:T(8,128)(2,1)S(1)}, bf16[256,256]{1,0:T(8,128)(2,1)S(1)}, u32[]{:S(2)}, u32[]{:S(2)}) %collective-permute-start.3) | collective-permute-done | bytes 131104 | tf_op jit(solution)/shard_map/ppermute | solution.py:47
  67.3 1.7 %collective-permute-start.4 = (bf16[256,256]{1,0:T(8,128)(2,1)S(1)}, bf16[256,256]{1,0:T(8,128)(2,1)S(1)}, u32[]{:S(2)}, u32[]{:S(2)}) collective-permute-start(bf16[256,256]{1,0:T(8,128)(2,1)S(1)} %copy-done.16), channel_id=1, source_target_pairs={{0,24},{4,28},{8,0},{12,4},{16,8},{20,12},{24,16},{28,20},{32,56},... | collective-permute-start | bytes 393224 | tf_op jit(solution)/shard_map/ppermute | solution.py:47
  69.0 3.2 %collective-permute-done.4.q1 = bf16[256,256]{1,0:T(8,128)(2,1)S(1)} collective-permute-done((bf16[256,256]{1,0:T(8,128)(2,1)S(1)}, bf16[256,256]{1,0:T(8,128)(2,1)S(1)}, u32[]{:S(2)}, u32[]{:S(2)}) %collective-permute-start.4) | collective-permute-done | bytes 131104 | tf_op jit(solution)/shard_map/ppermute | solution.py:47
  72.3 1.9 %collective-permute-start.5 = (bf16[256,256]{1,0:T(8,128)(2,1)S(1)}, bf16[256,256]{1,0:T(8,128)(2,1)S(1)}, u32[]{:S(2)}, u32[]{:S(2)}) collective-permute-start(bf16[256,256]{1,0:T(8,128)(2,1)S(1)} %copy-done.16), channel_id=1, source_target_pairs={{0,16},{4,20},{8,24},{12,28},{16,0},{20,4},{24,8},{28,12},{32,48},... | collective-permute-start | bytes 393224 | tf_op jit(solution)/shard_map/ppermute | solution.py:47
  74.2 4.5 %collective-permute-done.5.q2 = bf16[256,256]{1,0:T(8,128)(2,1)S(1)} collective-permute-done((bf16[256,256]{1,0:T(8,128)(2,1)S(1)}, bf16[256,256]{1,0:T(8,128)(2,1)S(1)}, u32[]{:S(2)}, u32[]{:S(2)}) %collective-permute-start.5) | collective-permute-done | bytes 131104 | tf_op jit(solution)/shard_map/ppermute | solution.py:47
  80.4 7.6 %remote.1 = (bf16[528,256]{1,0:T(8,128)(2,1)}, bf16[528,256]{1,0:T(8,128)(2,1)}, bf16[528,256]{1,0:T(8,128)(2,1)}) custom-call(bf16[256,256]{1,0:T(8,128)(2,1)} %copy-done.17, bf16[256,256]{1,0:T(8,128)(2,1)} %copy-done.18, bf16[256,256]{1,0:T(8,128)(2,1)} %copy-done.19, bf16[8,512,128]{2,1,0:T(8,128)(2,1)} %copy-done, bf16[8,512,128]{2,1,0:T(8,128)(2,1)} %copy-done.2), custom_call_target="tpu_custom_call" | custom-call | tf_op jit(solution)/shard_map/remote/pallas_call | solution.py:335
  88.0 7.4 %collective-permute-done.7.a1 = bf16[384,1024]{1,0:T(8,128)(2,1)S(1)} collective-permute-done((bf16[384,1024]{1,0:T(8,128)(2,1)S(1)}, bf16[384,1024]{1,0:T(8,128)(2,1)S(1)}, u32[]{:S(2)}, u32[]{:S(2)}) %collective-permute-start.7) | collective-permute-done | bytes 786464 | tf_op jit(solution)/shard_map/ppermute | solution.py:59
  96.2 3.0 %collective-permute-start.10 = (bf16[528,256]{1,0:T(8,128)(2,1)}, bf16[528,256]{1,0:T(8,128)(2,1)S(1)}, u32[]{:S(2)}, u32[]{:S(2)}) collective-permute-start(bf16[528,256]{1,0:T(8,128)(2,1)} %get-tuple-element.27), channel_id=1, source_target_pairs={{0,24},{4,28},{8,0},{12,4},{16,8},{20,12},{24,16},{28,20},{32,56},... | collective-permute-start | bytes 811016 | tf_op jit(solution)/shard_map/ppermute | solution.py:47
  99.2 1.6 %pad_maximum_fusion.weights = bf16[2048,640]{1,0:T(8,128)(2,1)} fusion(bf16[2048,128]{1,0:T(8,128)(2,1)S(1)} %copy-done.7, bf16[2048,256]{1,0:T(8,128)(2,1)S(1)} %copy-done.3, bf16[2048,128]{1,0:T(8,128)(2,1)S(1)} %copy-done.8, bf16[2048,128]{1,0:T(8,128)(2,1)S(1)} %copy-done.9), kind=kLoop, calls=%fused_computation | loop fusion | flops 10485760 | bytes 5242880 | tf_op jit(solution)/shard_map/concatenate | solution.py:292
  100.8 3.9 %rest.1 = (bf16[256,128]{1,0:T(8,128)(2,1)}, bf16[32,128]{1,0:T(8,128)(2,1)}, bf16[256,384]{1,0:T(8,128)(2,1)}) custom-call(bf16[4,256,512]{2,1,0:T(8,128)(2,1)} %get-tuple-element.31.scaled, f32[256,128]{1,0:T(8,128)} %get-tuple-element.32.inv_in, bf16[2048,640]{1,0:T(8,128)(2,1)} %pad_maximum_fusion.weights), custom_call_target="tpu_custom_call" | custom-call | tf_op jit(solution)/shard_map/rest/pallas_call | solution.py:307
  104.7 2.0 %collective-permute-start.13 = (bf16[32,128]{1,0:T(8,128)(2,1)}, bf16[32,128]{1,0:T(8,128)(2,1)S(1)}, u32[]{:S(2)}, u32[]{:S(2)}) collective-permute-start(bf16[32,128]{1,0:T(8,128)(2,1)} %get-tuple-element.34), channel_id=1, source_target_pairs={{0,4},{4,8},{8,12},{12,16},{16,20},{20,24},{24,28},{28,32},{32,36}... | collective-permute-start | bytes 24584 | tf_op jit(solution)/shard_map/ppermute | solution.py:315
  106.7 5.2 %collective-permute-done.13.before = bf16[32,128]{1,0:T(8,128)(2,1)S(1)} collective-permute-done((bf16[32,128]{1,0:T(8,128)(2,1)}, bf16[32,128]{1,0:T(8,128)(2,1)S(1)}, u32[]{:S(2)}, u32[]{:S(2)}) %collective-permute-start.13) | collective-permute-done | bytes 8224 | tf_op jit(solution)/shard_map/ppermute | solution.py:315
  112.6 1.8 %conv.1 = (f32[256,128]{1,0:T(8,128)}, f32[1,256]{1,0:T(1,128)}) custom-call(bf16[256,128]{1,0:T(8,128)(2,1)} %get-tuple-element.33.glued, bf16[32,128]{1,0:T(8,128)(2,1)} %copy-done.23, bf16[31,128]{1,0:T(8,128)(2,1)} %weight.1), custom_call_target="tpu_custom_call" | custom-call | tf_op jit(solution)/shard_map/conv/pallas_call | solution.py:316
  115.2 4.2 %collective-permute-done.14.s1 = f32[1,256]{1,0:T(1,128)S(1)} collective-permute-done((f32[1,256]{1,0:T(1,128)}, f32[1,256]{1,0:T(1,128)S(1)}, u32[]{:S(2)}, u32[]{:S(2)}) %collective-permute-start.14) | collective-permute-done | bytes 1056 | tf_op jit(solution)/shard_map/ppermute | solution.py:59
  119.4 1.7 %collective-permute-start.15 = (f32[1,256]{1,0:T(1,128)}, f32[1,256]{1,0:T(1,128)S(1)}, u32[]{:S(2)}, u32[]{:S(2)}) collective-permute-start(f32[1,256]{1,0:T(1,128)} %get-tuple-element.36.s0), channel_id=1, source_target_pairs={{0,3},{1,0},{2,1},{3,2},{4,7},{5,4},{6,5},{7,6},{8,11},{9,8},{10,9... | collective-permute-start | bytes 3080 | tf_op jit(solution)/shard_map/ppermute | solution.py:59
  121.1 2.1 %collective-permute-done.15.s2 = f32[1,256]{1,0:T(1,128)S(1)} collective-permute-done((f32[1,256]{1,0:T(1,128)}, f32[1,256]{1,0:T(1,128)S(1)}, u32[]{:S(2)}, u32[]{:S(2)}) %collective-permute-start.15) | collective-permute-done | bytes 1056 | tf_op jit(solution)/shard_map/ppermute | solution.py:59
  124.3 4.2 %collective-permute-done.16.s3 = f32[1,256]{1,0:T(1,128)S(1)} collective-permute-done((f32[1,256]{1,0:T(1,128)}, f32[1,256]{1,0:T(1,128)S(1)}, u32[]{:S(2)}, u32[]{:S(2)}) %collective-permute-start.16) | collective-permute-done | bytes 1056 | tf_op jit(solution)/shard_map/ppermute | solution.py:59
  128.7 4.1 %self.1.m0 = bf16[528,256]{1,0:T(8,128)(2,1)} custom-call(bf16[256,256]{1,0:T(8,128)(2,1)} %get-tuple-element.30.q0, bf16[8,512,128]{2,1,0:T(8,128)(2,1)} %copy-done, bf16[8,512,128]{2,1,0:T(8,128)(2,1)} %copy-done.2), custom_call_target="tpu_custom_call" | custom-call | tf_op jit(solution)/shard_map/self/pallas_call | solution.py:347
  132.8 6.2 %collective-permute-done.11.m2 = bf16[528,256]{1,0:T(8,128)(2,1)S(1)} collective-permute-done((bf16[528,256]{1,0:T(8,128)(2,1)S(1)}, bf16[528,256]{1,0:T(8,128)(2,1)S(1)}, u32[]{:S(2)}, u32[]{:S(2)}) %collective-permute-start.11) | collective-permute-done | bytes 270368 | tf_op jit(solution)/shard_map/ppermute | solution.py:47
  139.8 2.5 %merge.1 = (bf16[64,384]{1,0:T(8,128)(2,1)}, bf16[64,384]{1,0:T(8,128)(2,1)}, bf16[64,384]{1,0:T(8,128)(2,1)}, bf16[64,384]{1,0:T(8,128)(2,1)}) custom-call(bf16[528,256]{1,0:T(8,128)(2,1)} %self.1.m0, bf16[528,256]{1,0:T(8,128)(2,1)} %copy-done.10, bf16[528,256]{1,0:T(8,128)(2,1)} %copy-done.11, bf16[528,256]{1,0:T(8,128)(2,1)} %copy-done.12, ...), custom_call_target="tpu_custom_call" | custom-call | tf_op jit(solution)/shard_map/merge/pallas_call | solution.py:357
  142.7 3.0 %collective-permute-start.18 = (bf16[64,384]{1,0:T(8,128)(2,1)}, bf16[64,384]{1,0:T(8,128)(2,1)S(1)}, u32[]{:S(2)}, u32[]{:S(2)}) collective-permute-start(bf16[64,384]{1,0:T(8,128)(2,1)} %get-tuple-element.40), channel_id=1, source_target_pairs={{0,3},{1,0},{2,1},{3,2},{4,7},{5,4},{6,5},{7,6},{8,11},{9,8},{10,9... | collective-permute-start | bytes 147464 | tf_op jit(solution)/shard_map/ppermute | solution.py:59
  145.6 2.3 %collective-permute-done.17.y1 = bf16[64,384]{1,0:T(8,128)(2,1)S(1)} collective-permute-done((bf16[64,384]{1,0:T(8,128)(2,1)}, bf16[64,384]{1,0:T(8,128)(2,1)S(1)}, u32[]{:S(2)}, u32[]{:S(2)}) %collective-permute-start.17) | collective-permute-done | bytes 49184 | tf_op jit(solution)/shard_map/ppermute | solution.py:59
  148.8 4.9 %collective-permute-done.19.y3 = bf16[64,384]{1,0:T(8,128)(2,1)S(1)} collective-permute-done((bf16[64,384]{1,0:T(8,128)(2,1)}, bf16[64,384]{1,0:T(8,128)(2,1)S(1)}, u32[]{:S(2)}, u32[]{:S(2)}) %collective-permute-start.19) | collective-permute-done | bytes 49184 | tf_op jit(solution)/shard_map/ppermute | solution.py:59
  154.9 4.8 %output.1 = bf16[64,2048]{1,0:T(8,128)(2,1)} custom-call(bf16[64,384]{1,0:T(8,128)(2,1)} %get-tuple-element.38.y0, bf16[64,384]{1,0:T(8,128)(2,1)} %copy-done.20, bf16[64,384]{1,0:T(8,128)(2,1)} %copy-done.21, bf16[64,384]{1,0:T(8,128)(2,1)} %copy-done.22, bf16[128,2048]{1,0:T(8,128)(2,1)} %w_conv.1, bf16[256,2048]{1,0:T(8,128)(2,1)} %w_attn.1, ...), custom_call_target="tpu_custom_call" | custom-call | tf_op jit(solution)/shard_map/output/pallas_call | solution.py:367
  (84 shorter events, 15.7 us)
Async XLA Ops:
  0.0 9.6 %collective-permute-start = (bf16[256,512]{1,0:T(8,128)(2,1)}, bf16[256,512]{1,0:T(8,128)(2,1)S(1)}, u32[]{:S(2)}, u32[]{:S(2)}) collective-permute-start(bf16[256,512]{1,0:T(8,128)(2,1)} %t0.1), channel_id=1, source_target_pairs={{0,1},{1,2},{2,3},{3,0},{4,5},{5,6},{6,7},{7,4},{8,9},{9,10},{10,1... | collective-permute-start | bytes 786440 | tf_op jit(solution)/shard_map/ppermute | solution.py:59
  1.5 13.0 %collective-permute-start.1 = (bf16[256,512]{1,0:T(8,128)(2,1)}, bf16[256,512]{1,0:T(8,128)(2,1)S(1)}, u32[]{:S(2)}, u32[]{:S(2)}) collective-permute-start(bf16[256,512]{1,0:T(8,128)(2,1)} %t0.1), channel_id=1, source_target_pairs={{0,3},{1,0},{2,1},{3,2},{4,7},{5,4},{6,5},{7,6},{8,11},{9,8},{10,9... | collective-permute-start | bytes 786440 | tf_op jit(solution)/shard_map/ppermute | solution.py:59
  3.2 12.8 %collective-permute-start.2 = (bf16[256,512]{1,0:T(8,128)(2,1)}, bf16[256,512]{1,0:T(8,128)(2,1)S(1)}, u32[]{:S(2)}, u32[]{:S(2)}) collective-permute-start(bf16[256,512]{1,0:T(8,128)(2,1)} %t0.1), channel_id=1, source_target_pairs={{0,2},{1,3},{2,0},{3,1},{4,6},{5,7},{6,4},{7,5},{8,10},{9,11},{10,... | collective-permute-start | bytes 786440 | tf_op jit(solution)/shard_map/ppermute | solution.py:59
  9.4 46.7 %copy-start.1 = (bf16[256,2048]{1,0:T(8,128)(2,1)S(1)}, bf16[256,2048]{1,0:T(8,128)(2,1)}, u32[]{:S(2)}) copy-start(bf16[256,2048]{1,0:T(8,128)(2,1)} %w_attn.1) | copy-start | bytes 3145732
  21.0 39.9 %copy-start.16 = (bf16[256,256]{1,0:T(8,128)(2,1)S(1)}, bf16[256,256]{1,0:T(8,128)(2,1)}, u32[]{:S(2)}) copy-start(bf16[256,256]{1,0:T(8,128)(2,1)} %get-tuple-element.30.q0) | copy-start | bytes 393220
  56.2 22.6 %copy-start = (bf16[8,512,128]{2,1,0:T(8,128)(2,1)}, bf16[8,512,128]{2,1,0:T(8,128)(2,1)S(1)}, u32[]{:S(2)}) copy-start(bf16[8,512,128]{2,1,0:T(8,128)(2,1)S(1)} %all_to_all.5.own) | copy-start | bytes 3145732
  56.2 22.6 %collective-permute-start.6 = (bf16[8,512,128]{2,1,0:T(8,128)(2,1)S(1)}, bf16[8,512,128]{2,1,0:T(8,128)(2,1)S(1)}, u32[]{:S(2)}, u32[]{:S(2)}) collective-permute-start(bf16[8,512,128]{2,1,0:T(8,128)(2,1)S(1)} %all_to_all.5.own), channel_id=1, source_target_pairs={{0,4},{4,0},{8,12},{12,8},{16,20},{20,16},{24,28},{28,24},{32,36},... | collective-permute-start | bytes 3145736 | tf_op jit(solution)/shard_map/ppermute | solution.py:47
  56.2 43.0 %copy-start.3 = (bf16[2048,256]{1,0:T(8,128)(2,1)S(1)}, bf16[2048,256]{1,0:T(8,128)(2,1)}, u32[]{:S(2)}) copy-start(bf16[2048,256]{1,0:T(8,128)(2,1)} %param.23) | copy-start | bytes 3145732
  56.2 43.0 %copy-start.7 = (bf16[2048,128]{1,0:T(8,128)(2,1)S(1)}, bf16[2048,128]{1,0:T(8,128)(2,1)}, u32[]{:S(2)}) copy-start(bf16[2048,128]{1,0:T(8,128)(2,1)} %param.22) | copy-start | bytes 1572868
  56.2 43.0 %copy-start.8 = (bf16[2048,128]{1,0:T(8,128)(2,1)S(1)}, bf16[2048,128]{1,0:T(8,128)(2,1)}, u32[]{:S(2)}) copy-start(bf16[2048,128]{1,0:T(8,128)(2,1)} %param.18) | copy-start | bytes 1572868
  56.2 43.0 %copy-start.9 = (bf16[2048,128]{1,0:T(8,128)(2,1)S(1)}, bf16[2048,128]{1,0:T(8,128)(2,1)}, u32[]{:S(2)}) copy-start(bf16[2048,128]{1,0:T(8,128)(2,1)} %param.17) | copy-start | bytes 1572868
  57.6 37.8 %collective-permute-start.7 = (bf16[384,1024]{1,0:T(8,128)(2,1)S(1)}, bf16[384,1024]{1,0:T(8,128)(2,1)S(1)}, u32[]{:S(2)}, u32[]{:S(2)}) collective-permute-start(bf16[384,1024]{1,0:T(8,128)(2,1)S(1)} %fusion), channel_id=1, source_target_pairs={{0,1},{1,2},{2,3},{3,0},{4,5},{5,6},{6,7},{7,4},{8,9},{9,10},{10,1... | collective-permute-start | bytes 2359304 | tf_op jit(solution)/shard_map/ppermute | solution.py:59
  58.6 36.9 %collective-permute-start.8 = (bf16[384,1024]{1,0:T(8,128)(2,1)S(1)}, bf16[384,1024]{1,0:T(8,128)(2,1)}, u32[]{:S(2)}, u32[]{:S(2)}) collective-permute-start(bf16[384,1024]{1,0:T(8,128)(2,1)S(1)} %fusion), channel_id=1, source_target_pairs={{0,3},{1,0},{2,1},{3,2},{4,7},{5,4},{6,5},{7,6},{8,11},{9,8},{10,9... | collective-permute-start | bytes 2359304 | tf_op jit(solution)/shard_map/ppermute | solution.py:59
  61.0 34.5 %collective-permute-start.9 = (bf16[384,1024]{1,0:T(8,128)(2,1)S(1)}, bf16[384,1024]{1,0:T(8,128)(2,1)}, u32[]{:S(2)}, u32[]{:S(2)}) collective-permute-start(bf16[384,1024]{1,0:T(8,128)(2,1)S(1)} %fusion), channel_id=1, source_target_pairs={{0,2},{1,3},{2,0},{3,1},{4,6},{5,7},{6,4},{7,5},{8,10},{9,11},{10,... | collective-permute-start | bytes 2359304 | tf_op jit(solution)/shard_map/ppermute | solution.py:59
  61.0 6.3 %collective-permute-start.3 = (bf16[256,256]{1,0:T(8,128)(2,1)S(1)}, bf16[256,256]{1,0:T(8,128)(2,1)S(1)}, u32[]{:S(2)}, u32[]{:S(2)}) collective-permute-start(bf16[256,256]{1,0:T(8,128)(2,1)S(1)} %copy-done.16), channel_id=1, source_target_pairs={{0,8},{4,12},{8,16},{12,20},{16,24},{20,28},{24,0},{28,4},{32,40},... | collective-permute-start | bytes 393224 | tf_op jit(solution)/shard_map/ppermute | solution.py:47
  67.3 5.0 %collective-permute-start.4 = (bf16[256,256]{1,0:T(8,128)(2,1)S(1)}, bf16[256,256]{1,0:T(8,128)(2,1)S(1)}, u32[]{:S(2)}, u32[]{:S(2)}) collective-permute-start(bf16[256,256]{1,0:T(8,128)(2,1)S(1)} %copy-done.16), channel_id=1, source_target_pairs={{0,24},{4,28},{8,0},{12,4},{16,8},{20,12},{24,16},{28,20},{32,56},... | collective-permute-start | bytes 393224 | tf_op jit(solution)/shard_map/ppermute | solution.py:47
  72.3 6.5 %collective-permute-start.5 = (bf16[256,256]{1,0:T(8,128)(2,1)S(1)}, bf16[256,256]{1,0:T(8,128)(2,1)S(1)}, u32[]{:S(2)}, u32[]{:S(2)}) collective-permute-start(bf16[256,256]{1,0:T(8,128)(2,1)S(1)} %copy-done.16), channel_id=1, source_target_pairs={{0,16},{4,20},{8,24},{12,28},{16,0},{20,4},{24,8},{28,12},{32,48},... | collective-permute-start | bytes 393224 | tf_op jit(solution)/shard_map/ppermute | solution.py:47
  95.5 58.3 %collective-permute-start.20 = (bf16[384,1024]{1,0:T(8,128)(2,1)S(1)}, bf16[384,1024]{1,0:T(8,128)(2,1)S(1)}, u32[]{:S(2)}, u32[]{:S(2)}) collective-permute-start(bf16[384,1024]{1,0:T(8,128)(2,1)S(1)} %collective-permute-done.7.a1), channel_id=1, source_target_pairs={{0,4},{4,0},{8,12},{12,8},{16,20},{20,16},{24,28},{28,24},{32,36},... | collective-permute-start | bytes 2359304 | tf_op jit(solution)/shard_map/ppermute | solution.py:47
  95.6 58.2 %collective-permute-start.21 = (bf16[384,1024]{1,0:T(8,128)(2,1)}, bf16[384,1024]{1,0:T(8,128)(2,1)S(1)}, u32[]{:S(2)}, u32[]{:S(2)}) collective-permute-start(bf16[384,1024]{1,0:T(8,128)(2,1)} %collective-permute-done.8.a2), channel_id=1, source_target_pairs={{0,4},{4,0},{8,12},{12,8},{16,20},{20,16},{24,28},{28,24},{32,36},... | collective-permute-start | bytes 2359304 | tf_op jit(solution)/shard_map/ppermute | solution.py:47
  96.1 57.7 %collective-permute-start.22 = (bf16[384,1024]{1,0:T(8,128)(2,1)}, bf16[384,1024]{1,0:T(8,128)(2,1)}, u32[]{:S(2)}, u32[]{:S(2)}) collective-permute-start(bf16[384,1024]{1,0:T(8,128)(2,1)} %collective-permute-done.9.a3), channel_id=1, source_target_pairs={{0,4},{4,0},{8,12},{12,8},{16,20},{20,16},{24,28},{28,24},{32,36},... | collective-permute-start | bytes 2359304 | tf_op jit(solution)/shard_map/ppermute | solution.py:47
  96.2 32.3 %collective-permute-start.10 = (bf16[528,256]{1,0:T(8,128)(2,1)}, bf16[528,256]{1,0:T(8,128)(2,1)S(1)}, u32[]{:S(2)}, u32[]{:S(2)}) collective-permute-start(bf16[528,256]{1,0:T(8,128)(2,1)} %get-tuple-element.27), channel_id=1, source_target_pairs={{0,24},{4,28},{8,0},{12,4},{16,8},{20,12},{24,16},{28,20},{32,56},... | collective-permute-start | bytes 811016 | tf_op jit(solution)/shard_map/ppermute | solution.py:47
  100.8 27.6 %copy-start.28 = (bf16[528,256]{1,0:T(8,128)(2,1)S(1)}, bf16[528,256]{1,0:T(8,128)(2,1)}, u32[]{:S(2)}) copy-start(bf16[528,256]{1,0:T(8,128)(2,1)} %get-tuple-element.28) | copy-start | bytes 811012
  100.8 27.7 %copy-start.27 = (bf16[528,256]{1,0:T(8,128)(2,1)S(1)}, bf16[528,256]{1,0:T(8,128)(2,1)}, u32[]{:S(2)}) copy-start(bf16[528,256]{1,0:T(8,128)(2,1)} %get-tuple-element.29) | copy-start | bytes 811012
  104.7 7.3 %collective-permute-start.13 = (bf16[32,128]{1,0:T(8,128)(2,1)}, bf16[32,128]{1,0:T(8,128)(2,1)S(1)}, u32[]{:S(2)}, u32[]{:S(2)}) collective-permute-start(bf16[32,128]{1,0:T(8,128)(2,1)} %get-tuple-element.34), channel_id=1, source_target_pairs={{0,4},{4,8},{8,12},{12,16},{16,20},{20,24},{24,28},{28,32},{32,36}... | collective-permute-start | bytes 24584 | tf_op jit(solution)/shard_map/ppermute | solution.py:315
  114.4 5.0 %collective-permute-start.14 = (f32[1,256]{1,0:T(1,128)}, f32[1,256]{1,0:T(1,128)S(1)}, u32[]{:S(2)}, u32[]{:S(2)}) collective-permute-start(f32[1,256]{1,0:T(1,128)} %get-tuple-element.36.s0), channel_id=1, source_target_pairs={{0,1},{1,2},{2,3},{3,0},{4,5},{5,6},{6,7},{7,4},{8,9},{9,10},{10,1... | collective-permute-start | bytes 3080 | tf_op jit(solution)/shard_map/ppermute | solution.py:59
  119.4 3.8 %collective-permute-start.15 = (f32[1,256]{1,0:T(1,128)}, f32[1,256]{1,0:T(1,128)S(1)}, u32[]{:S(2)}, u32[]{:S(2)}) collective-permute-start(f32[1,256]{1,0:T(1,128)} %get-tuple-element.36.s0), channel_id=1, source_target_pairs={{0,3},{1,0},{2,1},{3,2},{4,7},{5,4},{6,5},{7,6},{8,11},{9,8},{10,9... | collective-permute-start | bytes 3080 | tf_op jit(solution)/shard_map/ppermute | solution.py:59
  123.2 5.3 %collective-permute-start.16 = (f32[1,256]{1,0:T(1,128)}, f32[1,256]{1,0:T(1,128)S(1)}, u32[]{:S(2)}, u32[]{:S(2)}) collective-permute-start(f32[1,256]{1,0:T(1,128)} %get-tuple-element.36.s0), channel_id=1, source_target_pairs={{0,2},{1,3},{2,0},{3,1},{4,6},{5,7},{6,4},{7,5},{8,10},{9,11},{10,... | collective-permute-start | bytes 3080 | tf_op jit(solution)/shard_map/ppermute | solution.py:59
  128.5 10.6 %collective-permute-start.11 = (bf16[528,256]{1,0:T(8,128)(2,1)S(1)}, bf16[528,256]{1,0:T(8,128)(2,1)S(1)}, u32[]{:S(2)}, u32[]{:S(2)}) collective-permute-start(bf16[528,256]{1,0:T(8,128)(2,1)S(1)} %copy-done.28), channel_id=1, source_target_pairs={{0,8},{4,12},{8,16},{12,20},{16,24},{20,28},{24,0},{28,4},{32,40},... | collective-permute-start | bytes 811016 | tf_op jit(solution)/shard_map/ppermute | solution.py:47
  128.5 10.5 %collective-permute-start.12 = (bf16[528,256]{1,0:T(8,128)(2,1)S(1)}, bf16[528,256]{1,0:T(8,128)(2,1)S(1)}, u32[]{:S(2)}, u32[]{:S(2)}) collective-permute-start(bf16[528,256]{1,0:T(8,128)(2,1)S(1)} %copy-done.27), channel_id=1, source_target_pairs={{0,16},{4,20},{8,24},{12,28},{16,0},{20,4},{24,8},{28,12},{32,48},... | collective-permute-start | bytes 811016 | tf_op jit(solution)/shard_map/ppermute | solution.py:47
  142.4 5.5 %collective-permute-start.17 = (bf16[64,384]{1,0:T(8,128)(2,1)}, bf16[64,384]{1,0:T(8,128)(2,1)S(1)}, u32[]{:S(2)}, u32[]{:S(2)}) collective-permute-start(bf16[64,384]{1,0:T(8,128)(2,1)} %get-tuple-element.39), channel_id=1, source_target_pairs={{0,1},{1,2},{2,3},{3,0},{4,5},{5,6},{6,7},{7,4},{8,9},{9,10},{10,1... | collective-permute-start | bytes 147464 | tf_op jit(solution)/shard_map/ppermute | solution.py:59
  142.7 6.1 %collective-permute-start.18 = (bf16[64,384]{1,0:T(8,128)(2,1)}, bf16[64,384]{1,0:T(8,128)(2,1)S(1)}, u32[]{:S(2)}, u32[]{:S(2)}) collective-permute-start(bf16[64,384]{1,0:T(8,128)(2,1)} %get-tuple-element.40), channel_id=1, source_target_pairs={{0,3},{1,0},{2,1},{3,2},{4,7},{5,4},{6,5},{7,6},{8,11},{9,8},{10,9... | collective-permute-start | bytes 147464 | tf_op jit(solution)/shard_map/ppermute | solution.py:59
  147.9 5.8 %collective-permute-start.19 = (bf16[64,384]{1,0:T(8,128)(2,1)}, bf16[64,384]{1,0:T(8,128)(2,1)S(1)}, u32[]{:S(2)}, u32[]{:S(2)}) collective-permute-start(bf16[64,384]{1,0:T(8,128)(2,1)} %get-tuple-element.41), channel_id=1, source_target_pairs={{0,2},{1,3},{2,0},{3,1},{4,6},{5,7},{6,4},{7,5},{8,10},{9,11},{10,... | collective-permute-start | bytes 147464 | tf_op jit(solution)/shard_map/ppermute | solution.py:59
  (20 other events, 106.1 us)

commit v3 on v2

--- a/solution.py
+++ b/solution.py
@@ -28,7 +28,8 @@
 OUT = pl.BlockSpec()
 SM = pl.BlockSpec(memory_space=pltpu.SMEM)
 ANY = pl.BlockSpec(memory_space=pltpu.MemorySpace.HBM)
-BIG = pltpu.CompilerParams(vmem_limit_bytes=56 * 1024 * 1024)
+BIG = pltpu.CompilerParams(vmem_limit_bytes=16 * 1024 * 1024)
+SMALL = pltpu.CompilerParams(vmem_limit_bytes=8 * 1024 * 1024)
 SHIFTS = (1, -1, 2)
 DEPTH = 3
 LOG2E = 1.4426950408889634
@@ -290,12 +291,13 @@
     gain = in_gain.astype(F32).reshape(4, 512)
     first = jnp.concatenate([w_query, w_key, w_value], axis=1)
     second = jnp.concatenate([w_glu_value, w_glu_gate, w_gate_attn, w_gate_conv], axis=1)
+    gain, first, second, half = lax.optimization_barrier((gain, first, second, half))
     qt, kv, scaled, inv = pl.pallas_call(
         project_kernel,
-        out_shape=[sent((256, ROWS)), sent((8, 512, 128)), shape((4, ROWS, 512)), shape((ROWS, 128), F32)],
+        out_shape=[sent((256, ROWS)), sent((8, 512, 128)), sent((4, ROWS, 512)), sent((ROWS, 128), F32)],
         in_specs=[VM] * 6,
-        out_specs=[OUT] * 2 + [VM] * 2,
-        compiler_params=BIG,
+        out_specs=[OUT] * 4,
+        compiler_params=SMALL,
         name="project",
     )(*pieces, gain, first)
 
@@ -309,16 +311,17 @@
         out_shape=[shape((ROWS, 128)), sent((32, 128)), shape((ROWS, 384))],
         in_specs=[VM] * 3,
         out_specs=[VM, OUT, VM],
-        compiler_params=BIG,
+        compiler_params=SMALL,
         name="rest",
     )(scaled, inv, second)
     before = lax.ppermute(tail, "sp", [(i, i + 1) for i in range(63)])
     conv, squares = pl.pallas_call(
         conv_kernel,
-        out_shape=[shape((ROWS, 128), F32), sent((1, ROWS), F32)],
+        out_shape=[sent((ROWS, 128), F32), sent((1, ROWS), F32)],
         in_specs=[VM] * 3,
-        out_specs=[VM, OUT],
+        out_specs=[OUT] * 2,
         scratch_shapes=[pltpu.VMEM((32 + ROWS, 128), F32)],
+        compiler_params=SMALL,
         name="conv",
     )(glued, before, conv_weight)
     sums = [squares] + [tp_shift(squares, by) for by in SHIFTS]
@@ -360,7 +363,7 @@
         in_specs=[VM] * 11 + [SM, VM],
         out_specs=[VM] + [OUT] * 3,
         scratch_shapes=[pltpu.VMEM((4, 64, 384), BF16)],
-        compiler_params=BIG,
+        compiler_params=SMALL,
         name="merge",
     )(part, *back, conv, *sums, conv_gain.reshape(1, 128), gates, lam, head_gain.reshape(1, 128))
     rows = [rows[0]] + [tp_shift(r, by) for r, by in zip(rows[1:], SHIFTS)]

time: 160 us -> 147 us (0.919)
  Pallas kernels: 29 us -> 16.2 us
  waiting for transfers between devices: 55.8 us -> 62.5 us
  local copies, waits for them, and re-layouts: 6.21 us -> 2.51 us
  other arithmetic: 6.14 us -> 2.76 us
  starting transfers between devices: 27.2 us -> 28.8 us
    ppermute x12, waiting for transfers between devices: 31.8 us -> 36.5 us  [tp_shift(): return lax.ppermute(x, 'tp', [(i, (i + by) % 4) for i in range(4)])]
    unnamed x58 -> x40, local copies, waits for them, and re-layouts: 4.92 us -> 1.82 us
    concatenate x1, other arithmetic: 3.08 us -> 0.18 us  [local(): first = jnp.concatenate([w_query, w_key, w_value], axis=1)]
    pallas_call x1, Pallas kernels: 4.79 us -> 1.95 us  [local(): pl.pallas_call(output_kernel, out_shape=shape((64, D)), in_specs=[VM] * 1...]
    pallas_call x1, Pallas kernels: 3.85 us -> 1.45 us  [local(): pl.pallas_call(rest_kernel, out_shape=[shape((ROWS, 128)), sent((32, 128)...]
    pallas_call x1, Pallas kernels: 4.13 us -> 1.86 us  [local(): pl.pallas_call(self_kernel, out_shape=shape((MSG, ROWS)), in_specs=[VM] *...]
    ppermute x10, waiting for transfers between devices: 18.8 us -> 20.8 us  [along_sp(): return lax.ppermute(x, 'sp', pairs)]
    pallas_call x1, Pallas kernels: 4.26 us -> 2.27 us  [local(): pl.pallas_call(project_kernel, out_shape=[sent((256, ROWS)), sent((8, 512...]
  transfers between devices with their start and end apart: 23 -> 23, of which waited for: 14 -> 14; matrix products, arithmetic and copies ran while one was open for 5% -> 2% of each run, Pallas kernels for 13% -> 8%
where the time goes in v3:
time: 147 us
  waiting for transfers between devices  62.5 us (43%)
  blocking collectives  33.9 us (23%)
  starting transfers between devices  28.8 us (20%)
  Pallas kernels  16.2 us (11%)
  other arithmetic  2.76 us (2%)
  local copies, waits for them, and re-layouts  2.51 us (2%)
    ppermute x12, waiting for transfers between devices, tp_shift(): return lax.ppermute(x, 'tp', [(i, (i + by) % 4) for i in range(4)])  36.5 us
    all_to_all x1, blocking collectives, local(): lax.all_to_all(kv, 'sp', 0, 0, tiled=True, axis_index_groups=groups)  33.9 us
    ppermute x10, waiting for transfers between devices, along_sp(): return lax.ppermute(x, 'sp', pairs)  20.8 us
    ppermute x12, starting transfers between devices, tp_shift(): return lax.ppermute(x, 'tp', [(i, (i + by) % 4) for i in range(4)])  15.8 us
    ppermute x10, starting transfers between devices, along_sp(): return lax.ppermute(x, 'sp', pairs)  10.7 us
    pallas_call x1, Pallas kernels, local(): pl.pallas_call(remote_kernel, out_shape=[sent((MSG, ROWS))] * 3, in_specs...  5.93 us
    ppermute x1, waiting for transfers between devices, local(): before = lax.ppermute(tail, 'sp', [(i, i + 1) for i in range(63)])  5.16 us
  transfers between devices with their start and end apart: 23, of which 14 were waited for; matrix products, arithmetic and copies ran while one was open for 2% of the time, Pallas kernels for 8%

profile of v3, /device:TPU:32, one launch (start us, length us, event | category | flops | bytes accessed | tf_op | source)
XLA Modules:
  0.0 146.8 jit_solution(221880784284575110)
XLA Ops:
  0.0 2.8 %collective-permute-start.1 = (bf16[256,512]{1,0:T(8,128)(2,1)}, bf16[256,512]{1,0:T(8,128)(2,1)S(1)}, u32[]{:S(2)}, u32[]{:S(2)}) collective-permute-start(bf16[256,512]{1,0:T(8,128)(2,1)} %t0.1), channel_id=1, source_target_pairs={{0,3},{1,0},{2,1},{3,2},{4,7},{5,4},{6,5},{7,6},{8,11},{9,8},{10,9... | collective-permute-start | bytes 786440 | tf_op jit(solution)/shard_map/ppermute | solution.py:60
  2.8 2.3 %collective-permute-start.2 = (bf16[256,512]{1,0:T(8,128)(2,1)}, bf16[256,512]{1,0:T(8,128)(2,1)S(1)}, u32[]{:S(2)}, u32[]{:S(2)}) collective-permute-start(bf16[256,512]{1,0:T(8,128)(2,1)} %t0.1), channel_id=1, source_target_pairs={{0,2},{1,3},{2,0},{3,1},{4,6},{5,7},{6,4},{7,5},{8,10},{9,11},{10,... | collective-permute-start | bytes 786440 | tf_op jit(solution)/shard_map/ppermute | solution.py:60
  7.1 1.4 pad_maximum_fusion.weights
  8.9 5.5 %collective-permute-done.1.t2 = bf16[256,512]{1,0:T(8,128)(2,1)S(1)} collective-permute-done((bf16[256,512]{1,0:T(8,128)(2,1)}, bf16[256,512]{1,0:T(8,128)(2,1)S(1)}, u32[]{:S(2)}, u32[]{:S(2)}) %collective-permute-start.1) | collective-permute-done | bytes 262176 | tf_op jit(solution)/shard_map/ppermute | solution.py:60
  14.4 3.3 %collective-permute-done.t1 = bf16[256,512]{1,0:T(8,128)(2,1)S(1)} collective-permute-done((bf16[256,512]{1,0:T(8,128)(2,1)}, bf16[256,512]{1,0:T(8,128)(2,1)S(1)}, u32[]{:S(2)}, u32[]{:S(2)}) %collective-permute-start) | collective-permute-done | bytes 262176 | tf_op jit(solution)/shard_map/ppermute | solution.py:60
  17.7 2.3 %project.1 = (bf16[256,256]{1,0:T(8,128)(2,1)}, bf16[8,512,128]{2,1,0:T(8,128)(2,1)}, bf16[4,256,512]{2,1,0:T(8,128)(2,1)}, f32[256,128]{1,0:T(8,128)}) custom-call(bf16[256,512]{1,0:T(8,128)(2,1)S(1)} %copy-done.3, bf16[256,512]{1,0:T(8,128)(2,1)S(1)} %collective-permute-done.t1, bf16[256,512]{1,0:T(8,128)(2,1)S(1)} %collective-permute-done.1.t2, ...), custom_call_target="tpu_custom_call" | custom-call | tf_op jit(solution)/shard_map/project/pallas_call | solution.py:295
  19.9 33.9 %all_to_all.5.own = bf16[8,512,128]{2,1,0:T(8,128)(2,1)S(1)} all-to-all(bf16[8,512,128]{2,1,0:T(8,128)(2,1)} %get-tuple-element.32), channel_id=1, replica_groups={{0,32,64,96,128,160,192,224},{4,36,68,100,132,164,196,228},{8,40,72,104..., dimensions={0} | all-to-all | bytes 2097152 | tf_op jit(solution)/shard_map/all_to_all | solution.py:305
  53.9 1.8 %collective-permute-start.9 = (bf16[384,1024]{1,0:T(8,128)(2,1)S(1)}, bf16[384,1024]{1,0:T(8,128)(2,1)S(1)}, u32[]{:S(2)}, u32[]{:S(2)}) collective-permute-start(bf16[384,1024]{1,0:T(8,128)(2,1)S(1)} %fusion), channel_id=1, source_target_pairs={{0,2},{1,3},{2,0},{3,1},{4,6},{5,7},{6,4},{7,5},{8,10},{9,11},{10,... | collective-permute-start | bytes 2359304 | tf_op jit(solution)/shard_map/ppermute | solution.py:60
  56.5 1.2 collective-permute-start.7
  57.7 3.2 %collective-permute-start.5 = (bf16[256,256]{1,0:T(8,128)(2,1)}, bf16[256,256]{1,0:T(8,128)(2,1)S(1)}, u32[]{:S(2)}, u32[]{:S(2)}) collective-permute-start(bf16[256,256]{1,0:T(8,128)(2,1)} %get-tuple-element.37.q0), channel_id=1, source_target_pairs={{0,16},{4,20},{8,24},{12,28},{16,0},{20,4},{24,8},{28,12},{32,48},... | collective-permute-start | bytes 393224 | tf_op jit(solution)/shard_map/ppermute | solution.py:48
  60.9 3.6 %collective-permute-done.5.q2 = bf16[256,256]{1,0:T(8,128)(2,1)S(1)} collective-permute-done((bf16[256,256]{1,0:T(8,128)(2,1)}, bf16[256,256]{1,0:T(8,128)(2,1)S(1)}, u32[]{:S(2)}, u32[]{:S(2)}) %collective-permute-start.5) | collective-permute-done | bytes 131104 | tf_op jit(solution)/shard_map/ppermute | solution.py:48
  64.5 3.0 %collective-permute-start.4 = (bf16[256,256]{1,0:T(8,128)(2,1)}, bf16[256,256]{1,0:T(8,128)(2,1)S(1)}, u32[]{:S(2)}, u32[]{:S(2)}) collective-permute-start(bf16[256,256]{1,0:T(8,128)(2,1)} %get-tuple-element.37.q0), channel_id=1, source_target_pairs={{0,24},{4,28},{8,0},{12,4},{16,8},{20,12},{24,16},{28,20},{32,56},... | collective-permute-start | bytes 393224 | tf_op jit(solution)/shard_map/ppermute | solution.py:48
  67.5 2.8 %collective-permute-done.4.q1 = bf16[256,256]{1,0:T(8,128)(2,1)S(1)} collective-permute-done((bf16[256,256]{1,0:T(8,128)(2,1)}, bf16[256,256]{1,0:T(8,128)(2,1)S(1)}, u32[]{:S(2)}, u32[]{:S(2)}) %collective-permute-start.4) | collective-permute-done | bytes 131104 | tf_op jit(solution)/shard_map/ppermute | solution.py:48
  71.2 5.8 %collective-permute-done.3.q0 = bf16[256,256]{1,0:T(8,128)(2,1)S(1)} collective-permute-done((bf16[256,256]{1,0:T(8,128)(2,1)}, bf16[256,256]{1,0:T(8,128)(2,1)S(1)}, u32[]{:S(2)}, u32[]{:S(2)}) %collective-permute-start.3) | collective-permute-done | bytes 131104 | tf_op jit(solution)/shard_map/ppermute | solution.py:48
  77.0 5.9 %remote.1 = (bf16[528,256]{1,0:T(8,128)(2,1)}, bf16[528,256]{1,0:T(8,128)(2,1)}, bf16[528,256]{1,0:T(8,128)(2,1)}) custom-call(bf16[256,256]{1,0:T(8,128)(2,1)S(1)} %collective-permute-done.3.q0, bf16[256,256]{1,0:T(8,128)(2,1)S(1)} %collective-permute-done.4.q1, bf16[256,256]{1,0:T(8,128)(2,1)S(1)} %collective-permute-done.5.q2, ...), custom_call_target="tpu_custom_call" | custom-call | tf_op jit(solution)/shard_map/remote/pallas_call | solution.py:338
  83.0 8.0 %collective-permute-done.8.a2 = bf16[384,1024]{1,0:T(8,128)(2,1)S(1)} collective-permute-done((bf16[384,1024]{1,0:T(8,128)(2,1)S(1)}, bf16[384,1024]{1,0:T(8,128)(2,1)S(1)}, u32[]{:S(2)}, u32[]{:S(2)}) %collective-permute-start.8) | collective-permute-done | bytes 786464 | tf_op jit(solution)/shard_map/ppermute | solution.py:60
  92.7 3.0 %collective-permute-start.10 = (bf16[528,256]{1,0:T(8,128)(2,1)}, bf16[528,256]{1,0:T(8,128)(2,1)S(1)}, u32[]{:S(2)}, u32[]{:S(2)}) collective-permute-start(bf16[528,256]{1,0:T(8,128)(2,1)} %get-tuple-element.33), channel_id=1, source_target_pairs={{0,24},{4,28},{8,0},{12,4},{16,8},{20,12},{24,16},{28,20},{32,56},... | collective-permute-start | bytes 811016 | tf_op jit(solution)/shard_map/ppermute | solution.py:48
  95.7 1.5 rest.1
  97.2 2.2 %collective-permute-start.13 = (bf16[32,128]{1,0:T(8,128)(2,1)}, bf16[32,128]{1,0:T(8,128)(2,1)S(1)}, u32[]{:S(2)}, u32[]{:S(2)}) collective-permute-start(bf16[32,128]{1,0:T(8,128)(2,1)} %get-tuple-element.42), channel_id=1, source_target_pairs={{0,4},{4,8},{8,12},{12,16},{16,20},{20,24},{24,28},{28,32},{32,36}... | collective-permute-start | bytes 24584 | tf_op jit(solution)/shard_map/ppermute | solution.py:317
  99.5 5.2 %collective-permute-done.13.before = bf16[32,128]{1,0:T(8,128)(2,1)S(1)} collective-permute-done((bf16[32,128]{1,0:T(8,128)(2,1)}, bf16[32,128]{1,0:T(8,128)(2,1)S(1)}, u32[]{:S(2)}, u32[]{:S(2)}) %collective-permute-start.13) | collective-permute-done | bytes 8224 | tf_op jit(solution)/shard_map/ppermute | solution.py:317
  105.6 1.8 %collective-permute-start.16 = (f32[1,256]{1,0:T(1,128)}, f32[1,256]{1,0:T(1,128)S(1)}, u32[]{:S(2)}, u32[]{:S(2)}) collective-permute-start(f32[1,256]{1,0:T(1,128)} %get-tuple-element.44.s0), channel_id=1, source_target_pairs={{0,2},{1,3},{2,0},{3,1},{4,6},{5,7},{6,4},{7,5},{8,10},{9,11},{10,... | collective-permute-start | bytes 3080 | tf_op jit(solution)/shard_map/ppermute | solution.py:60
  107.4 3.5 %collective-permute-done.16.s3 = f32[1,256]{1,0:T(1,128)S(1)} collective-permute-done((f32[1,256]{1,0:T(1,128)}, f32[1,256]{1,0:T(1,128)S(1)}, u32[]{:S(2)}, u32[]{:S(2)}) %collective-permute-start.16) | collective-permute-done | bytes 1056 | tf_op jit(solution)/shard_map/ppermute | solution.py:60
  110.9 1.5 %collective-permute-start.15 = (f32[1,256]{1,0:T(1,128)}, f32[1,256]{1,0:T(1,128)S(1)}, u32[]{:S(2)}, u32[]{:S(2)}) collective-permute-start(f32[1,256]{1,0:T(1,128)} %get-tuple-element.44.s0), channel_id=1, source_target_pairs={{0,3},{1,0},{2,1},{3,2},{4,7},{5,4},{6,5},{7,6},{8,11},{9,8},{10,9... | collective-permute-start | bytes 3080 | tf_op jit(solution)/shard_map/ppermute | solution.py:60
  112.4 2.3 %collective-permute-done.15.s2 = f32[1,256]{1,0:T(1,128)S(1)} collective-permute-done((f32[1,256]{1,0:T(1,128)}, f32[1,256]{1,0:T(1,128)S(1)}, u32[]{:S(2)}, u32[]{:S(2)}) %collective-permute-start.15) | collective-permute-done | bytes 1056 | tf_op jit(solution)/shard_map/ppermute | solution.py:60
  115.0 4.7 %collective-permute-done.14.s1 = f32[1,256]{1,0:T(1,128)S(1)} collective-permute-done((f32[1,256]{1,0:T(1,128)}, f32[1,256]{1,0:T(1,128)S(1)}, u32[]{:S(2)}, u32[]{:S(2)}) %collective-permute-start.14) | collective-permute-done | bytes 1056 | tf_op jit(solution)/shard_map/ppermute | solution.py:60
  119.8 1.9 %self.1.m0 = bf16[528,256]{1,0:T(8,128)(2,1)S(1)} custom-call(bf16[256,256]{1,0:T(8,128)(2,1)S(1)} %copy-done.4, bf16[8,512,128]{2,1,0:T(8,128)(2,1)S(1)} %all_to_all.5.own, bf16[8,512,128]{2,1,0:T(8,128)(2,1)S(1)} %collective-permute-done.6.other), custom_call_target="tpu_custom_call" | custom-call | tf_op jit(solution)/shard_map/self/pallas_call | solution.py:350
  121.7 8.6 %collective-permute-done.11.m2 = bf16[528,256]{1,0:T(8,128)(2,1)S(1)} collective-permute-done((bf16[528,256]{1,0:T(8,128)(2,1)S(1)}, bf16[528,256]{1,0:T(8,128)(2,1)S(1)}, u32[]{:S(2)}, u32[]{:S(2)}) %collective-permute-start.11) | collective-permute-done | bytes 270368 | tf_op jit(solution)/shard_map/ppermute | solution.py:48
  131.8 1.7 %merge.1 = (bf16[64,384]{1,0:T(8,128)(2,1)S(1)}, bf16[64,384]{1,0:T(8,128)(2,1)}, bf16[64,384]{1,0:T(8,128)(2,1)}, bf16[64,384]{1,0:T(8,128)(2,1)}) custom-call(bf16[528,256]{1,0:T(8,128)(2,1)S(1)} %self.1.m0, bf16[528,256]{1,0:T(8,128)(2,1)S(1)} %collective-permute-done.10.m1, bf16[528,256]{1,0:T(8,128)(2,1)S(1)} %collective-permute-done.11.m2, ...), custom_call_target="tpu_custom_call" | custom-call | tf_op jit(solution)/shard_map/merge/pallas_call | solution.py:360
  133.5 3.2 %collective-permute-start.18 = (bf16[64,384]{1,0:T(8,128)(2,1)}, bf16[64,384]{1,0:T(8,128)(2,1)S(1)}, u32[]{:S(2)}, u32[]{:S(2)}) collective-permute-start(bf16[64,384]{1,0:T(8,128)(2,1)} %get-tuple-element.48), channel_id=1, source_target_pairs={{0,3},{1,0},{2,1},{3,2},{4,7},{5,4},{6,5},{7,6},{8,11},{9,8},{10,9... | collective-permute-start | bytes 147464 | tf_op jit(solution)/shard_map/ppermute | solution.py:60
  136.8 2.3 %collective-permute-done.17.y1 = bf16[64,384]{1,0:T(8,128)(2,1)S(1)} collective-permute-done((bf16[64,384]{1,0:T(8,128)(2,1)}, bf16[64,384]{1,0:T(8,128)(2,1)S(1)}, u32[]{:S(2)}, u32[]{:S(2)}) %collective-permute-start.17) | collective-permute-done | bytes 49184 | tf_op jit(solution)/shard_map/ppermute | solution.py:60
  139.0 5.8 %collective-permute-done.19.y3 = bf16[64,384]{1,0:T(8,128)(2,1)S(1)} collective-permute-done((bf16[64,384]{1,0:T(8,128)(2,1)}, bf16[64,384]{1,0:T(8,128)(2,1)S(1)}, u32[]{:S(2)}, u32[]{:S(2)}) %collective-permute-start.19) | collective-permute-done | bytes 49184 | tf_op jit(solution)/shard_map/ppermute | solution.py:60
  144.9 2.0 %output.1 = bf16[64,2048]{1,0:T(8,128)(2,1)} custom-call(bf16[64,384]{1,0:T(8,128)(2,1)S(1)} %get-tuple-element.46.y0, bf16[64,384]{1,0:T(8,128)(2,1)S(1)} %collective-permute-done.17.y1, bf16[64,384]{1,0:T(8,128)(2,1)S(1)} %collective-permute-done.18.y2, bf16[64,384]{1,0:T(8,128)(2,1)S(1)} %collective-permute-done.19.y3, bf16[128,2048]{1,0:T(8,128)(2,1)S(1)} %copy-done.1, ...), custom_call_target="tpu_custom_call" | custom-call | tf_op jit(solution)/shard_map/output/pallas_call | solution.py:370
  (66 shorter events, 8.7 us)
Async XLA Ops:
  0.0 14.4 %collective-permute-start.1 = (bf16[256,512]{1,0:T(8,128)(2,1)}, bf16[256,512]{1,0:T(8,128)(2,1)S(1)}, u32[]{:S(2)}, u32[]{:S(2)}) collective-permute-start(bf16[256,512]{1,0:T(8,128)(2,1)} %t0.1), channel_id=1, source_target_pairs={{0,3},{1,0},{2,1},{3,2},{4,7},{5,4},{6,5},{7,6},{8,11},{9,8},{10,9... | collective-permute-start | bytes 786440 | tf_op jit(solution)/shard_map/ppermute | solution.py:60
  2.8 14.8 %collective-permute-start = (bf16[256,512]{1,0:T(8,128)(2,1)}, bf16[256,512]{1,0:T(8,128)(2,1)S(1)}, u32[]{:S(2)}, u32[]{:S(2)}) collective-permute-start(bf16[256,512]{1,0:T(8,128)(2,1)} %t0.1), channel_id=1, source_target_pairs={{0,1},{1,2},{2,3},{3,0},{4,5},{5,6},{6,7},{7,4},{8,9},{9,10},{10,1... | collective-permute-start | bytes 786440 | tf_op jit(solution)/shard_map/ppermute | solution.py:60
  2.8 14.8 %collective-permute-start.2 = (bf16[256,512]{1,0:T(8,128)(2,1)}, bf16[256,512]{1,0:T(8,128)(2,1)S(1)}, u32[]{:S(2)}, u32[]{:S(2)}) collective-permute-start(bf16[256,512]{1,0:T(8,128)(2,1)} %t0.1), channel_id=1, source_target_pairs={{0,2},{1,3},{2,0},{3,1},{4,6},{5,7},{6,4},{7,5},{8,10},{9,11},{10,... | collective-permute-start | bytes 786440 | tf_op jit(solution)/shard_map/ppermute | solution.py:60
  19.9 75.8 %copy-start.2 = (bf16[4,256,512]{2,1,0:T(8,128)(2,1)S(1)}, bf16[4,256,512]{2,1,0:T(8,128)(2,1)}, u32[]{:S(2)}) copy-start(bf16[4,256,512]{2,1,0:T(8,128)(2,1)} %get-tuple-element.38.scaled) | copy-start | bytes 3145732
  19.9 75.8 %copy-start.6 = (f32[256,128]{1,0:T(8,128)S(1)}, f32[256,128]{1,0:T(8,128)}, u32[]{:S(2)}) copy-start(f32[256,128]{1,0:T(8,128)} %get-tuple-element.39.inv_in) | copy-start | bytes 393220
  53.9 23.2 %collective-permute-start.6 = (bf16[8,512,128]{2,1,0:T(8,128)(2,1)S(1)}, bf16[8,512,128]{2,1,0:T(8,128)(2,1)S(1)}, u32[]{:S(2)}, u32[]{:S(2)}) collective-permute-start(bf16[8,512,128]{2,1,0:T(8,128)(2,1)S(1)} %all_to_all.5.own), channel_id=1, source_target_pairs={{0,4},{4,0},{8,12},{12,8},{16,20},{20,16},{24,28},{28,24},{32,36},... | collective-permute-start | bytes 3145736 | tf_op jit(solution)/shard_map/ppermute | solution.py:48
  53.9 29.1 %collective-permute-start.9 = (bf16[384,1024]{1,0:T(8,128)(2,1)S(1)}, bf16[384,1024]{1,0:T(8,128)(2,1)S(1)}, u32[]{:S(2)}, u32[]{:S(2)}) collective-permute-start(bf16[384,1024]{1,0:T(8,128)(2,1)S(1)} %fusion), channel_id=1, source_target_pairs={{0,2},{1,3},{2,0},{3,1},{4,6},{5,7},{6,4},{7,5},{8,10},{9,11},{10,... | collective-permute-start | bytes 2359304 | tf_op jit(solution)/shard_map/ppermute | solution.py:60
  55.7 35.4 %collective-permute-start.8 = (bf16[384,1024]{1,0:T(8,128)(2,1)S(1)}, bf16[384,1024]{1,0:T(8,128)(2,1)S(1)}, u32[]{:S(2)}, u32[]{:S(2)}) collective-permute-start(bf16[384,1024]{1,0:T(8,128)(2,1)S(1)} %fusion), channel_id=1, source_target_pairs={{0,3},{1,0},{2,1},{3,2},{4,7},{5,4},{6,5},{7,6},{8,11},{9,8},{10,9... | collective-permute-start | bytes 2359304 | tf_op jit(solution)/shard_map/ppermute | solution.py:60
  56.5 35.7 %collective-permute-start.7 = (bf16[384,1024]{1,0:T(8,128)(2,1)S(1)}, bf16[384,1024]{1,0:T(8,128)(2,1)S(1)}, u32[]{:S(2)}, u32[]{:S(2)}) collective-permute-start(bf16[384,1024]{1,0:T(8,128)(2,1)S(1)} %fusion), channel_id=1, source_target_pairs={{0,1},{1,2},{2,3},{3,0},{4,5},{5,6},{6,7},{7,4},{8,9},{9,10},{10,1... | collective-permute-start | bytes 2359304 | tf_op jit(solution)/shard_map/ppermute | solution.py:60
  57.7 46.9 %copy-start.7 = (bf16[31,128]{1,0:T(8,128)(2,1)S(1)}, bf16[31,128]{1,0:T(8,128)(2,1)}, u32[]{:S(2)}) copy-start(bf16[31,128]{1,0:T(8,128)(2,1)} %weight.1) | copy-start | bytes 23812
  57.7 62.1 %copy-start.4 = (bf16[256,256]{1,0:T(8,128)(2,1)S(1)}, bf16[256,256]{1,0:T(8,128)(2,1)}, u32[]{:S(2)}) copy-start(bf16[256,256]{1,0:T(8,128)(2,1)} %get-tuple-element.37.q0) | copy-start | bytes 393220
  57.7 6.8 %collective-permute-start.5 = (bf16[256,256]{1,0:T(8,128)(2,1)}, bf16[256,256]{1,0:T(8,128)(2,1)S(1)}, u32[]{:S(2)}, u32[]{:S(2)}) collective-permute-start(bf16[256,256]{1,0:T(8,128)(2,1)} %get-tuple-element.37.q0), channel_id=1, source_target_pairs={{0,16},{4,20},{8,24},{12,28},{16,0},{20,4},{24,8},{28,12},{32,48},... | collective-permute-start | bytes 393224 | tf_op jit(solution)/shard_map/ppermute | solution.py:48
  64.5 5.8 %collective-permute-start.4 = (bf16[256,256]{1,0:T(8,128)(2,1)}, bf16[256,256]{1,0:T(8,128)(2,1)S(1)}, u32[]{:S(2)}, u32[]{:S(2)}) collective-permute-start(bf16[256,256]{1,0:T(8,128)(2,1)} %get-tuple-element.37.q0), channel_id=1, source_target_pairs={{0,24},{4,28},{8,0},{12,4},{16,8},{20,12},{24,16},{28,20},{32,56},... | collective-permute-start | bytes 393224 | tf_op jit(solution)/shard_map/ppermute | solution.py:48
  70.3 6.7 %collective-permute-start.3 = (bf16[256,256]{1,0:T(8,128)(2,1)}, bf16[256,256]{1,0:T(8,128)(2,1)S(1)}, u32[]{:S(2)}, u32[]{:S(2)}) collective-permute-start(bf16[256,256]{1,0:T(8,128)(2,1)} %get-tuple-element.37.q0), channel_id=1, source_target_pairs={{0,8},{4,12},{8,16},{12,20},{16,24},{20,28},{24,0},{28,4},{32,40},... | collective-permute-start | bytes 393224 | tf_op jit(solution)/shard_map/ppermute | solution.py:48
  83.0 36.7 %copy-start.19 = (bf16[528,256]{1,0:T(8,128)(2,1)S(1)}, bf16[528,256]{1,0:T(8,128)(2,1)}, u32[]{:S(2)}) copy-start(bf16[528,256]{1,0:T(8,128)(2,1)} %get-tuple-element.34) | copy-start | bytes 811012
  83.0 36.7 %copy-start.18 = (bf16[528,256]{1,0:T(8,128)(2,1)S(1)}, bf16[528,256]{1,0:T(8,128)(2,1)}, u32[]{:S(2)}) copy-start(bf16[528,256]{1,0:T(8,128)(2,1)} %get-tuple-element.35) | copy-start | bytes 811012
  92.2 52.7 %collective-permute-start.20 = (bf16[384,1024]{1,0:T(8,128)(2,1)S(1)}, bf16[384,1024]{1,0:T(8,128)(2,1)S(1)}, u32[]{:S(2)}, u32[]{:S(2)}) collective-permute-start(bf16[384,1024]{1,0:T(8,128)(2,1)S(1)} %collective-permute-done.7.a1), channel_id=1, source_target_pairs={{0,4},{4,0},{8,12},{12,8},{16,20},{20,16},{24,28},{28,24},{32,36},... | collective-permute-start | bytes 2359304 | tf_op jit(solution)/shard_map/ppermute | solution.py:48
  92.2 52.7 %collective-permute-start.21 = (bf16[384,1024]{1,0:T(8,128)(2,1)S(1)}, bf16[384,1024]{1,0:T(8,128)(2,1)S(1)}, u32[]{:S(2)}, u32[]{:S(2)}) collective-permute-start(bf16[384,1024]{1,0:T(8,128)(2,1)S(1)} %collective-permute-done.8.a2), channel_id=1, source_target_pairs={{0,4},{4,0},{8,12},{12,8},{16,20},{20,16},{24,28},{28,24},{32,36},... | collective-permute-start | bytes 2359304 | tf_op jit(solution)/shard_map/ppermute | solution.py:48
  92.7 52.2 %collective-permute-start.22 = (bf16[384,1024]{1,0:T(8,128)(2,1)S(1)}, bf16[384,1024]{1,0:T(8,128)(2,1)S(1)}, u32[]{:S(2)}, u32[]{:S(2)}) collective-permute-start(bf16[384,1024]{1,0:T(8,128)(2,1)S(1)} %collective-permute-done.9.a3), channel_id=1, source_target_pairs={{0,4},{4,0},{8,12},{12,8},{16,20},{20,16},{24,28},{28,24},{32,36},... | collective-permute-start | bytes 2359304 | tf_op jit(solution)/shard_map/ppermute | solution.py:48
  92.7 27.0 %collective-permute-start.10 = (bf16[528,256]{1,0:T(8,128)(2,1)}, bf16[528,256]{1,0:T(8,128)(2,1)S(1)}, u32[]{:S(2)}, u32[]{:S(2)}) collective-permute-start(bf16[528,256]{1,0:T(8,128)(2,1)} %get-tuple-element.33), channel_id=1, source_target_pairs={{0,24},{4,28},{8,0},{12,4},{16,8},{20,12},{24,16},{28,20},{32,56},... | collective-permute-start | bytes 811016 | tf_op jit(solution)/shard_map/ppermute | solution.py:48
  95.7 34.5 %copy-start.10 = (f32[2]{0:T(128)S(1)}, f32[2]{0:T(128)}, u32[]{:S(2)}) copy-start(f32[2]{0:T(128)} %lam.1) | copy-start | bytes 28
  97.2 47.7 %copy-start = (bf16[256,2048]{1,0:T(8,128)(2,1)S(1)}, bf16[256,2048]{1,0:T(8,128)(2,1)}, u32[]{:S(2)}) copy-start(bf16[256,2048]{1,0:T(8,128)(2,1)} %w_attn.1) | copy-start | bytes 3145732
  97.2 47.7 %copy-start.1 = (bf16[128,2048]{1,0:T(8,128)(2,1)S(1)}, bf16[128,2048]{1,0:T(8,128)(2,1)}, u32[]{:S(2)}) copy-start(bf16[128,2048]{1,0:T(8,128)(2,1)} %w_conv.1) | copy-start | bytes 1572868
  97.2 7.4 %collective-permute-start.13 = (bf16[32,128]{1,0:T(8,128)(2,1)}, bf16[32,128]{1,0:T(8,128)(2,1)S(1)}, u32[]{:S(2)}, u32[]{:S(2)}) collective-permute-start(bf16[32,128]{1,0:T(8,128)(2,1)} %get-tuple-element.42), channel_id=1, source_target_pairs={{0,4},{4,8},{8,12},{12,16},{16,20},{20,24},{24,28},{28,32},{32,36}... | collective-permute-start | bytes 24584 | tf_op jit(solution)/shard_map/ppermute | solution.py:317
  105.6 5.3 %collective-permute-start.16 = (f32[1,256]{1,0:T(1,128)}, f32[1,256]{1,0:T(1,128)S(1)}, u32[]{:S(2)}, u32[]{:S(2)}) collective-permute-start(f32[1,256]{1,0:T(1,128)} %get-tuple-element.44.s0), channel_id=1, source_target_pairs={{0,2},{1,3},{2,0},{3,1},{4,6},{5,7},{6,4},{7,5},{8,10},{9,11},{10,... | collective-permute-start | bytes 3080 | tf_op jit(solution)/shard_map/ppermute | solution.py:60
  110.9 3.8 %collective-permute-start.15 = (f32[1,256]{1,0:T(1,128)}, f32[1,256]{1,0:T(1,128)S(1)}, u32[]{:S(2)}, u32[]{:S(2)}) collective-permute-start(f32[1,256]{1,0:T(1,128)} %get-tuple-element.44.s0), channel_id=1, source_target_pairs={{0,3},{1,0},{2,1},{3,2},{4,7},{5,4},{6,5},{7,6},{8,11},{9,8},{10,9... | collective-permute-start | bytes 3080 | tf_op jit(solution)/shard_map/ppermute | solution.py:60
  114.7 5.0 %collective-permute-start.14 = (f32[1,256]{1,0:T(1,128)}, f32[1,256]{1,0:T(1,128)S(1)}, u32[]{:S(2)}, u32[]{:S(2)}) collective-permute-start(f32[1,256]{1,0:T(1,128)} %get-tuple-element.44.s0), channel_id=1, source_target_pairs={{0,1},{1,2},{2,3},{3,0},{4,5},{5,6},{6,7},{7,4},{8,9},{9,10},{10,1... | collective-permute-start | bytes 3080 | tf_op jit(solution)/shard_map/ppermute | solution.py:60
  119.7 10.6 %collective-permute-start.11 = (bf16[528,256]{1,0:T(8,128)(2,1)S(1)}, bf16[528,256]{1,0:T(8,128)(2,1)S(1)}, u32[]{:S(2)}, u32[]{:S(2)}) collective-permute-start(bf16[528,256]{1,0:T(8,128)(2,1)S(1)} %copy-done.19), channel_id=1, source_target_pairs={{0,8},{4,12},{8,16},{12,20},{16,24},{20,28},{24,0},{28,4},{32,40},... | collective-permute-start | bytes 811016 | tf_op jit(solution)/shard_map/ppermute | solution.py:48
  119.7 10.6 %collective-permute-start.12 = (bf16[528,256]{1,0:T(8,128)(2,1)S(1)}, bf16[528,256]{1,0:T(8,128)(2,1)S(1)}, u32[]{:S(2)}, u32[]{:S(2)}) collective-permute-start(bf16[528,256]{1,0:T(8,128)(2,1)S(1)} %copy-done.18), channel_id=1, source_target_pairs={{0,16},{4,20},{8,24},{12,28},{16,0},{20,4},{24,8},{28,12},{32,48},... | collective-permute-start | bytes 811016 | tf_op jit(solution)/shard_map/ppermute | solution.py:48
  133.5 5.5 %collective-permute-start.17 = (bf16[64,384]{1,0:T(8,128)(2,1)}, bf16[64,384]{1,0:T(8,128)(2,1)S(1)}, u32[]{:S(2)}, u32[]{:S(2)}) collective-permute-start(bf16[64,384]{1,0:T(8,128)(2,1)} %get-tuple-element.47), channel_id=1, source_target_pairs={{0,1},{1,2},{2,3},{3,0},{4,5},{5,6},{6,7},{7,4},{8,9},{9,10},{10,1... | collective-permute-start | bytes 147464 | tf_op jit(solution)/shard_map/ppermute | solution.py:60
  133.5 5.5 %collective-permute-start.18 = (bf16[64,384]{1,0:T(8,128)(2,1)}, bf16[64,384]{1,0:T(8,128)(2,1)S(1)}, u32[]{:S(2)}, u32[]{:S(2)}) collective-permute-start(bf16[64,384]{1,0:T(8,128)(2,1)} %get-tuple-element.48), channel_id=1, source_target_pairs={{0,3},{1,0},{2,1},{3,2},{4,7},{5,4},{6,5},{7,6},{8,11},{9,8},{10,9... | collective-permute-start | bytes 147464 | tf_op jit(solution)/shard_map/ppermute | solution.py:60
  139.0 5.8 %collective-permute-start.19 = (bf16[64,384]{1,0:T(8,128)(2,1)}, bf16[64,384]{1,0:T(8,128)(2,1)S(1)}, u32[]{:S(2)}, u32[]{:S(2)}) collective-permute-start(bf16[64,384]{1,0:T(8,128)(2,1)} %get-tuple-element.49), channel_id=1, source_target_pairs={{0,2},{1,3},{2,0},{3,1},{4,6},{5,7},{6,4},{7,5},{8,10},{9,11},{10,... | collective-permute-start | bytes 147464 | tf_op jit(solution)/shard_map/ppermute | solution.py:60
  (11 other events, 105.2 us)

commit v4 on v3

--- a/solution.py
+++ b/solution.py
@@ -99,7 +99,7 @@
     gates[:, 0:128] = (dot(rows, weights[:, 512:640]) * inv).astype(BF16)
 
 
-def conv_kernel(glued, before, weight, conv, squares, padded):
+def conv_kernel(glued, before, weight, conv, squares, kept, padded):
     padded[0:32, :] = before[...].astype(F32)
     padded[32 : 32 + ROWS, :] = glued[...].astype(F32)
     taps = weight[...].astype(F32)
@@ -107,7 +107,9 @@
     for j in range(WIDTH):
         total += padded[j + 2 : j + 2 + ROWS, :] * taps[j : j + 1, :]
     conv[...] = total
-    squares[...] = jnp.sum(jnp.transpose(total * total), axis=0, keepdims=True)
+    sums = jnp.sum(jnp.transpose(total * total), axis=0, keepdims=True)
+    squares[...] = sums
+    kept[...] = sums
 
 
 def attend(tiles, own, other, slot, queries, maxima, acc, mask=None):
@@ -315,16 +317,16 @@
         name="rest",
     )(scaled, inv, second)
     before = lax.ppermute(tail, "sp", [(i, i + 1) for i in range(63)])
-    conv, squares = pl.pallas_call(
+    conv, squares, kept = pl.pallas_call(
         conv_kernel,
-        out_shape=[sent((ROWS, 128), F32), sent((1, ROWS), F32)],
+        out_shape=[shape((ROWS, 128), F32), sent((1, ROWS), F32), shape((1, ROWS), F32)],
         in_specs=[VM] * 3,
-        out_specs=[OUT] * 2,
+        out_specs=[VM, OUT, VM],
         scratch_shapes=[pltpu.VMEM((32 + ROWS, 128), F32)],
         compiler_params=SMALL,
         name="conv",
     )(glued, before, conv_weight)
-    sums = [squares] + [tp_shift(squares, by) for by in SHIFTS]
+    sums = [kept] + [tp_shift(squares, by) for by in SHIFTS]
 
     swapped = core_swap(gathered)
 

time: 147 us -> 146 us (level)
  local copies, waits for them, and re-layouts: 2.51 us -> 0.99 us
    unnamed x40 -> x36, local copies, waits for them, and re-layouts: 1.82 us -> 0.29 us
where the time goes in v4:
time: 146 us; the launch traced here: 145 us
  waiting for transfers between devices  62.5 us (43%)
  blocking collectives  33.9 us (23%)
  starting transfers between devices  28.8 us (20%)
  Pallas kernels  16.2 us (11%)
  other arithmetic  2.76 us (2%)
    ppermute x12, waiting for transfers between devices, tp_shift(): return lax.ppermute(x, 'tp', [(i, (i + by) % 4) for i in range(4)])  36.5 us
    all_to_all x1, blocking collectives, local(): lax.all_to_all(kv, 'sp', 0, 0, tiled=True, axis_index_groups=groups)  33.9 us
    ppermute x10, waiting for transfers between devices, along_sp(): return lax.ppermute(x, 'sp', pairs)  20.8 us
    ppermute x12, starting transfers between devices, tp_shift(): return lax.ppermute(x, 'tp', [(i, (i + by) % 4) for i in range(4)])  15.8 us
    ppermute x10, starting transfers between devices, along_sp(): return lax.ppermute(x, 'sp', pairs)  10.7 us
    pallas_call x1, Pallas kernels, local(): pl.pallas_call(remote_kernel, out_shape=[sent((MSG, ROWS))] * 3, in_specs...  5.93 us
    ppermute x1, waiting for transfers between devices, local(): before = lax.ppermute(tail, 'sp', [(i, i + 1) for i in range(63)])  5.16 us
  transfers between devices with their start and end apart: 23, of which 14 were waited for; matrix products, arithmetic and copies ran while one was open for 2% of the time, Pallas kernels for 8%

profile of v4, /device:TPU:32, one launch (start us, length us, event | category | flops | bytes accessed | tf_op | source)
XLA Modules:
  0.0 145.3 jit_solution(18425587838440321258)
XLA Ops:
  0.0 2.8 %collective-permute-start.1 = (bf16[256,512]{1,0:T(8,128)(2,1)}, bf16[256,512]{1,0:T(8,128)(2,1)S(1)}, u32[]{:S(2)}, u32[]{:S(2)}) collective-permute-start(bf16[256,512]{1,0:T(8,128)(2,1)} %t0.1), channel_id=1, source_target_pairs={{0,3},{1,0},{2,1},{3,2},{4,7},{5,4},{6,5},{7,6},{8,11},{9,8},{10,9... | collective-permute-start | bytes 786440 | tf_op jit(solution)/shard_map/ppermute | solution.py:60
  2.8 2.3 %collective-permute-start.2 = (bf16[256,512]{1,0:T(8,128)(2,1)}, bf16[256,512]{1,0:T(8,128)(2,1)S(1)}, u32[]{:S(2)}, u32[]{:S(2)}) collective-permute-start(bf16[256,512]{1,0:T(8,128)(2,1)} %t0.1), channel_id=1, source_target_pairs={{0,2},{1,3},{2,0},{3,1},{4,6},{5,7},{6,4},{7,5},{8,10},{9,11},{10,... | collective-permute-start | bytes 786440 | tf_op jit(solution)/shard_map/ppermute | solution.py:60
  7.1 1.4 pad_maximum_fusion.weights
  8.9 5.5 %collective-permute-done.1.t2 = bf16[256,512]{1,0:T(8,128)(2,1)S(1)} collective-permute-done((bf16[256,512]{1,0:T(8,128)(2,1)}, bf16[256,512]{1,0:T(8,128)(2,1)S(1)}, u32[]{:S(2)}, u32[]{:S(2)}) %collective-permute-start.1) | collective-permute-done | bytes 262176 | tf_op jit(solution)/shard_map/ppermute | solution.py:60
  14.4 3.3 %collective-permute-done.t1 = bf16[256,512]{1,0:T(8,128)(2,1)S(1)} collective-permute-done((bf16[256,512]{1,0:T(8,128)(2,1)}, bf16[256,512]{1,0:T(8,128)(2,1)S(1)}, u32[]{:S(2)}, u32[]{:S(2)}) %collective-permute-start) | collective-permute-done | bytes 262176 | tf_op jit(solution)/shard_map/ppermute | solution.py:60
  17.7 2.3 %project.1 = (bf16[256,256]{1,0:T(8,128)(2,1)}, bf16[8,512,128]{2,1,0:T(8,128)(2,1)}, bf16[4,256,512]{2,1,0:T(8,128)(2,1)}, f32[256,128]{1,0:T(8,128)}) custom-call(bf16[256,512]{1,0:T(8,128)(2,1)S(1)} %copy-done.3, bf16[256,512]{1,0:T(8,128)(2,1)S(1)} %collective-permute-done.t1, bf16[256,512]{1,0:T(8,128)(2,1)S(1)} %collective-permute-done.1.t2, ...), custom_call_target="tpu_custom_call" | custom-call | tf_op jit(solution)/shard_map/project/pallas_call | solution.py:297
  19.9 33.9 %all_to_all.5.own = bf16[8,512,128]{2,1,0:T(8,128)(2,1)S(1)} all-to-all(bf16[8,512,128]{2,1,0:T(8,128)(2,1)} %get-tuple-element.33), channel_id=1, replica_groups={{0,32,64,96,128,160,192,224},{4,36,68,100,132,164,196,228},{8,40,72,104..., dimensions={0} | all-to-all | bytes 2097152 | tf_op jit(solution)/shard_map/all_to_all | solution.py:307
  53.9 1.8 %collective-permute-start.9 = (bf16[384,1024]{1,0:T(8,128)(2,1)S(1)}, bf16[384,1024]{1,0:T(8,128)(2,1)S(1)}, u32[]{:S(2)}, u32[]{:S(2)}) collective-permute-start(bf16[384,1024]{1,0:T(8,128)(2,1)S(1)} %fusion), channel_id=1, source_target_pairs={{0,2},{1,3},{2,0},{3,1},{4,6},{5,7},{6,4},{7,5},{8,10},{9,11},{10,... | collective-permute-start | bytes 2359304 | tf_op jit(solution)/shard_map/ppermute | solution.py:60
  56.5 1.2 collective-permute-start.7
  57.7 3.2 %collective-permute-start.5 = (bf16[256,256]{1,0:T(8,128)(2,1)}, bf16[256,256]{1,0:T(8,128)(2,1)S(1)}, u32[]{:S(2)}, u32[]{:S(2)}) collective-permute-start(bf16[256,256]{1,0:T(8,128)(2,1)} %get-tuple-element.38.q0), channel_id=1, source_target_pairs={{0,16},{4,20},{8,24},{12,28},{16,0},{20,4},{24,8},{28,12},{32,48},... | collective-permute-start | bytes 393224 | tf_op jit(solution)/shard_map/ppermute | solution.py:48
  60.9 3.6 %collective-permute-done.5.q2 = bf16[256,256]{1,0:T(8,128)(2,1)S(1)} collective-permute-done((bf16[256,256]{1,0:T(8,128)(2,1)}, bf16[256,256]{1,0:T(8,128)(2,1)S(1)}, u32[]{:S(2)}, u32[]{:S(2)}) %collective-permute-start.5) | collective-permute-done | bytes 131104 | tf_op jit(solution)/shard_map/ppermute | solution.py:48
  64.5 3.0 %collective-permute-start.4 = (bf16[256,256]{1,0:T(8,128)(2,1)}, bf16[256,256]{1,0:T(8,128)(2,1)S(1)}, u32[]{:S(2)}, u32[]{:S(2)}) collective-permute-start(bf16[256,256]{1,0:T(8,128)(2,1)} %get-tuple-element.38.q0), channel_id=1, source_target_pairs={{0,24},{4,28},{8,0},{12,4},{16,8},{20,12},{24,16},{28,20},{32,56},... | collective-permute-start | bytes 393224 | tf_op jit(solution)/shard_map/ppermute | solution.py:48
  67.5 2.8 %collective-permute-done.4.q1 = bf16[256,256]{1,0:T(8,128)(2,1)S(1)} collective-permute-done((bf16[256,256]{1,0:T(8,128)(2,1)}, bf16[256,256]{1,0:T(8,128)(2,1)S(1)}, u32[]{:S(2)}, u32[]{:S(2)}) %collective-permute-start.4) | collective-permute-done | bytes 131104 | tf_op jit(solution)/shard_map/ppermute | solution.py:48
  71.2 5.8 %collective-permute-done.3.q0 = bf16[256,256]{1,0:T(8,128)(2,1)S(1)} collective-permute-done((bf16[256,256]{1,0:T(8,128)(2,1)}, bf16[256,256]{1,0:T(8,128)(2,1)S(1)}, u32[]{:S(2)}, u32[]{:S(2)}) %collective-permute-start.3) | collective-permute-done | bytes 131104 | tf_op jit(solution)/shard_map/ppermute | solution.py:48
  77.0 5.9 %remote.1 = (bf16[528,256]{1,0:T(8,128)(2,1)}, bf16[528,256]{1,0:T(8,128)(2,1)}, bf16[528,256]{1,0:T(8,128)(2,1)}) custom-call(bf16[256,256]{1,0:T(8,128)(2,1)S(1)} %collective-permute-done.3.q0, bf16[256,256]{1,0:T(8,128)(2,1)S(1)} %collective-permute-done.4.q1, bf16[256,256]{1,0:T(8,128)(2,1)S(1)} %collective-permute-done.5.q2, ...), custom_call_target="tpu_custom_call" | custom-call | tf_op jit(solution)/shard_map/remote/pallas_call | solution.py:340
  83.0 8.0 %collective-permute-done.8.a2 = bf16[384,1024]{1,0:T(8,128)(2,1)S(1)} collective-permute-done((bf16[384,1024]{1,0:T(8,128)(2,1)S(1)}, bf16[384,1024]{1,0:T(8,128)(2,1)S(1)}, u32[]{:S(2)}, u32[]{:S(2)}) %collective-permute-start.8) | collective-permute-done | bytes 786464 | tf_op jit(solution)/shard_map/ppermute | solution.py:60
  92.7 3.0 %collective-permute-start.10 = (bf16[528,256]{1,0:T(8,128)(2,1)}, bf16[528,256]{1,0:T(8,128)(2,1)S(1)}, u32[]{:S(2)}, u32[]{:S(2)}) collective-permute-start(bf16[528,256]{1,0:T(8,128)(2,1)} %get-tuple-element.34), channel_id=1, source_target_pairs={{0,24},{4,28},{8,0},{12,4},{16,8},{20,12},{24,16},{28,20},{32,56},... | collective-permute-start | bytes 811016 | tf_op jit(solution)/shard_map/ppermute | solution.py:48
  95.7 1.4 rest.1
  97.2 2.2 %collective-permute-start.13 = (bf16[32,128]{1,0:T(8,128)(2,1)}, bf16[32,128]{1,0:T(8,128)(2,1)S(1)}, u32[]{:S(2)}, u32[]{:S(2)}) collective-permute-start(bf16[32,128]{1,0:T(8,128)(2,1)} %get-tuple-element.43), channel_id=1, source_target_pairs={{0,4},{4,8},{8,12},{12,16},{16,20},{20,24},{24,28},{28,32},{32,36}... | collective-permute-start | bytes 24584 | tf_op jit(solution)/shard_map/ppermute | solution.py:319
  99.4 5.2 %collective-permute-done.13.before = bf16[32,128]{1,0:T(8,128)(2,1)S(1)} collective-permute-done((bf16[32,128]{1,0:T(8,128)(2,1)}, bf16[32,128]{1,0:T(8,128)(2,1)S(1)}, u32[]{:S(2)}, u32[]{:S(2)}) %collective-permute-start.13) | collective-permute-done | bytes 8224 | tf_op jit(solution)/shard_map/ppermute | solution.py:319
  105.6 1.8 %collective-permute-start.16 = (f32[1,256]{1,0:T(1,128)}, f32[1,256]{1,0:T(1,128)S(1)}, u32[]{:S(2)}, u32[]{:S(2)}) collective-permute-start(f32[1,256]{1,0:T(1,128)} %get-tuple-element.46), channel_id=1, source_target_pairs={{0,2},{1,3},{2,0},{3,1},{4,6},{5,7},{6,4},{7,5},{8,10},{9,11},{10,... | collective-permute-start | bytes 3080 | tf_op jit(solution)/shard_map/ppermute | solution.py:60
  107.4 3.5 %collective-permute-done.16.s3 = f32[1,256]{1,0:T(1,128)S(1)} collective-permute-done((f32[1,256]{1,0:T(1,128)}, f32[1,256]{1,0:T(1,128)S(1)}, u32[]{:S(2)}, u32[]{:S(2)}) %collective-permute-start.16) | collective-permute-done | bytes 1056 | tf_op jit(solution)/shard_map/ppermute | solution.py:60
  110.9 1.5 %collective-permute-start.15 = (f32[1,256]{1,0:T(1,128)}, f32[1,256]{1,0:T(1,128)S(1)}, u32[]{:S(2)}, u32[]{:S(2)}) collective-permute-start(f32[1,256]{1,0:T(1,128)} %get-tuple-element.46), channel_id=1, source_target_pairs={{0,3},{1,0},{2,1},{3,2},{4,7},{5,4},{6,5},{7,6},{8,11},{9,8},{10,9... | collective-permute-start | bytes 3080 | tf_op jit(solution)/shard_map/ppermute | solution.py:60
  112.4 2.3 %collective-permute-done.15.s2 = f32[1,256]{1,0:T(1,128)S(1)} collective-permute-done((f32[1,256]{1,0:T(1,128)}, f32[1,256]{1,0:T(1,128)S(1)}, u32[]{:S(2)}, u32[]{:S(2)}) %collective-permute-start.15) | collective-permute-done | bytes 1056 | tf_op jit(solution)/shard_map/ppermute | solution.py:60
  115.0 4.7 %collective-permute-done.14.s1 = f32[1,256]{1,0:T(1,128)S(1)} collective-permute-done((f32[1,256]{1,0:T(1,128)}, f32[1,256]{1,0:T(1,128)S(1)}, u32[]{:S(2)}, u32[]{:S(2)}) %collective-permute-start.14) | collective-permute-done | bytes 1056 | tf_op jit(solution)/shard_map/ppermute | solution.py:60
  119.8 1.9 %self.1.m0 = bf16[528,256]{1,0:T(8,128)(2,1)S(1)} custom-call(bf16[256,256]{1,0:T(8,128)(2,1)S(1)} %copy-done.4, bf16[8,512,128]{2,1,0:T(8,128)(2,1)S(1)} %all_to_all.5.own, bf16[8,512,128]{2,1,0:T(8,128)(2,1)S(1)} %collective-permute-done.6.other), custom_call_target="tpu_custom_call" | custom-call | tf_op jit(solution)/shard_map/self/pallas_call | solution.py:352
  121.7 8.6 %collective-permute-done.11.m2 = bf16[528,256]{1,0:T(8,128)(2,1)S(1)} collective-permute-done((bf16[528,256]{1,0:T(8,128)(2,1)S(1)}, bf16[528,256]{1,0:T(8,128)(2,1)S(1)}, u32[]{:S(2)}, u32[]{:S(2)}) %collective-permute-start.11) | collective-permute-done | bytes 270368 | tf_op jit(solution)/shard_map/ppermute | solution.py:48
  130.3 1.7 %merge.1 = (bf16[64,384]{1,0:T(8,128)(2,1)S(1)}, bf16[64,384]{1,0:T(8,128)(2,1)}, bf16[64,384]{1,0:T(8,128)(2,1)}, bf16[64,384]{1,0:T(8,128)(2,1)}) custom-call(bf16[528,256]{1,0:T(8,128)(2,1)S(1)} %self.1.m0, bf16[528,256]{1,0:T(8,128)(2,1)S(1)} %collective-permute-done.10.m1, bf16[528,256]{1,0:T(8,128)(2,1)S(1)} %collective-permute-done.11.m2, ...), custom_call_target="tpu_custom_call" | custom-call | tf_op jit(solution)/shard_map/merge/pallas_call | solution.py:362
  132.0 3.2 %collective-permute-start.18 = (bf16[64,384]{1,0:T(8,128)(2,1)}, bf16[64,384]{1,0:T(8,128)(2,1)S(1)}, u32[]{:S(2)}, u32[]{:S(2)}) collective-permute-start(bf16[64,384]{1,0:T(8,128)(2,1)} %get-tuple-element.50), channel_id=1, source_target_pairs={{0,3},{1,0},{2,1},{3,2},{4,7},{5,4},{6,5},{7,6},{8,11},{9,8},{10,9... | collective-permute-start | bytes 147464 | tf_op jit(solution)/shard_map/ppermute | solution.py:60
  135.2 2.3 %collective-permute-done.17.y1 = bf16[64,384]{1,0:T(8,128)(2,1)S(1)} collective-permute-done((bf16[64,384]{1,0:T(8,128)(2,1)}, bf16[64,384]{1,0:T(8,128)(2,1)S(1)}, u32[]{:S(2)}, u32[]{:S(2)}) %collective-permute-start.17) | collective-permute-done | bytes 49184 | tf_op jit(solution)/shard_map/ppermute | solution.py:60
  137.5 5.8 %collective-permute-done.19.y3 = bf16[64,384]{1,0:T(8,128)(2,1)S(1)} collective-permute-done((bf16[64,384]{1,0:T(8,128)(2,1)}, bf16[64,384]{1,0:T(8,128)(2,1)S(1)}, u32[]{:S(2)}, u32[]{:S(2)}) %collective-permute-start.19) | collective-permute-done | bytes 49184 | tf_op jit(solution)/shard_map/ppermute | solution.py:60
  143.3 2.0 %output.1 = bf16[64,2048]{1,0:T(8,128)(2,1)} custom-call(bf16[64,384]{1,0:T(8,128)(2,1)S(1)} %get-tuple-element.48.y0, bf16[64,384]{1,0:T(8,128)(2,1)S(1)} %collective-permute-done.17.y1, bf16[64,384]{1,0:T(8,128)(2,1)S(1)} %collective-permute-done.18.y2, bf16[64,384]{1,0:T(8,128)(2,1)S(1)} %collective-permute-done.19.y3, bf16[128,2048]{1,0:T(8,128)(2,1)S(1)} %copy-done.1, ...), custom_call_target="tpu_custom_call" | custom-call | tf_op jit(solution)/shard_map/output/pallas_call | solution.py:372
  (62 shorter events, 7.1 us)
Async XLA Ops:
  0.0 14.4 %collective-permute-start.1 = (bf16[256,512]{1,0:T(8,128)(2,1)}, bf16[256,512]{1,0:T(8,128)(2,1)S(1)}, u32[]{:S(2)}, u32[]{:S(2)}) collective-permute-start(bf16[256,512]{1,0:T(8,128)(2,1)} %t0.1), channel_id=1, source_target_pairs={{0,3},{1,0},{2,1},{3,2},{4,7},{5,4},{6,5},{7,6},{8,11},{9,8},{10,9... | collective-permute-start | bytes 786440 | tf_op jit(solution)/shard_map/ppermute | solution.py:60
  2.8 14.8 %collective-permute-start = (bf16[256,512]{1,0:T(8,128)(2,1)}, bf16[256,512]{1,0:T(8,128)(2,1)S(1)}, u32[]{:S(2)}, u32[]{:S(2)}) collective-permute-start(bf16[256,512]{1,0:T(8,128)(2,1)} %t0.1), channel_id=1, source_target_pairs={{0,1},{1,2},{2,3},{3,0},{4,5},{5,6},{6,7},{7,4},{8,9},{9,10},{10,1... | collective-permute-start | bytes 786440 | tf_op jit(solution)/shard_map/ppermute | solution.py:60
  2.8 14.8 %collective-permute-start.2 = (bf16[256,512]{1,0:T(8,128)(2,1)}, bf16[256,512]{1,0:T(8,128)(2,1)S(1)}, u32[]{:S(2)}, u32[]{:S(2)}) collective-permute-start(bf16[256,512]{1,0:T(8,128)(2,1)} %t0.1), channel_id=1, source_target_pairs={{0,2},{1,3},{2,0},{3,1},{4,6},{5,7},{6,4},{7,5},{8,10},{9,11},{10,... | collective-permute-start | bytes 786440 | tf_op jit(solution)/shard_map/ppermute | solution.py:60
  19.9 75.8 %copy-start.2 = (bf16[4,256,512]{2,1,0:T(8,128)(2,1)S(1)}, bf16[4,256,512]{2,1,0:T(8,128)(2,1)}, u32[]{:S(2)}) copy-start(bf16[4,256,512]{2,1,0:T(8,128)(2,1)} %get-tuple-element.39.scaled) | copy-start | bytes 3145732
  19.9 75.8 %copy-start.5 = (f32[256,128]{1,0:T(8,128)S(1)}, f32[256,128]{1,0:T(8,128)}, u32[]{:S(2)}) copy-start(f32[256,128]{1,0:T(8,128)} %get-tuple-element.40.inv_in) | copy-start | bytes 393220
  53.9 23.2 %collective-permute-start.6 = (bf16[8,512,128]{2,1,0:T(8,128)(2,1)S(1)}, bf16[8,512,128]{2,1,0:T(8,128)(2,1)S(1)}, u32[]{:S(2)}, u32[]{:S(2)}) collective-permute-start(bf16[8,512,128]{2,1,0:T(8,128)(2,1)S(1)} %all_to_all.5.own), channel_id=1, source_target_pairs={{0,4},{4,0},{8,12},{12,8},{16,20},{20,16},{24,28},{28,24},{32,36},... | collective-permute-start | bytes 3145736 | tf_op jit(solution)/shard_map/ppermute | solution.py:48
  53.9 29.1 %collective-permute-start.9 = (bf16[384,1024]{1,0:T(8,128)(2,1)S(1)}, bf16[384,1024]{1,0:T(8,128)(2,1)S(1)}, u32[]{:S(2)}, u32[]{:S(2)}) collective-permute-start(bf16[384,1024]{1,0:T(8,128)(2,1)S(1)} %fusion), channel_id=1, source_target_pairs={{0,2},{1,3},{2,0},{3,1},{4,6},{5,7},{6,4},{7,5},{8,10},{9,11},{10,... | collective-permute-start | bytes 2359304 | tf_op jit(solution)/shard_map/ppermute | solution.py:60
  55.7 35.4 %collective-permute-start.8 = (bf16[384,1024]{1,0:T(8,128)(2,1)S(1)}, bf16[384,1024]{1,0:T(8,128)(2,1)S(1)}, u32[]{:S(2)}, u32[]{:S(2)}) collective-permute-start(bf16[384,1024]{1,0:T(8,128)(2,1)S(1)} %fusion), channel_id=1, source_target_pairs={{0,3},{1,0},{2,1},{3,2},{4,7},{5,4},{6,5},{7,6},{8,11},{9,8},{10,9... | collective-permute-start | bytes 2359304 | tf_op jit(solution)/shard_map/ppermute | solution.py:60
  56.5 35.7 %collective-permute-start.7 = (bf16[384,1024]{1,0:T(8,128)(2,1)S(1)}, bf16[384,1024]{1,0:T(8,128)(2,1)S(1)}, u32[]{:S(2)}, u32[]{:S(2)}) collective-permute-start(bf16[384,1024]{1,0:T(8,128)(2,1)S(1)} %fusion), channel_id=1, source_target_pairs={{0,1},{1,2},{2,3},{3,0},{4,5},{5,6},{6,7},{7,4},{8,9},{9,10},{10,1... | collective-permute-start | bytes 2359304 | tf_op jit(solution)/shard_map/ppermute | solution.py:60
  57.7 46.9 %copy-start.6 = (bf16[31,128]{1,0:T(8,128)(2,1)S(1)}, bf16[31,128]{1,0:T(8,128)(2,1)}, u32[]{:S(2)}) copy-start(bf16[31,128]{1,0:T(8,128)(2,1)} %weight.1) | copy-start | bytes 23812
  57.7 62.1 %copy-start.4 = (bf16[256,256]{1,0:T(8,128)(2,1)S(1)}, bf16[256,256]{1,0:T(8,128)(2,1)}, u32[]{:S(2)}) copy-start(bf16[256,256]{1,0:T(8,128)(2,1)} %get-tuple-element.38.q0) | copy-start | bytes 393220
  57.7 6.8 %collective-permute-start.5 = (bf16[256,256]{1,0:T(8,128)(2,1)}, bf16[256,256]{1,0:T(8,128)(2,1)S(1)}, u32[]{:S(2)}, u32[]{:S(2)}) collective-permute-start(bf16[256,256]{1,0:T(8,128)(2,1)} %get-tuple-element.38.q0), channel_id=1, source_target_pairs={{0,16},{4,20},{8,24},{12,28},{16,0},{20,4},{24,8},{28,12},{32,48},... | collective-permute-start | bytes 393224 | tf_op jit(solution)/shard_map/ppermute | solution.py:48
  64.5 5.8 %collective-permute-start.4 = (bf16[256,256]{1,0:T(8,128)(2,1)}, bf16[256,256]{1,0:T(8,128)(2,1)S(1)}, u32[]{:S(2)}, u32[]{:S(2)}) collective-permute-start(bf16[256,256]{1,0:T(8,128)(2,1)} %get-tuple-element.38.q0), channel_id=1, source_target_pairs={{0,24},{4,28},{8,0},{12,4},{16,8},{20,12},{24,16},{28,20},{32,56},... | collective-permute-start | bytes 393224 | tf_op jit(solution)/shard_map/ppermute | solution.py:48
  70.3 6.7 %collective-permute-start.3 = (bf16[256,256]{1,0:T(8,128)(2,1)}, bf16[256,256]{1,0:T(8,128)(2,1)S(1)}, u32[]{:S(2)}, u32[]{:S(2)}) collective-permute-start(bf16[256,256]{1,0:T(8,128)(2,1)} %get-tuple-element.38.q0), channel_id=1, source_target_pairs={{0,8},{4,12},{8,16},{12,20},{16,24},{20,28},{24,0},{28,4},{32,40},... | collective-permute-start | bytes 393224 | tf_op jit(solution)/shard_map/ppermute | solution.py:48
  83.0 36.7 %copy-start.17 = (bf16[528,256]{1,0:T(8,128)(2,1)S(1)}, bf16[528,256]{1,0:T(8,128)(2,1)}, u32[]{:S(2)}) copy-start(bf16[528,256]{1,0:T(8,128)(2,1)} %get-tuple-element.35) | copy-start | bytes 811012
  83.0 36.7 %copy-start.16 = (bf16[528,256]{1,0:T(8,128)(2,1)S(1)}, bf16[528,256]{1,0:T(8,128)(2,1)}, u32[]{:S(2)}) copy-start(bf16[528,256]{1,0:T(8,128)(2,1)} %get-tuple-element.36) | copy-start | bytes 811012
  92.2 51.1 %collective-permute-start.20 = (bf16[384,1024]{1,0:T(8,128)(2,1)S(1)}, bf16[384,1024]{1,0:T(8,128)(2,1)S(1)}, u32[]{:S(2)}, u32[]{:S(2)}) collective-permute-start(bf16[384,1024]{1,0:T(8,128)(2,1)S(1)} %collective-permute-done.7.a1), channel_id=1, source_target_pairs={{0,4},{4,0},{8,12},{12,8},{16,20},{20,16},{24,28},{28,24},{32,36},... | collective-permute-start | bytes 2359304 | tf_op jit(solution)/shard_map/ppermute | solution.py:48
  92.2 51.1 %collective-permute-start.21 = (bf16[384,1024]{1,0:T(8,128)(2,1)S(1)}, bf16[384,1024]{1,0:T(8,128)(2,1)S(1)}, u32[]{:S(2)}, u32[]{:S(2)}) collective-permute-start(bf16[384,1024]{1,0:T(8,128)(2,1)S(1)} %collective-permute-done.8.a2), channel_id=1, source_target_pairs={{0,4},{4,0},{8,12},{12,8},{16,20},{20,16},{24,28},{28,24},{32,36},... | collective-permute-start | bytes 2359304 | tf_op jit(solution)/shard_map/ppermute | solution.py:48
  92.7 50.6 %collective-permute-start.22 = (bf16[384,1024]{1,0:T(8,128)(2,1)S(1)}, bf16[384,1024]{1,0:T(8,128)(2,1)S(1)}, u32[]{:S(2)}, u32[]{:S(2)}) collective-permute-start(bf16[384,1024]{1,0:T(8,128)(2,1)S(1)} %collective-permute-done.9.a3), channel_id=1, source_target_pairs={{0,4},{4,0},{8,12},{12,8},{16,20},{20,16},{24,28},{28,24},{32,36},... | collective-permute-start | bytes 2359304 | tf_op jit(solution)/shard_map/ppermute | solution.py:48
  92.7 27.0 %collective-permute-start.10 = (bf16[528,256]{1,0:T(8,128)(2,1)}, bf16[528,256]{1,0:T(8,128)(2,1)S(1)}, u32[]{:S(2)}, u32[]{:S(2)}) collective-permute-start(bf16[528,256]{1,0:T(8,128)(2,1)} %get-tuple-element.34), channel_id=1, source_target_pairs={{0,24},{4,28},{8,0},{12,4},{16,8},{20,12},{24,16},{28,20},{32,56},... | collective-permute-start | bytes 811016 | tf_op jit(solution)/shard_map/ppermute | solution.py:48
  95.7 34.5 %copy-start.8 = (f32[2]{0:T(128)S(1)}, f32[2]{0:T(128)}, u32[]{:S(2)}) copy-start(f32[2]{0:T(128)} %lam.1) | copy-start | bytes 28
  97.2 46.1 %copy-start = (bf16[256,2048]{1,0:T(8,128)(2,1)S(1)}, bf16[256,2048]{1,0:T(8,128)(2,1)}, u32[]{:S(2)}) copy-start(bf16[256,2048]{1,0:T(8,128)(2,1)} %w_attn.1) | copy-start | bytes 3145732
  97.2 46.1 %copy-start.1 = (bf16[128,2048]{1,0:T(8,128)(2,1)S(1)}, bf16[128,2048]{1,0:T(8,128)(2,1)}, u32[]{:S(2)}) copy-start(bf16[128,2048]{1,0:T(8,128)(2,1)} %w_conv.1) | copy-start | bytes 1572868
  97.2 7.4 %collective-permute-start.13 = (bf16[32,128]{1,0:T(8,128)(2,1)}, bf16[32,128]{1,0:T(8,128)(2,1)S(1)}, u32[]{:S(2)}, u32[]{:S(2)}) collective-permute-start(bf16[32,128]{1,0:T(8,128)(2,1)} %get-tuple-element.43), channel_id=1, source_target_pairs={{0,4},{4,8},{8,12},{12,16},{16,20},{20,24},{24,28},{28,32},{32,36}... | collective-permute-start | bytes 24584 | tf_op jit(solution)/shard_map/ppermute | solution.py:319
  105.6 5.3 %collective-permute-start.16 = (f32[1,256]{1,0:T(1,128)}, f32[1,256]{1,0:T(1,128)S(1)}, u32[]{:S(2)}, u32[]{:S(2)}) collective-permute-start(f32[1,256]{1,0:T(1,128)} %get-tuple-element.46), channel_id=1, source_target_pairs={{0,2},{1,3},{2,0},{3,1},{4,6},{5,7},{6,4},{7,5},{8,10},{9,11},{10,... | collective-permute-start | bytes 3080 | tf_op jit(solution)/shard_map/ppermute | solution.py:60
  110.9 3.8 %collective-permute-start.15 = (f32[1,256]{1,0:T(1,128)}, f32[1,256]{1,0:T(1,128)S(1)}, u32[]{:S(2)}, u32[]{:S(2)}) collective-permute-start(f32[1,256]{1,0:T(1,128)} %get-tuple-element.46), channel_id=1, source_target_pairs={{0,3},{1,0},{2,1},{3,2},{4,7},{5,4},{6,5},{7,6},{8,11},{9,8},{10,9... | collective-permute-start | bytes 3080 | tf_op jit(solution)/shard_map/ppermute | solution.py:60
  114.7 5.0 %collective-permute-start.14 = (f32[1,256]{1,0:T(1,128)}, f32[1,256]{1,0:T(1,128)S(1)}, u32[]{:S(2)}, u32[]{:S(2)}) collective-permute-start(f32[1,256]{1,0:T(1,128)} %get-tuple-element.46), channel_id=1, source_target_pairs={{0,1},{1,2},{2,3},{3,0},{4,5},{5,6},{6,7},{7,4},{8,9},{9,10},{10,1... | collective-permute-start | bytes 3080 | tf_op jit(solution)/shard_map/ppermute | solution.py:60
  119.7 10.6 %collective-permute-start.11 = (bf16[528,256]{1,0:T(8,128)(2,1)S(1)}, bf16[528,256]{1,0:T(8,128)(2,1)S(1)}, u32[]{:S(2)}, u32[]{:S(2)}) collective-permute-start(bf16[528,256]{1,0:T(8,128)(2,1)S(1)} %copy-done.17), channel_id=1, source_target_pairs={{0,8},{4,12},{8,16},{12,20},{16,24},{20,28},{24,0},{28,4},{32,40},... | collective-permute-start | bytes 811016 | tf_op jit(solution)/shard_map/ppermute | solution.py:48
  119.7 10.6 %collective-permute-start.12 = (bf16[528,256]{1,0:T(8,128)(2,1)S(1)}, bf16[528,256]{1,0:T(8,128)(2,1)S(1)}, u32[]{:S(2)}, u32[]{:S(2)}) collective-permute-start(bf16[528,256]{1,0:T(8,128)(2,1)S(1)} %copy-done.16), channel_id=1, source_target_pairs={{0,16},{4,20},{8,24},{12,28},{16,0},{20,4},{24,8},{28,12},{32,48},... | collective-permute-start | bytes 811016 | tf_op jit(solution)/shard_map/ppermute | solution.py:48
  132.0 5.5 %collective-permute-start.17 = (bf16[64,384]{1,0:T(8,128)(2,1)}, bf16[64,384]{1,0:T(8,128)(2,1)S(1)}, u32[]{:S(2)}, u32[]{:S(2)}) collective-permute-start(bf16[64,384]{1,0:T(8,128)(2,1)} %get-tuple-element.49), channel_id=1, source_target_pairs={{0,1},{1,2},{2,3},{3,0},{4,5},{5,6},{6,7},{7,4},{8,9},{9,10},{10,1... | collective-permute-start | bytes 147464 | tf_op jit(solution)/shard_map/ppermute | solution.py:60
  132.0 5.5 %collective-permute-start.18 = (bf16[64,384]{1,0:T(8,128)(2,1)}, bf16[64,384]{1,0:T(8,128)(2,1)S(1)}, u32[]{:S(2)}, u32[]{:S(2)}) collective-permute-start(bf16[64,384]{1,0:T(8,128)(2,1)} %get-tuple-element.50), channel_id=1, source_target_pairs={{0,3},{1,0},{2,1},{3,2},{4,7},{5,4},{6,5},{7,6},{8,11},{9,8},{10,9... | collective-permute-start | bytes 147464 | tf_op jit(solution)/shard_map/ppermute | solution.py:60
  137.5 5.8 %collective-permute-start.19 = (bf16[64,384]{1,0:T(8,128)(2,1)}, bf16[64,384]{1,0:T(8,128)(2,1)S(1)}, u32[]{:S(2)}, u32[]{:S(2)}) collective-permute-start(bf16[64,384]{1,0:T(8,128)(2,1)} %get-tuple-element.51), channel_id=1, source_target_pairs={{0,2},{1,3},{2,0},{3,1},{4,6},{5,7},{6,4},{7,5},{8,10},{9,11},{10,... | collective-permute-start | bytes 147464 | tf_op jit(solution)/shard_map/ppermute | solution.py:60
  (9 other events, 103.6 us)

commit v5 on v4

--- a/solution.py
+++ b/solution.py
@@ -112,32 +112,41 @@
     kept[...] = sums
 
 
-def attend(tiles, own, other, slot, queries, maxima, acc, mask=None):
-    keys = jnp.concatenate([own[slot, 0:256, :], other[slot, 0:256, :]], axis=0)
-    keys = jnp.concatenate([keys, keys], axis=1)
-    values = jnp.concatenate(
-        [
-            own[slot, 256:384, :],
-            own[slot, 384:512, :],
-            other[slot, 256:384, :],
-            other[slot, 384:512, :],
-        ],
-        axis=1,
-    )
-    values = jnp.concatenate([values, jnp.ones((ACC - VDIM, 512), BF16)], axis=0)
-    ahead = [dot(keys, queries[t]) for t in tiles[:DEPTH]]
-    for i, t in enumerate(tiles):
+def attend(tiles, own, other, slots, queries, maxima, acc, mask=None):
+    keys, values, units = [], [], []
+    for n, slot in enumerate(slots):
+        both = jnp.concatenate([own[slot, 0:256, :], other[slot, 0:256, :]], axis=0)
+        keys.append(jnp.concatenate([both, both], axis=1))
+        parts = [ref[slot, r : r + 128, :] for ref in (own, other) for r in (256, 384)]
+        ones = jnp.ones((ACC - VDIM, 512), BF16)
+        values.append(jnp.concatenate([jnp.concatenate(parts, axis=1), ones], axis=0))
+        units += [(t, n) for t in tiles]
+    ahead = [dot(keys[n], queries[t]) for t, n in units[:DEPTH]]
+    for i, (t, n) in enumerate(units):
         scores = ahead.pop(0)
-        if i + DEPTH < len(tiles):
-            ahead.append(dot(keys, queries[tiles[i + DEPTH]]))
+        if i + DEPTH < len(units):
+            later, m = units[i + DEPTH]
+            ahead.append(dot(keys[m], queries[later]))
         if mask is not None:
             scores = jnp.where(mask, scores, NEG_BIG)
         old = maxima[t]
         new = jnp.maximum(old, jnp.max(scores, axis=0, keepdims=True))
         factor = jnp.exp2(old - new)
         expd = jnp.exp2(scores - new).astype(BF16)
-        acc[t] = acc[t] * factor + dot(values, expd)
+        acc[t] = acc[t] * factor + dot(values[n], expd)
         maxima[t] = new
+
+
+def attend_before(z, tiles, own, other, queries, maxima, acc):
+    def visit(i, carry):
+        attend(tiles, own, other, (2 * i, 2 * i + 1), queries, maxima, acc)
+        return carry
+
+    lax.fori_loop(0, z // 2, visit, 0)
+
+    @pl.when(lax.rem(z, 2) == 1)
+    def _():
+        attend(tiles, own, other, (z - 1,), queries, maxima, acc)
 
 
 def lay_queries(q_refs, queries):
@@ -186,16 +195,12 @@
     lay_queries((q0, q1, q2), queries)
     start_state(maxima, acc)
 
-    def visit(i, carry):
-        attend(range(12), own, other, i, queries, maxima, acc)
-        return carry
-
-    lax.fori_loop(0, z, visit, 0)
+    attend_before(z, range(12), own, other, queries, maxima, acc)
     for b, by in enumerate(SHIFTS):
 
         @pl.when(lax.rem(y - by + 4, 4) > y)
         def _(b=b):
-            attend(range(4 * b, 4 * b + 4), own, other, z, queries, maxima, acc)
+            attend(range(4 * b, 4 * b + 4), own, other, (z,), queries, maxima, acc)
 
     for b, out in enumerate((o0, o1, o2)):
         write_part(out, 4 * b, maxima, acc)
@@ -208,13 +213,9 @@
     row = lax.broadcasted_iota(jnp.int32, (512, ROWS), 0)
     key_row = jnp.where(row < ROWS, row + c * ROWS, row - c * ROWS)
     query_row = lax.broadcasted_iota(jnp.int32, (512, ROWS), 1) + c * ROWS
-    attend(range(4), own, other, z, queries, maxima, acc, key_row <= query_row)
-
-    def visit(i, carry):
-        attend(range(4), own, other, i, queries, maxima, acc)
-        return carry
-
-    lax.fori_loop(0, z, visit, 0)
+    attend(range(4), own, other, (z,), queries, maxima, acc, key_row <= query_row)
+
+    attend_before(z, range(4), own, other, queries, maxima, acc)
     write_part(out, 0, maxima, acc)
 
 

time: 146 us -> 146 us (level)
  no operation moved by 1% of the time
where the time goes in v5:
time: 146 us; the launch traced here: 145 us
  waiting for transfers between devices  62.3 us (43%)
  blocking collectives  33.9 us (23%)
  starting transfers between devices  28.8 us (20%)
  Pallas kernels  16.4 us (11%)
  other arithmetic  2.76 us (2%)
    ppermute x12, waiting for transfers between devices, tp_shift(): return lax.ppermute(x, 'tp', [(i, (i + by) % 4) for i in range(4)])  36.5 us
    all_to_all x1, blocking collectives, local(): lax.all_to_all(kv, 'sp', 0, 0, tiled=True, axis_index_groups=groups)  33.9 us
    ppermute x10, waiting for transfers between devices, along_sp(): return lax.ppermute(x, 'sp', pairs)  20.6 us
    ppermute x12, starting transfers between devices, tp_shift(): return lax.ppermute(x, 'tp', [(i, (i + by) % 4) for i in range(4)])  15.8 us
    ppermute x10, starting transfers between devices, along_sp(): return lax.ppermute(x, 'sp', pairs)  10.7 us
    pallas_call x1, Pallas kernels, local(): pl.pallas_call(remote_kernel, out_shape=[sent((MSG, ROWS))] * 3, in_specs...  5.93 us
    ppermute x1, waiting for transfers between devices, local(): before = lax.ppermute(tail, 'sp', [(i, i + 1) for i in range(63)])  5.16 us
  transfers between devices with their start and end apart: 23, of which 14 were waited for; matrix products, arithmetic and copies ran while one was open for 2% of the time, Pallas kernels for 8%

profile of v5, /device:TPU:32, one launch (start us, length us, event | category | flops | bytes accessed | tf_op | source)
XLA Modules:
  0.0 145.3 jit_solution(5066084183604913098)
XLA Ops:
  0.0 2.8 %collective-permute-start.1 = (bf16[256,512]{1,0:T(8,128)(2,1)}, bf16[256,512]{1,0:T(8,128)(2,1)S(1)}, u32[]{:S(2)}, u32[]{:S(2)}) collective-permute-start(bf16[256,512]{1,0:T(8,128)(2,1)} %t0.1), channel_id=1, source_target_pairs={{0,3},{1,0},{2,1},{3,2},{4,7},{5,4},{6,5},{7,6},{8,11},{9,8},{10,9... | collective-permute-start | bytes 786440 | tf_op jit(solution)/shard_map/ppermute | solution.py:60
  2.8 2.3 %collective-permute-start.2 = (bf16[256,512]{1,0:T(8,128)(2,1)}, bf16[256,512]{1,0:T(8,128)(2,1)S(1)}, u32[]{:S(2)}, u32[]{:S(2)}) collective-permute-start(bf16[256,512]{1,0:T(8,128)(2,1)} %t0.1), channel_id=1, source_target_pairs={{0,2},{1,3},{2,0},{3,1},{4,6},{5,7},{6,4},{7,5},{8,10},{9,11},{10,... | collective-permute-start | bytes 786440 | tf_op jit(solution)/shard_map/ppermute | solution.py:60
  7.1 1.4 pad_maximum_fusion.weights
  8.9 5.5 %collective-permute-done.1.t2 = bf16[256,512]{1,0:T(8,128)(2,1)S(1)} collective-permute-done((bf16[256,512]{1,0:T(8,128)(2,1)}, bf16[256,512]{1,0:T(8,128)(2,1)S(1)}, u32[]{:S(2)}, u32[]{:S(2)}) %collective-permute-start.1) | collective-permute-done | bytes 262176 | tf_op jit(solution)/shard_map/ppermute | solution.py:60
  14.4 3.3 %collective-permute-done.t1 = bf16[256,512]{1,0:T(8,128)(2,1)S(1)} collective-permute-done((bf16[256,512]{1,0:T(8,128)(2,1)}, bf16[256,512]{1,0:T(8,128)(2,1)S(1)}, u32[]{:S(2)}, u32[]{:S(2)}) %collective-permute-start) | collective-permute-done | bytes 262176 | tf_op jit(solution)/shard_map/ppermute | solution.py:60
  17.7 2.3 %project.1 = (bf16[256,256]{1,0:T(8,128)(2,1)}, bf16[8,512,128]{2,1,0:T(8,128)(2,1)}, bf16[4,256,512]{2,1,0:T(8,128)(2,1)}, f32[256,128]{1,0:T(8,128)}) custom-call(bf16[256,512]{1,0:T(8,128)(2,1)S(1)} %copy-done.3, bf16[256,512]{1,0:T(8,128)(2,1)S(1)} %collective-permute-done.t1, bf16[256,512]{1,0:T(8,128)(2,1)S(1)} %collective-permute-done.1.t2, ...), custom_call_target="tpu_custom_call" | custom-call | tf_op jit(solution)/shard_map/project/pallas_call | solution.py:298
  19.9 33.9 %all_to_all.5.own = bf16[8,512,128]{2,1,0:T(8,128)(2,1)S(1)} all-to-all(bf16[8,512,128]{2,1,0:T(8,128)(2,1)} %get-tuple-element.33), channel_id=1, replica_groups={{0,32,64,96,128,160,192,224},{4,36,68,100,132,164,196,228},{8,40,72,104..., dimensions={0} | all-to-all | bytes 2097152 | tf_op jit(solution)/shard_map/all_to_all | solution.py:308
  53.9 1.8 %collective-permute-start.9 = (bf16[384,1024]{1,0:T(8,128)(2,1)S(1)}, bf16[384,1024]{1,0:T(8,128)(2,1)S(1)}, u32[]{:S(2)}, u32[]{:S(2)}) collective-permute-start(bf16[384,1024]{1,0:T(8,128)(2,1)S(1)} %fusion), channel_id=1, source_target_pairs={{0,2},{1,3},{2,0},{3,1},{4,6},{5,7},{6,4},{7,5},{8,10},{9,11},{10,... | collective-permute-start | bytes 2359304 | tf_op jit(solution)/shard_map/ppermute | solution.py:60
  56.5 1.2 collective-permute-start.7
  57.7 3.2 %collective-permute-start.5 = (bf16[256,256]{1,0:T(8,128)(2,1)}, bf16[256,256]{1,0:T(8,128)(2,1)S(1)}, u32[]{:S(2)}, u32[]{:S(2)}) collective-permute-start(bf16[256,256]{1,0:T(8,128)(2,1)} %get-tuple-element.38.q0), channel_id=1, source_target_pairs={{0,16},{4,20},{8,24},{12,28},{16,0},{20,4},{24,8},{28,12},{32,48},... | collective-permute-start | bytes 393224 | tf_op jit(solution)/shard_map/ppermute | solution.py:48
  60.9 3.6 %collective-permute-done.5.q2 = bf16[256,256]{1,0:T(8,128)(2,1)S(1)} collective-permute-done((bf16[256,256]{1,0:T(8,128)(2,1)}, bf16[256,256]{1,0:T(8,128)(2,1)S(1)}, u32[]{:S(2)}, u32[]{:S(2)}) %collective-permute-start.5) | collective-permute-done | bytes 131104 | tf_op jit(solution)/shard_map/ppermute | solution.py:48
  64.5 3.0 %collective-permute-start.4 = (bf16[256,256]{1,0:T(8,128)(2,1)}, bf16[256,256]{1,0:T(8,128)(2,1)S(1)}, u32[]{:S(2)}, u32[]{:S(2)}) collective-permute-start(bf16[256,256]{1,0:T(8,128)(2,1)} %get-tuple-element.38.q0), channel_id=1, source_target_pairs={{0,24},{4,28},{8,0},{12,4},{16,8},{20,12},{24,16},{28,20},{32,56},... | collective-permute-start | bytes 393224 | tf_op jit(solution)/shard_map/ppermute | solution.py:48
  67.5 2.8 %collective-permute-done.4.q1 = bf16[256,256]{1,0:T(8,128)(2,1)S(1)} collective-permute-done((bf16[256,256]{1,0:T(8,128)(2,1)}, bf16[256,256]{1,0:T(8,128)(2,1)S(1)}, u32[]{:S(2)}, u32[]{:S(2)}) %collective-permute-start.4) | collective-permute-done | bytes 131104 | tf_op jit(solution)/shard_map/ppermute | solution.py:48
  71.2 5.8 %collective-permute-done.3.q0 = bf16[256,256]{1,0:T(8,128)(2,1)S(1)} collective-permute-done((bf16[256,256]{1,0:T(8,128)(2,1)}, bf16[256,256]{1,0:T(8,128)(2,1)S(1)}, u32[]{:S(2)}, u32[]{:S(2)}) %collective-permute-start.3) | collective-permute-done | bytes 131104 | tf_op jit(solution)/shard_map/ppermute | solution.py:48
  77.0 5.9 %remote.1 = (bf16[528,256]{1,0:T(8,128)(2,1)}, bf16[528,256]{1,0:T(8,128)(2,1)}, bf16[528,256]{1,0:T(8,128)(2,1)}) custom-call(bf16[256,256]{1,0:T(8,128)(2,1)S(1)} %collective-permute-done.3.q0, bf16[256,256]{1,0:T(8,128)(2,1)S(1)} %collective-permute-done.4.q1, bf16[256,256]{1,0:T(8,128)(2,1)S(1)} %collective-permute-done.5.q2, ...), custom_call_target="tpu_custom_call" | custom-call | tf_op jit(solution)/shard_map/remote/pallas_call | solution.py:341
  83.0 8.0 %collective-permute-done.8.a2 = bf16[384,1024]{1,0:T(8,128)(2,1)S(1)} collective-permute-done((bf16[384,1024]{1,0:T(8,128)(2,1)S(1)}, bf16[384,1024]{1,0:T(8,128)(2,1)S(1)}, u32[]{:S(2)}, u32[]{:S(2)}) %collective-permute-start.8) | collective-permute-done | bytes 786464 | tf_op jit(solution)/shard_map/ppermute | solution.py:60
  92.7 3.0 %collective-permute-start.10 = (bf16[528,256]{1,0:T(8,128)(2,1)}, bf16[528,256]{1,0:T(8,128)(2,1)S(1)}, u32[]{:S(2)}, u32[]{:S(2)}) collective-permute-start(bf16[528,256]{1,0:T(8,128)(2,1)} %get-tuple-element.34), channel_id=1, source_target_pairs={{0,24},{4,28},{8,0},{12,4},{16,8},{20,12},{24,16},{28,20},{32,56},... | collective-permute-start | bytes 811016 | tf_op jit(solution)/shard_map/ppermute | solution.py:48
  95.7 1.4 rest.1
  97.2 2.2 %collective-permute-start.13 = (bf16[32,128]{1,0:T(8,128)(2,1)}, bf16[32,128]{1,0:T(8,128)(2,1)S(1)}, u32[]{:S(2)}, u32[]{:S(2)}) collective-permute-start(bf16[32,128]{1,0:T(8,128)(2,1)} %get-tuple-element.43), channel_id=1, source_target_pairs={{0,4},{4,8},{8,12},{12,16},{16,20},{20,24},{24,28},{28,32},{32,36}... | collective-permute-start | bytes 24584 | tf_op jit(solution)/shard_map/ppermute | solution.py:320
  99.4 5.2 %collective-permute-done.13.before = bf16[32,128]{1,0:T(8,128)(2,1)S(1)} collective-permute-done((bf16[32,128]{1,0:T(8,128)(2,1)}, bf16[32,128]{1,0:T(8,128)(2,1)S(1)}, u32[]{:S(2)}, u32[]{:S(2)}) %collective-permute-start.13) | collective-permute-done | bytes 8224 | tf_op jit(solution)/shard_map/ppermute | solution.py:320
  105.6 1.8 %collective-permute-start.16 = (f32[1,256]{1,0:T(1,128)}, f32[1,256]{1,0:T(1,128)S(1)}, u32[]{:S(2)}, u32[]{:S(2)}) collective-permute-start(f32[1,256]{1,0:T(1,128)} %get-tuple-element.46), channel_id=1, source_target_pairs={{0,2},{1,3},{2,0},{3,1},{4,6},{5,7},{6,4},{7,5},{8,10},{9,11},{10,... | collective-permute-start | bytes 3080 | tf_op jit(solution)/shard_map/ppermute | solution.py:60
  107.4 3.5 %collective-permute-done.16.s3 = f32[1,256]{1,0:T(1,128)S(1)} collective-permute-done((f32[1,256]{1,0:T(1,128)}, f32[1,256]{1,0:T(1,128)S(1)}, u32[]{:S(2)}, u32[]{:S(2)}) %collective-permute-start.16) | collective-permute-done | bytes 1056 | tf_op jit(solution)/shard_map/ppermute | solution.py:60
  110.9 1.5 %collective-permute-start.15 = (f32[1,256]{1,0:T(1,128)}, f32[1,256]{1,0:T(1,128)S(1)}, u32[]{:S(2)}, u32[]{:S(2)}) collective-permute-start(f32[1,256]{1,0:T(1,128)} %get-tuple-element.46), channel_id=1, source_target_pairs={{0,3},{1,0},{2,1},{3,2},{4,7},{5,4},{6,5},{7,6},{8,11},{9,8},{10,9... | collective-permute-start | bytes 3080 | tf_op jit(solution)/shard_map/ppermute | solution.py:60
  112.4 2.3 %collective-permute-done.15.s2 = f32[1,256]{1,0:T(1,128)S(1)} collective-permute-done((f32[1,256]{1,0:T(1,128)}, f32[1,256]{1,0:T(1,128)S(1)}, u32[]{:S(2)}, u32[]{:S(2)}) %collective-permute-start.15) | collective-permute-done | bytes 1056 | tf_op jit(solution)/shard_map/ppermute | solution.py:60
  115.0 4.7 %collective-permute-done.14.s1 = f32[1,256]{1,0:T(1,128)S(1)} collective-permute-done((f32[1,256]{1,0:T(1,128)}, f32[1,256]{1,0:T(1,128)S(1)}, u32[]{:S(2)}, u32[]{:S(2)}) %collective-permute-start.14) | collective-permute-done | bytes 1056 | tf_op jit(solution)/shard_map/ppermute | solution.py:60
  119.8 2.1 %self.1.m0 = bf16[528,256]{1,0:T(8,128)(2,1)S(1)} custom-call(bf16[256,256]{1,0:T(8,128)(2,1)S(1)} %copy-done.4, bf16[8,512,128]{2,1,0:T(8,128)(2,1)S(1)} %all_to_all.5.own, bf16[8,512,128]{2,1,0:T(8,128)(2,1)S(1)} %collective-permute-done.6.other), custom_call_target="tpu_custom_call" | custom-call | tf_op jit(solution)/shard_map/self/pallas_call | solution.py:353
  121.9 8.4 %collective-permute-done.11.m2 = bf16[528,256]{1,0:T(8,128)(2,1)S(1)} collective-permute-done((bf16[528,256]{1,0:T(8,128)(2,1)S(1)}, bf16[528,256]{1,0:T(8,128)(2,1)S(1)}, u32[]{:S(2)}, u32[]{:S(2)}) %collective-permute-start.11) | collective-permute-done | bytes 270368 | tf_op jit(solution)/shard_map/ppermute | solution.py:48
  130.3 1.7 %merge.1 = (bf16[64,384]{1,0:T(8,128)(2,1)S(1)}, bf16[64,384]{1,0:T(8,128)(2,1)}, bf16[64,384]{1,0:T(8,128)(2,1)}, bf16[64,384]{1,0:T(8,128)(2,1)}) custom-call(bf16[528,256]{1,0:T(8,128)(2,1)S(1)} %self.1.m0, bf16[528,256]{1,0:T(8,128)(2,1)S(1)} %collective-permute-done.10.m1, bf16[528,256]{1,0:T(8,128)(2,1)S(1)} %collective-permute-done.11.m2, ...), custom_call_target="tpu_custom_call" | custom-call | tf_op jit(solution)/shard_map/merge/pallas_call | solution.py:363
  132.0 3.2 %collective-permute-start.18 = (bf16[64,384]{1,0:T(8,128)(2,1)}, bf16[64,384]{1,0:T(8,128)(2,1)S(1)}, u32[]{:S(2)}, u32[]{:S(2)}) collective-permute-start(bf16[64,384]{1,0:T(8,128)(2,1)} %get-tuple-element.50), channel_id=1, source_target_pairs={{0,3},{1,0},{2,1},{3,2},{4,7},{5,4},{6,5},{7,6},{8,11},{9,8},{10,9... | collective-permute-start | bytes 147464 | tf_op jit(solution)/shard_map/ppermute | solution.py:60
  135.2 2.3 %collective-permute-done.17.y1 = bf16[64,384]{1,0:T(8,128)(2,1)S(1)} collective-permute-done((bf16[64,384]{1,0:T(8,128)(2,1)}, bf16[64,384]{1,0:T(8,128)(2,1)S(1)}, u32[]{:S(2)}, u32[]{:S(2)}) %collective-permute-start.17) | collective-permute-done | bytes 49184 | tf_op jit(solution)/shard_map/ppermute | solution.py:60
  137.5 5.8 %collective-permute-done.19.y3 = bf16[64,384]{1,0:T(8,128)(2,1)S(1)} collective-permute-done((bf16[64,384]{1,0:T(8,128)(2,1)}, bf16[64,384]{1,0:T(8,128)(2,1)S(1)}, u32[]{:S(2)}, u32[]{:S(2)}) %collective-permute-start.19) | collective-permute-done | bytes 49184 | tf_op jit(solution)/shard_map/ppermute | solution.py:60
  143.3 2.0 %output.1 = bf16[64,2048]{1,0:T(8,128)(2,1)} custom-call(bf16[64,384]{1,0:T(8,128)(2,1)S(1)} %get-tuple-element.48.y0, bf16[64,384]{1,0:T(8,128)(2,1)S(1)} %collective-permute-done.17.y1, bf16[64,384]{1,0:T(8,128)(2,1)S(1)} %collective-permute-done.18.y2, bf16[64,384]{1,0:T(8,128)(2,1)S(1)} %collective-permute-done.19.y3, bf16[128,2048]{1,0:T(8,128)(2,1)S(1)} %copy-done.1, ...), custom_call_target="tpu_custom_call" | custom-call | tf_op jit(solution)/shard_map/output/pallas_call | solution.py:373
  (62 shorter events, 7.1 us)
Async XLA Ops:
  0.0 14.4 %collective-permute-start.1 = (bf16[256,512]{1,0:T(8,128)(2,1)}, bf16[256,512]{1,0:T(8,128)(2,1)S(1)}, u32[]{:S(2)}, u32[]{:S(2)}) collective-permute-start(bf16[256,512]{1,0:T(8,128)(2,1)} %t0.1), channel_id=1, source_target_pairs={{0,3},{1,0},{2,1},{3,2},{4,7},{5,4},{6,5},{7,6},{8,11},{9,8},{10,9... | collective-permute-start | bytes 786440 | tf_op jit(solution)/shard_map/ppermute | solution.py:60
  2.8 14.8 %collective-permute-start = (bf16[256,512]{1,0:T(8,128)(2,1)}, bf16[256,512]{1,0:T(8,128)(2,1)S(1)}, u32[]{:S(2)}, u32[]{:S(2)}) collective-permute-start(bf16[256,512]{1,0:T(8,128)(2,1)} %t0.1), channel_id=1, source_target_pairs={{0,1},{1,2},{2,3},{3,0},{4,5},{5,6},{6,7},{7,4},{8,9},{9,10},{10,1... | collective-permute-start | bytes 786440 | tf_op jit(solution)/shard_map/ppermute | solution.py:60
  2.8 14.8 %collective-permute-start.2 = (bf16[256,512]{1,0:T(8,128)(2,1)}, bf16[256,512]{1,0:T(8,128)(2,1)S(1)}, u32[]{:S(2)}, u32[]{:S(2)}) collective-permute-start(bf16[256,512]{1,0:T(8,128)(2,1)} %t0.1), channel_id=1, source_target_pairs={{0,2},{1,3},{2,0},{3,1},{4,6},{5,7},{6,4},{7,5},{8,10},{9,11},{10,... | collective-permute-start | bytes 786440 | tf_op jit(solution)/shard_map/ppermute | solution.py:60
  19.9 75.8 %copy-start.2 = (bf16[4,256,512]{2,1,0:T(8,128)(2,1)S(1)}, bf16[4,256,512]{2,1,0:T(8,128)(2,1)}, u32[]{:S(2)}) copy-start(bf16[4,256,512]{2,1,0:T(8,128)(2,1)} %get-tuple-element.39.scaled) | copy-start | bytes 3145732
  19.9 75.8 %copy-start.5 = (f32[256,128]{1,0:T(8,128)S(1)}, f32[256,128]{1,0:T(8,128)}, u32[]{:S(2)}) copy-start(f32[256,128]{1,0:T(8,128)} %get-tuple-element.40.inv_in) | copy-start | bytes 393220
  53.9 23.2 %collective-permute-start.6 = (bf16[8,512,128]{2,1,0:T(8,128)(2,1)S(1)}, bf16[8,512,128]{2,1,0:T(8,128)(2,1)S(1)}, u32[]{:S(2)}, u32[]{:S(2)}) collective-permute-start(bf16[8,512,128]{2,1,0:T(8,128)(2,1)S(1)} %all_to_all.5.own), channel_id=1, source_target_pairs={{0,4},{4,0},{8,12},{12,8},{16,20},{20,16},{24,28},{28,24},{32,36},... | collective-permute-start | bytes 3145736 | tf_op jit(solution)/shard_map/ppermute | solution.py:48
  53.9 29.1 %collective-permute-start.9 = (bf16[384,1024]{1,0:T(8,128)(2,1)S(1)}, bf16[384,1024]{1,0:T(8,128)(2,1)S(1)}, u32[]{:S(2)}, u32[]{:S(2)}) collective-permute-start(bf16[384,1024]{1,0:T(8,128)(2,1)S(1)} %fusion), channel_id=1, source_target_pairs={{0,2},{1,3},{2,0},{3,1},{4,6},{5,7},{6,4},{7,5},{8,10},{9,11},{10,... | collective-permute-start | bytes 2359304 | tf_op jit(solution)/shard_map/ppermute | solution.py:60
  55.7 35.4 %collective-permute-start.8 = (bf16[384,1024]{1,0:T(8,128)(2,1)S(1)}, bf16[384,1024]{1,0:T(8,128)(2,1)S(1)}, u32[]{:S(2)}, u32[]{:S(2)}) collective-permute-start(bf16[384,1024]{1,0:T(8,128)(2,1)S(1)} %fusion), channel_id=1, source_target_pairs={{0,3},{1,0},{2,1},{3,2},{4,7},{5,4},{6,5},{7,6},{8,11},{9,8},{10,9... | collective-permute-start | bytes 2359304 | tf_op jit(solution)/shard_map/ppermute | solution.py:60
  56.5 35.7 %collective-permute-start.7 = (bf16[384,1024]{1,0:T(8,128)(2,1)S(1)}, bf16[384,1024]{1,0:T(8,128)(2,1)S(1)}, u32[]{:S(2)}, u32[]{:S(2)}) collective-permute-start(bf16[384,1024]{1,0:T(8,128)(2,1)S(1)} %fusion), channel_id=1, source_target_pairs={{0,1},{1,2},{2,3},{3,0},{4,5},{5,6},{6,7},{7,4},{8,9},{9,10},{10,1... | collective-permute-start | bytes 2359304 | tf_op jit(solution)/shard_map/ppermute | solution.py:60
  57.7 46.9 %copy-start.6 = (bf16[31,128]{1,0:T(8,128)(2,1)S(1)}, bf16[31,128]{1,0:T(8,128)(2,1)}, u32[]{:S(2)}) copy-start(bf16[31,128]{1,0:T(8,128)(2,1)} %weight.1) | copy-start | bytes 23812
  57.7 62.1 %copy-start.4 = (bf16[256,256]{1,0:T(8,128)(2,1)S(1)}, bf16[256,256]{1,0:T(8,128)(2,1)}, u32[]{:S(2)}) copy-start(bf16[256,256]{1,0:T(8,128)(2,1)} %get-tuple-element.38.q0) | copy-start | bytes 393220
  57.7 6.8 %collective-permute-start.5 = (bf16[256,256]{1,0:T(8,128)(2,1)}, bf16[256,256]{1,0:T(8,128)(2,1)S(1)}, u32[]{:S(2)}, u32[]{:S(2)}) collective-permute-start(bf16[256,256]{1,0:T(8,128)(2,1)} %get-tuple-element.38.q0), channel_id=1, source_target_pairs={{0,16},{4,20},{8,24},{12,28},{16,0},{20,4},{24,8},{28,12},{32,48},... | collective-permute-start | bytes 393224 | tf_op jit(solution)/shard_map/ppermute | solution.py:48
  64.5 5.8 %collective-permute-start.4 = (bf16[256,256]{1,0:T(8,128)(2,1)}, bf16[256,256]{1,0:T(8,128)(2,1)S(1)}, u32[]{:S(2)}, u32[]{:S(2)}) collective-permute-start(bf16[256,256]{1,0:T(8,128)(2,1)} %get-tuple-element.38.q0), channel_id=1, source_target_pairs={{0,24},{4,28},{8,0},{12,4},{16,8},{20,12},{24,16},{28,20},{32,56},... | collective-permute-start | bytes 393224 | tf_op jit(solution)/shard_map/ppermute | solution.py:48
  70.3 6.7 %collective-permute-start.3 = (bf16[256,256]{1,0:T(8,128)(2,1)}, bf16[256,256]{1,0:T(8,128)(2,1)S(1)}, u32[]{:S(2)}, u32[]{:S(2)}) collective-permute-start(bf16[256,256]{1,0:T(8,128)(2,1)} %get-tuple-element.38.q0), channel_id=1, source_target_pairs={{0,8},{4,12},{8,16},{12,20},{16,24},{20,28},{24,0},{28,4},{32,40},... | collective-permute-start | bytes 393224 | tf_op jit(solution)/shard_map/ppermute | solution.py:48
  83.0 36.7 %copy-start.17 = (bf16[528,256]{1,0:T(8,128)(2,1)S(1)}, bf16[528,256]{1,0:T(8,128)(2,1)}, u32[]{:S(2)}) copy-start(bf16[528,256]{1,0:T(8,128)(2,1)} %get-tuple-element.35) | copy-start | bytes 811012
  83.0 36.7 %copy-start.16 = (bf16[528,256]{1,0:T(8,128)(2,1)S(1)}, bf16[528,256]{1,0:T(8,128)(2,1)}, u32[]{:S(2)}) copy-start(bf16[528,256]{1,0:T(8,128)(2,1)} %get-tuple-element.36) | copy-start | bytes 811012
  92.2 51.1 %collective-permute-start.20 = (bf16[384,1024]{1,0:T(8,128)(2,1)S(1)}, bf16[384,1024]{1,0:T(8,128)(2,1)S(1)}, u32[]{:S(2)}, u32[]{:S(2)}) collective-permute-start(bf16[384,1024]{1,0:T(8,128)(2,1)S(1)} %collective-permute-done.7.a1), channel_id=1, source_target_pairs={{0,4},{4,0},{8,12},{12,8},{16,20},{20,16},{24,28},{28,24},{32,36},... | collective-permute-start | bytes 2359304 | tf_op jit(solution)/shard_map/ppermute | solution.py:48
  92.2 51.1 %collective-permute-start.21 = (bf16[384,1024]{1,0:T(8,128)(2,1)S(1)}, bf16[384,1024]{1,0:T(8,128)(2,1)S(1)}, u32[]{:S(2)}, u32[]{:S(2)}) collective-permute-start(bf16[384,1024]{1,0:T(8,128)(2,1)S(1)} %collective-permute-done.8.a2), channel_id=1, source_target_pairs={{0,4},{4,0},{8,12},{12,8},{16,20},{20,16},{24,28},{28,24},{32,36},... | collective-permute-start | bytes 2359304 | tf_op jit(solution)/shard_map/ppermute | solution.py:48
  92.7 50.6 %collective-permute-start.22 = (bf16[384,1024]{1,0:T(8,128)(2,1)S(1)}, bf16[384,1024]{1,0:T(8,128)(2,1)S(1)}, u32[]{:S(2)}, u32[]{:S(2)}) collective-permute-start(bf16[384,1024]{1,0:T(8,128)(2,1)S(1)} %collective-permute-done.9.a3), channel_id=1, source_target_pairs={{0,4},{4,0},{8,12},{12,8},{16,20},{20,16},{24,28},{28,24},{32,36},... | collective-permute-start | bytes 2359304 | tf_op jit(solution)/shard_map/ppermute | solution.py:48
  92.7 27.0 %collective-permute-start.10 = (bf16[528,256]{1,0:T(8,128)(2,1)}, bf16[528,256]{1,0:T(8,128)(2,1)S(1)}, u32[]{:S(2)}, u32[]{:S(2)}) collective-permute-start(bf16[528,256]{1,0:T(8,128)(2,1)} %get-tuple-element.34), channel_id=1, source_target_pairs={{0,24},{4,28},{8,0},{12,4},{16,8},{20,12},{24,16},{28,20},{32,56},... | collective-permute-start | bytes 811016 | tf_op jit(solution)/shard_map/ppermute | solution.py:48
  95.7 34.5 %copy-start.8 = (f32[2]{0:T(128)S(1)}, f32[2]{0:T(128)}, u32[]{:S(2)}) copy-start(f32[2]{0:T(128)} %lam.1) | copy-start | bytes 28
  97.2 46.1 %copy-start = (bf16[256,2048]{1,0:T(8,128)(2,1)S(1)}, bf16[256,2048]{1,0:T(8,128)(2,1)}, u32[]{:S(2)}) copy-start(bf16[256,2048]{1,0:T(8,128)(2,1)} %w_attn.1) | copy-start | bytes 3145732
  97.2 46.1 %copy-start.1 = (bf16[128,2048]{1,0:T(8,128)(2,1)S(1)}, bf16[128,2048]{1,0:T(8,128)(2,1)}, u32[]{:S(2)}) copy-start(bf16[128,2048]{1,0:T(8,128)(2,1)} %w_conv.1) | copy-start | bytes 1572868
  97.2 7.4 %collective-permute-start.13 = (bf16[32,128]{1,0:T(8,128)(2,1)}, bf16[32,128]{1,0:T(8,128)(2,1)S(1)}, u32[]{:S(2)}, u32[]{:S(2)}) collective-permute-start(bf16[32,128]{1,0:T(8,128)(2,1)} %get-tuple-element.43), channel_id=1, source_target_pairs={{0,4},{4,8},{8,12},{12,16},{16,20},{20,24},{24,28},{28,32},{32,36}... | collective-permute-start | bytes 24584 | tf_op jit(solution)/shard_map/ppermute | solution.py:320
  105.6 5.3 %collective-permute-start.16 = (f32[1,256]{1,0:T(1,128)}, f32[1,256]{1,0:T(1,128)S(1)}, u32[]{:S(2)}, u32[]{:S(2)}) collective-permute-start(f32[1,256]{1,0:T(1,128)} %get-tuple-element.46), channel_id=1, source_target_pairs={{0,2},{1,3},{2,0},{3,1},{4,6},{5,7},{6,4},{7,5},{8,10},{9,11},{10,... | collective-permute-start | bytes 3080 | tf_op jit(solution)/shard_map/ppermute | solution.py:60
  110.9 3.8 %collective-permute-start.15 = (f32[1,256]{1,0:T(1,128)}, f32[1,256]{1,0:T(1,128)S(1)}, u32[]{:S(2)}, u32[]{:S(2)}) collective-permute-start(f32[1,256]{1,0:T(1,128)} %get-tuple-element.46), channel_id=1, source_target_pairs={{0,3},{1,0},{2,1},{3,2},{4,7},{5,4},{6,5},{7,6},{8,11},{9,8},{10,9... | collective-permute-start | bytes 3080 | tf_op jit(solution)/shard_map/ppermute | solution.py:60
  114.7 5.0 %collective-permute-start.14 = (f32[1,256]{1,0:T(1,128)}, f32[1,256]{1,0:T(1,128)S(1)}, u32[]{:S(2)}, u32[]{:S(2)}) collective-permute-start(f32[1,256]{1,0:T(1,128)} %get-tuple-element.46), channel_id=1, source_target_pairs={{0,1},{1,2},{2,3},{3,0},{4,5},{5,6},{6,7},{7,4},{8,9},{9,10},{10,1... | collective-permute-start | bytes 3080 | tf_op jit(solution)/shard_map/ppermute | solution.py:60
  119.7 10.6 %collective-permute-start.11 = (bf16[528,256]{1,0:T(8,128)(2,1)S(1)}, bf16[528,256]{1,0:T(8,128)(2,1)S(1)}, u32[]{:S(2)}, u32[]{:S(2)}) collective-permute-start(bf16[528,256]{1,0:T(8,128)(2,1)S(1)} %copy-done.17), channel_id=1, source_target_pairs={{0,8},{4,12},{8,16},{12,20},{16,24},{20,28},{24,0},{28,4},{32,40},... | collective-permute-start | bytes 811016 | tf_op jit(solution)/shard_map/ppermute | solution.py:48
  119.7 10.6 %collective-permute-start.12 = (bf16[528,256]{1,0:T(8,128)(2,1)S(1)}, bf16[528,256]{1,0:T(8,128)(2,1)S(1)}, u32[]{:S(2)}, u32[]{:S(2)}) collective-permute-start(bf16[528,256]{1,0:T(8,128)(2,1)S(1)} %copy-done.16), channel_id=1, source_target_pairs={{0,16},{4,20},{8,24},{12,28},{16,0},{20,4},{24,8},{28,12},{32,48},... | collective-permute-start | bytes 811016 | tf_op jit(solution)/shard_map/ppermute | solution.py:48
  132.0 5.5 %collective-permute-start.17 = (bf16[64,384]{1,0:T(8,128)(2,1)}, bf16[64,384]{1,0:T(8,128)(2,1)S(1)}, u32[]{:S(2)}, u32[]{:S(2)}) collective-permute-start(bf16[64,384]{1,0:T(8,128)(2,1)} %get-tuple-element.49), channel_id=1, source_target_pairs={{0,1},{1,2},{2,3},{3,0},{4,5},{5,6},{6,7},{7,4},{8,9},{9,10},{10,1... | collective-permute-start | bytes 147464 | tf_op jit(solution)/shard_map/ppermute | solution.py:60
  132.0 5.5 %collective-permute-start.18 = (bf16[64,384]{1,0:T(8,128)(2,1)}, bf16[64,384]{1,0:T(8,128)(2,1)S(1)}, u32[]{:S(2)}, u32[]{:S(2)}) collective-permute-start(bf16[64,384]{1,0:T(8,128)(2,1)} %get-tuple-element.50), channel_id=1, source_target_pairs={{0,3},{1,0},{2,1},{3,2},{4,7},{5,4},{6,5},{7,6},{8,11},{9,8},{10,9... | collective-permute-start | bytes 147464 | tf_op jit(solution)/shard_map/ppermute | solution.py:60
  137.5 5.8 %collective-permute-start.19 = (bf16[64,384]{1,0:T(8,128)(2,1)}, bf16[64,384]{1,0:T(8,128)(2,1)S(1)}, u32[]{:S(2)}, u32[]{:S(2)}) collective-permute-start(bf16[64,384]{1,0:T(8,128)(2,1)} %get-tuple-element.51), channel_id=1, source_target_pairs={{0,2},{1,3},{2,0},{3,1},{4,6},{5,7},{6,4},{7,5},{8,10},{9,11},{10,... | collective-permute-start | bytes 147464 | tf_op jit(solution)/shard_map/ppermute | solution.py:60
  (9 other events, 103.6 us)

commit v6 on v5

--- a/solution.py
+++ b/solution.py
@@ -64,7 +64,7 @@
     return jnp.dot(a, b, preferred_element_type=F32)
 
 
-def project_kernel(t0, t1, t2, t3, gain, weights, qt, kv, scaled, inv_out):
+def project_kernel(t0, t1, t2, t3, gain, weights, qt, kv, alone, scaled, inv_out):
     x = lax.axis_index("tp")
     squares = jnp.zeros((ROWS, 128), F32)
     for ref, by in zip((t0, t1, t2, t3), (0,) + SHIFTS):
@@ -79,10 +79,10 @@
     both = dot(rows, weights[:, 256:512]) * inv
     k = both[:, 0:128].astype(BF16)
     vt = jnp.transpose(both[:, 128:256]).astype(BF16)
-    for z in range(8):
-        kv[z, 0:256, :] = k
-        kv[z, 256:384, :] = vt[:, 0:128]
-        kv[z, 384:512, :] = vt[:, 128:256]
+    for ref, z in [(kv, z) for z in range(8)] + [(alone, 0)]:
+        ref[z, 0:256, :] = k
+        ref[z, 256:384, :] = vt[:, 0:128]
+        ref[z, 384:512, :] = vt[:, 128:256]
     q = dot(rows, weights[:, 0:256]) * inv
     qt[...] = jnp.transpose(q * (QK ** -0.5)).astype(BF16)
 
@@ -190,31 +190,38 @@
     acc[...] = jnp.zeros(acc.shape, F32)
 
 
-def remote_kernel(q0, q1, q2, own, other, o0, o1, o2, queries, maxima, acc):
-    z, y, _ = position()
-    lay_queries((q0, q1, q2), queries)
-    start_state(maxima, acc)
-
-    attend_before(z, range(12), own, other, queries, maxima, acc)
-    for b, by in enumerate(SHIFTS):
-
-        @pl.when(lax.rem(y - by + 4, 4) > y)
-        def _(b=b):
-            attend(range(4 * b, 4 * b + 4), own, other, (z,), queries, maxima, acc)
-
-    for b, out in enumerate((o0, o1, o2)):
-        write_part(out, 4 * b, maxima, acc)
-
-
-def self_kernel(q0, own, other, out, queries, maxima, acc):
-    z, _, c = position()
-    lay_queries((q0,), queries)
-    start_state(maxima, acc)
+def near_kernel(q0, q1, q2, q3, own, other, far_max, far_acc, self_max, self_acc, far_queries, self_queries):
+    _, y, c = position()
+    lay_queries((q0, q1, q2), far_queries)
+    lay_queries((q3,), self_queries)
+    start_state(far_max, far_acc)
+    start_state(self_max, self_acc)
     row = lax.broadcasted_iota(jnp.int32, (512, ROWS), 0)
     key_row = jnp.where(row < ROWS, row + c * ROWS, row - c * ROWS)
     query_row = lax.broadcasted_iota(jnp.int32, (512, ROWS), 1) + c * ROWS
-    attend(range(4), own, other, (z,), queries, maxima, acc, key_row <= query_row)
-
+    attend(range(4), own, other, (0,), self_queries, self_max, self_acc, key_row <= query_row)
+    for b, by in enumerate(SHIFTS):
+
+        @pl.when(lax.rem(y - by + 4, 4) > y)
+        def _(b=b):
+            attend(range(4 * b, 4 * b + 4), own, other, (0,), far_queries, far_max, far_acc)
+
+
+def remote_kernel(q0, q1, q2, own, other, max_in, acc_in, o0, o1, o2, queries, maxima, acc):
+    z, _, _ = position()
+    lay_queries((q0, q1, q2), queries)
+    maxima[...] = max_in[...]
+    acc[...] = acc_in[...]
+    attend_before(z, range(12), own, other, queries, maxima, acc)
+    for b, out in enumerate((o0, o1, o2)):
+        write_part(out, 4 * b, maxima, acc)
+
+
+def self_kernel(q0, own, other, max_in, acc_in, out, queries, maxima, acc):
+    z, _, _ = position()
+    lay_queries((q0,), queries)
+    maxima[...] = max_in[...]
+    acc[...] = acc_in[...]
     attend_before(z, range(4), own, other, queries, maxima, acc)
     write_part(out, 0, maxima, acc)
 
@@ -295,11 +302,11 @@
     first = jnp.concatenate([w_query, w_key, w_value], axis=1)
     second = jnp.concatenate([w_glu_value, w_glu_gate, w_gate_attn, w_gate_conv], axis=1)
     gain, first, second, half = lax.optimization_barrier((gain, first, second, half))
-    qt, kv, scaled, inv = pl.pallas_call(
+    qt, kv, alone, scaled, inv = pl.pallas_call(
         project_kernel,
-        out_shape=[sent((256, ROWS)), sent((8, 512, 128)), sent((4, ROWS, 512)), sent((ROWS, 128), F32)],
+        out_shape=[sent((256, ROWS)), sent((8, 512, 128)), sent((1, 512, 128)), sent((4, ROWS, 512)), sent((ROWS, 128), F32)],
         in_specs=[VM] * 6,
-        out_specs=[OUT] * 4,
+        out_specs=[OUT] * 5,
         compiler_params=SMALL,
         name="project",
     )(*pieces, gain, first)
@@ -338,27 +345,37 @@
             pltpu.VMEM((tiles, ACC, ROWS), F32),
         ]
 
+    far_max, far_acc, self_max, self_acc = pl.pallas_call(
+        near_kernel,
+        out_shape=[shape((n, r, ROWS), F32) for n in (12, 4) for r in (1, ACC)],
+        in_specs=[VM] * 6,
+        out_specs=[VM] * 4,
+        scratch_shapes=[pltpu.VMEM((12, 256, ROWS), BF16), pltpu.VMEM((4, 256, ROWS), BF16)],
+        compiler_params=BIG,
+        name="near",
+    )(*q_blocks, qt, alone, core_swap(alone))
+
     parts = pl.pallas_call(
         remote_kernel,
         out_shape=[sent((MSG, ROWS))] * 3,
-        in_specs=[VM] * 5,
+        in_specs=[VM] * 7,
         out_specs=[OUT] * 3,
         scratch_shapes=scratch(12),
         compiler_params=BIG,
         name="remote",
-    )(*q_blocks, gathered, swapped)
+    )(*q_blocks, gathered, swapped, far_max, far_acc)
     back = [y_shift(part, -by) for part, by in zip(parts, SHIFTS)]
     parts, qt, weights = lax.optimization_barrier((parts, qt, weights))
     weights_s = [core_swap(w) for w in weights]
     part = pl.pallas_call(
         self_kernel,
         out_shape=shape((MSG, ROWS)),
-        in_specs=[VM] * 3,
+        in_specs=[VM] * 5,
         out_specs=VM,
         scratch_shapes=scratch(4),
         compiler_params=BIG,
         name="self",
-    )(qt, gathered, swapped)
+    )(qt, gathered, swapped, self_max, self_acc)
 
     rows = pl.pallas_call(
         merge_kernel,

time: 146 us -> 145 us (level)
  waiting for transfers between devices: 62.3 us -> 60 us
  local copies, waits for them, and re-layouts: 0.99 us -> 2.79 us
    ppermute x12, waiting for transfers between devices: 36.5 us -> 31.4 us  [tp_shift(): return lax.ppermute(x, 'tp', [(i, (i + by) % 4) for i in range(4)])]
    pallas_call x0 -> x1, Pallas kernels: none -> 4 us  [local(): pl.pallas_call(near_kernel, out_shape=[shape((n, r, ROWS), F32) for n in...]
    ppermute x10 -> x11, waiting for transfers between devices: 20.6 us -> 23.5 us  [along_sp(): return lax.ppermute(x, 'sp', pairs)]
    pallas_call x1, Pallas kernels: 5.93 us -> 3.16 us  [local(): pl.pallas_call(remote_kernel, out_shape=[sent((MSG, ROWS))] * 3, in_specs...]
    unnamed x36 -> x40, local copies, waits for them, and re-layouts: 0.29 us -> 2.1 us
    ppermute x10 -> x11, starting transfers between devices: 10.7 us -> 11 us  [along_sp(): return lax.ppermute(x, 'sp', pairs)]
  transfers between devices with their start and end apart: 23 -> 24, of which waited for: 14 -> 15; matrix products, arithmetic and copies ran while one was open for 2% -> 2% of each run, Pallas kernels for 8% -> 8%
where the time goes in v6:
time: 145 us
  waiting for transfers between devices  60 us (41%)
  blocking collectives  33.9 us (23%)
  starting transfers between devices  29 us (20%)
  Pallas kernels  16.3 us (11%)
  local copies, waits for them, and re-layouts  2.79 us (2%)
  other arithmetic  2.76 us (2%)
    all_to_all x1, blocking collectives, local(): lax.all_to_all(kv, 'sp', 0, 0, tiled=True, axis_index_groups=groups)  33.9 us
    ppermute x12, waiting for transfers between devices, tp_shift(): return lax.ppermute(x, 'tp', [(i, (i + by) % 4) for i in range(4)])  31.4 us
    ppermute x11, waiting for transfers between devices, along_sp(): return lax.ppermute(x, 'sp', pairs)  23.5 us
    ppermute x12, starting transfers between devices, tp_shift(): return lax.ppermute(x, 'tp', [(i, (i + by) % 4) for i in range(4)])  15.8 us
    ppermute x11, starting transfers between devices, along_sp(): return lax.ppermute(x, 'sp', pairs)  11 us
    ppermute x1, waiting for transfers between devices, local(): before = lax.ppermute(tail, 'sp', [(i, i + 1) for i in range(63)])  5.16 us
    pallas_call x1, Pallas kernels, local(): pl.pallas_call(near_kernel, out_shape=[shape((n, r, ROWS), F32) for n in...  4 us
    pallas_call x1, Pallas kernels, local(): pl.pallas_call(remote_kernel, out_shape=[sent((MSG, ROWS))] * 3, in_specs...  3.16 us
  transfers between devices with their start and end apart: 24, of which 15 were waited for; matrix products, arithmetic and copies ran while one was open for 2% of the time, Pallas kernels for 8%

profile of v6, /device:TPU:32, one launch (start us, length us, event | category | flops | bytes accessed | tf_op | source)
XLA Modules:
  0.0 145.1 jit_solution(3188530571305808750)
XLA Ops:
  0.0 2.8 %collective-permute-start.1 = (bf16[256,512]{1,0:T(8,128)(2,1)}, bf16[256,512]{1,0:T(8,128)(2,1)S(1)}, u32[]{:S(2)}, u32[]{:S(2)}) collective-permute-start(bf16[256,512]{1,0:T(8,128)(2,1)} %t0.1), channel_id=1, source_target_pairs={{0,3},{1,0},{2,1},{3,2},{4,7},{5,4},{6,5},{7,6},{8,11},{9,8},{10,9... | collective-permute-start | bytes 786440 | tf_op jit(solution)/shard_map/ppermute | solution.py:60
  2.8 2.3 %collective-permute-start.2 = (bf16[256,512]{1,0:T(8,128)(2,1)}, bf16[256,512]{1,0:T(8,128)(2,1)S(1)}, u32[]{:S(2)}, u32[]{:S(2)}) collective-permute-start(bf16[256,512]{1,0:T(8,128)(2,1)} %t0.1), channel_id=1, source_target_pairs={{0,2},{1,3},{2,0},{3,1},{4,6},{5,7},{6,4},{7,5},{8,10},{9,11},{10,... | collective-permute-start | bytes 786440 | tf_op jit(solution)/shard_map/ppermute | solution.py:60
  7.1 1.4 pad_maximum_fusion.weights
  8.9 5.5 %collective-permute-done.1.t2 = bf16[256,512]{1,0:T(8,128)(2,1)S(1)} collective-permute-done((bf16[256,512]{1,0:T(8,128)(2,1)}, bf16[256,512]{1,0:T(8,128)(2,1)S(1)}, u32[]{:S(2)}, u32[]{:S(2)}) %collective-permute-start.1) | collective-permute-done | bytes 262176 | tf_op jit(solution)/shard_map/ppermute | solution.py:60
  14.4 3.3 %collective-permute-done.t1 = bf16[256,512]{1,0:T(8,128)(2,1)S(1)} collective-permute-done((bf16[256,512]{1,0:T(8,128)(2,1)}, bf16[256,512]{1,0:T(8,128)(2,1)S(1)}, u32[]{:S(2)}, u32[]{:S(2)}) %collective-permute-start) | collective-permute-done | bytes 262176 | tf_op jit(solution)/shard_map/ppermute | solution.py:60
  17.7 2.0 %project.1 = (bf16[256,256]{1,0:T(8,128)(2,1)}, bf16[8,512,128]{2,1,0:T(8,128)(2,1)}, bf16[1,512,128]{2,1,0:T(8,128)(2,1)}, bf16[4,256,512]{2,1,0:T(8,128)(2,1)}, f32[256,128]{1,0:T(8,128)}) custom-call(bf16[256,512]{1,0:T(8,128)(2,1)S(1)} %copy-done.5, bf16[256,512]{1,0:T(8,128)(2,1)S(1)} %collective-permute-done.t1, ...), custom_call_target="tpu_custom_call" | custom-call | tf_op jit(solution)/shard_map/project/pallas_call | solution.py:305
  19.7 33.9 %all_to_all.5.own = bf16[8,512,128]{2,1,0:T(8,128)(2,1)S(1)} all-to-all(bf16[8,512,128]{2,1,0:T(8,128)(2,1)} %get-tuple-element.38), channel_id=1, replica_groups={{0,32,64,96,128,160,192,224},{4,36,68,100,132,164,196,228},{8,40,72,104..., dimensions={0} | all-to-all | bytes 2097152 | tf_op jit(solution)/shard_map/all_to_all | solution.py:315
  53.6 1.8 %collective-permute-start.10 = (bf16[384,1024]{1,0:T(8,128)(2,1)S(1)}, bf16[384,1024]{1,0:T(8,128)(2,1)S(1)}, u32[]{:S(2)}, u32[]{:S(2)}) collective-permute-start(bf16[384,1024]{1,0:T(8,128)(2,1)S(1)} %fusion), channel_id=1, source_target_pairs={{0,2},{1,3},{2,0},{3,1},{4,6},{5,7},{6,4},{7,5},{8,10},{9,11},{10,... | collective-permute-start | bytes 2359304 | tf_op jit(solution)/shard_map/ppermute | solution.py:60
  57.5 1.6 %collective-permute-done.7.other = bf16[1,512,128]{2,1,0:T(8,128)(2,1)S(1)} collective-permute-done((bf16[1,512,128]{2,1,0:T(8,128)(2,1)}, bf16[1,512,128]{2,1,0:T(8,128)(2,1)S(1)}, u32[]{:S(2)}, u32[]{:S(2)}) %collective-permute-start.7) | collective-permute-done | bytes 131104 | tf_op jit(solution)/shard_map/ppermute | solution.py:48
  59.0 3.2 %collective-permute-start.5 = (bf16[256,256]{1,0:T(8,128)(2,1)}, bf16[256,256]{1,0:T(8,128)(2,1)S(1)}, u32[]{:S(2)}, u32[]{:S(2)}) collective-permute-start(bf16[256,256]{1,0:T(8,128)(2,1)} %get-tuple-element.46.q3.q0), channel_id=1, source_target_pairs={{0,16},{4,20},{8,24},{12,28},{16,0},{20,4},{24,8},{28,12},{32,48},... | collective-permute-start | bytes 393224 | tf_op jit(solution)/shard_map/ppermute | solution.py:48
  62.2 4.1 %collective-permute-done.5.q2 = bf16[256,256]{1,0:T(8,128)(2,1)S(1)} collective-permute-done((bf16[256,256]{1,0:T(8,128)(2,1)}, bf16[256,256]{1,0:T(8,128)(2,1)S(1)}, u32[]{:S(2)}, u32[]{:S(2)}) %collective-permute-start.5) | collective-permute-done | bytes 131104 | tf_op jit(solution)/shard_map/ppermute | solution.py:48
  66.3 3.0 %collective-permute-start.4 = (bf16[256,256]{1,0:T(8,128)(2,1)}, bf16[256,256]{1,0:T(8,128)(2,1)S(1)}, u32[]{:S(2)}, u32[]{:S(2)}) collective-permute-start(bf16[256,256]{1,0:T(8,128)(2,1)} %get-tuple-element.46.q3.q0), channel_id=1, source_target_pairs={{0,24},{4,28},{8,0},{12,4},{16,8},{20,12},{24,16},{28,20},{32,56},... | collective-permute-start | bytes 393224 | tf_op jit(solution)/shard_map/ppermute | solution.py:48
  69.3 2.8 %collective-permute-done.4.q1 = bf16[256,256]{1,0:T(8,128)(2,1)S(1)} collective-permute-done((bf16[256,256]{1,0:T(8,128)(2,1)}, bf16[256,256]{1,0:T(8,128)(2,1)S(1)}, u32[]{:S(2)}, u32[]{:S(2)}) %collective-permute-start.4) | collective-permute-done | bytes 131104 | tf_op jit(solution)/shard_map/ppermute | solution.py:48
  73.0 5.8 %collective-permute-done.3.q0 = bf16[256,256]{1,0:T(8,128)(2,1)S(1)} collective-permute-done((bf16[256,256]{1,0:T(8,128)(2,1)}, bf16[256,256]{1,0:T(8,128)(2,1)S(1)}, u32[]{:S(2)}, u32[]{:S(2)}) %collective-permute-start.3) | collective-permute-done | bytes 131104 | tf_op jit(solution)/shard_map/ppermute | solution.py:48
  80.7 4.0 %near.1 = (f32[12,1,256]{2,1,0:T(1,128)S(1)}, f32[12,144,256]{2,1,0:T(8,128)S(1)}, f32[4,1,256]{2,1,0:T(1,128)S(1)}, f32[4,144,256]{2,1,0:T(8,128)S(1)}) custom-call(bf16[256,256]{1,0:T(8,128)(2,1)S(1)} %collective-permute-done.3.q0, bf16[256,256]{1,0:T(8,128)(2,1)S(1)} %collective-permute-done.4.q1, bf16[256,256]{1,0:T(8,128)(2,1)S(1)} %collective-permute-done.5.q2, ...), custom_call_target="tpu_custom_call" | custom-call | tf_op jit(solution)/shard_map/near/pallas_call | solution.py:348
  84.7 3.2 %remote.1 = (bf16[528,256]{1,0:T(8,128)(2,1)}, bf16[528,256]{1,0:T(8,128)(2,1)}, bf16[528,256]{1,0:T(8,128)(2,1)}) custom-call(bf16[256,256]{1,0:T(8,128)(2,1)S(1)} %collective-permute-done.3.q0, bf16[256,256]{1,0:T(8,128)(2,1)S(1)} %collective-permute-done.4.q1, bf16[256,256]{1,0:T(8,128)(2,1)S(1)} %collective-permute-done.5.q2, ...), custom_call_target="tpu_custom_call" | custom-call | tf_op jit(solution)/shard_map/remote/pallas_call | solution.py:358
  87.8 2.9 %collective-permute-done.9.a2 = bf16[384,1024]{1,0:T(8,128)(2,1)S(1)} collective-permute-done((bf16[384,1024]{1,0:T(8,128)(2,1)S(1)}, bf16[384,1024]{1,0:T(8,128)(2,1)S(1)}, u32[]{:S(2)}, u32[]{:S(2)}) %collective-permute-start.9) | collective-permute-done | bytes 786464 | tf_op jit(solution)/shard_map/ppermute | solution.py:60
  92.5 3.0 %collective-permute-start.11 = (bf16[528,256]{1,0:T(8,128)(2,1)}, bf16[528,256]{1,0:T(8,128)(2,1)S(1)}, u32[]{:S(2)}, u32[]{:S(2)}) collective-permute-start(bf16[528,256]{1,0:T(8,128)(2,1)} %get-tuple-element.42), channel_id=1, source_target_pairs={{0,24},{4,28},{8,0},{12,4},{16,8},{20,12},{24,16},{28,20},{32,56},... | collective-permute-start | bytes 811016 | tf_op jit(solution)/shard_map/ppermute | solution.py:48
  95.5 1.5 %rest.1 = (bf16[256,128]{1,0:T(8,128)(2,1)S(1)}, bf16[32,128]{1,0:T(8,128)(2,1)}, bf16[256,384]{1,0:T(8,128)(2,1)S(1)}) custom-call(bf16[4,256,512]{2,1,0:T(8,128)(2,1)S(1)} %copy-done.2, f32[256,128]{1,0:T(8,128)S(1)} %copy-done.7, bf16[2048,640]{1,0:T(8,128)(2,1)S(1)} %pad_maximum_fusion.weights), custom_call_target="tpu_custom_call" | custom-call | tf_op jit(solution)/shard_map/rest/pallas_call | solution.py:319
  97.0 2.2 %collective-permute-start.14 = (bf16[32,128]{1,0:T(8,128)(2,1)}, bf16[32,128]{1,0:T(8,128)(2,1)S(1)}, u32[]{:S(2)}, u32[]{:S(2)}) collective-permute-start(bf16[32,128]{1,0:T(8,128)(2,1)} %get-tuple-element.53), channel_id=1, source_target_pairs={{0,4},{4,8},{8,12},{12,16},{16,20},{20,24},{24,28},{28,32},{32,36}... | collective-permute-start | bytes 24584 | tf_op jit(solution)/shard_map/ppermute | solution.py:327
  99.2 5.2 %collective-permute-done.14.before = bf16[32,128]{1,0:T(8,128)(2,1)S(1)} collective-permute-done((bf16[32,128]{1,0:T(8,128)(2,1)}, bf16[32,128]{1,0:T(8,128)(2,1)S(1)}, u32[]{:S(2)}, u32[]{:S(2)}) %collective-permute-start.14) | collective-permute-done | bytes 8224 | tf_op jit(solution)/shard_map/ppermute | solution.py:327
  105.4 1.8 %collective-permute-start.17 = (f32[1,256]{1,0:T(1,128)}, f32[1,256]{1,0:T(1,128)S(1)}, u32[]{:S(2)}, u32[]{:S(2)}) collective-permute-start(f32[1,256]{1,0:T(1,128)} %get-tuple-element.56), channel_id=1, source_target_pairs={{0,2},{1,3},{2,0},{3,1},{4,6},{5,7},{6,4},{7,5},{8,10},{9,11},{10,... | collective-permute-start | bytes 3080 | tf_op jit(solution)/shard_map/ppermute | solution.py:60
  107.2 3.5 %collective-permute-done.17.s3 = f32[1,256]{1,0:T(1,128)S(1)} collective-permute-done((f32[1,256]{1,0:T(1,128)}, f32[1,256]{1,0:T(1,128)S(1)}, u32[]{:S(2)}, u32[]{:S(2)}) %collective-permute-start.17) | collective-permute-done | bytes 1056 | tf_op jit(solution)/shard_map/ppermute | solution.py:60
  110.6 1.5 %collective-permute-start.16 = (f32[1,256]{1,0:T(1,128)}, f32[1,256]{1,0:T(1,128)S(1)}, u32[]{:S(2)}, u32[]{:S(2)}) collective-permute-start(f32[1,256]{1,0:T(1,128)} %get-tuple-element.56), channel_id=1, source_target_pairs={{0,3},{1,0},{2,1},{3,2},{4,7},{5,4},{6,5},{7,6},{8,11},{9,8},{10,9... | collective-permute-start | bytes 3080 | tf_op jit(solution)/shard_map/ppermute | solution.py:60
  112.2 2.3 %collective-permute-done.16.s2 = f32[1,256]{1,0:T(1,128)S(1)} collective-permute-done((f32[1,256]{1,0:T(1,128)}, f32[1,256]{1,0:T(1,128)S(1)}, u32[]{:S(2)}, u32[]{:S(2)}) %collective-permute-start.16) | collective-permute-done | bytes 1056 | tf_op jit(solution)/shard_map/ppermute | solution.py:60
  114.8 4.7 %collective-permute-done.15.s1 = f32[1,256]{1,0:T(1,128)S(1)} collective-permute-done((f32[1,256]{1,0:T(1,128)}, f32[1,256]{1,0:T(1,128)S(1)}, u32[]{:S(2)}, u32[]{:S(2)}) %collective-permute-start.15) | collective-permute-done | bytes 1056 | tf_op jit(solution)/shard_map/ppermute | solution.py:60
  120.8 9.2 %collective-permute-done.12.m2 = bf16[528,256]{1,0:T(8,128)(2,1)S(1)} collective-permute-done((bf16[528,256]{1,0:T(8,128)(2,1)S(1)}, bf16[528,256]{1,0:T(8,128)(2,1)S(1)}, u32[]{:S(2)}, u32[]{:S(2)}) %collective-permute-start.12) | collective-permute-done | bytes 270368 | tf_op jit(solution)/shard_map/ppermute | solution.py:48
  130.0 1.7 %merge.1 = (bf16[64,384]{1,0:T(8,128)(2,1)S(1)}, bf16[64,384]{1,0:T(8,128)(2,1)}, bf16[64,384]{1,0:T(8,128)(2,1)}, bf16[64,384]{1,0:T(8,128)(2,1)}) custom-call(bf16[528,256]{1,0:T(8,128)(2,1)S(1)} %self.1.m0, bf16[528,256]{1,0:T(8,128)(2,1)S(1)} %collective-permute-done.11.m1, bf16[528,256]{1,0:T(8,128)(2,1)S(1)} %collective-permute-done.12.m2, ...), custom_call_target="tpu_custom_call" | custom-call | tf_op jit(solution)/shard_map/merge/pallas_call | solution.py:380
  131.8 3.2 %collective-permute-start.19 = (bf16[64,384]{1,0:T(8,128)(2,1)}, bf16[64,384]{1,0:T(8,128)(2,1)S(1)}, u32[]{:S(2)}, u32[]{:S(2)}) collective-permute-start(bf16[64,384]{1,0:T(8,128)(2,1)} %get-tuple-element.60), channel_id=1, source_target_pairs={{0,3},{1,0},{2,1},{3,2},{4,7},{5,4},{6,5},{7,6},{8,11},{9,8},{10,9... | collective-permute-start | bytes 147464 | tf_op jit(solution)/shard_map/ppermute | solution.py:60
  135.0 2.3 %collective-permute-done.18.y1 = bf16[64,384]{1,0:T(8,128)(2,1)S(1)} collective-permute-done((bf16[64,384]{1,0:T(8,128)(2,1)}, bf16[64,384]{1,0:T(8,128)(2,1)S(1)}, u32[]{:S(2)}, u32[]{:S(2)}) %collective-permute-start.18) | collective-permute-done | bytes 49184 | tf_op jit(solution)/shard_map/ppermute | solution.py:60
  137.3 5.8 %collective-permute-done.20.y3 = bf16[64,384]{1,0:T(8,128)(2,1)S(1)} collective-permute-done((bf16[64,384]{1,0:T(8,128)(2,1)}, bf16[64,384]{1,0:T(8,128)(2,1)S(1)}, u32[]{:S(2)}, u32[]{:S(2)}) %collective-permute-start.20) | collective-permute-done | bytes 49184 | tf_op jit(solution)/shard_map/ppermute | solution.py:60
  143.1 2.0 %output.1 = bf16[64,2048]{1,0:T(8,128)(2,1)} custom-call(bf16[64,384]{1,0:T(8,128)(2,1)S(1)} %get-tuple-element.58.y0, bf16[64,384]{1,0:T(8,128)(2,1)S(1)} %collective-permute-done.18.y1, bf16[64,384]{1,0:T(8,128)(2,1)S(1)} %collective-permute-done.19.y2, bf16[64,384]{1,0:T(8,128)(2,1)S(1)} %collective-permute-done.20.y3, bf16[128,2048]{1,0:T(8,128)(2,1)S(1)} %copy-done.1, ...), custom_call_target="tpu_custom_call" | custom-call | tf_op jit(solution)/shard_map/output/pallas_call | solution.py:390
  (69 shorter events, 11.4 us)
Async XLA Ops:
  0.0 14.4 %collective-permute-start.1 = (bf16[256,512]{1,0:T(8,128)(2,1)}, bf16[256,512]{1,0:T(8,128)(2,1)S(1)}, u32[]{:S(2)}, u32[]{:S(2)}) collective-permute-start(bf16[256,512]{1,0:T(8,128)(2,1)} %t0.1), channel_id=1, source_target_pairs={{0,3},{1,0},{2,1},{3,2},{4,7},{5,4},{6,5},{7,6},{8,11},{9,8},{10,9... | collective-permute-start | bytes 786440 | tf_op jit(solution)/shard_map/ppermute | solution.py:60
  2.8 14.8 %collective-permute-start = (bf16[256,512]{1,0:T(8,128)(2,1)}, bf16[256,512]{1,0:T(8,128)(2,1)S(1)}, u32[]{:S(2)}, u32[]{:S(2)}) collective-permute-start(bf16[256,512]{1,0:T(8,128)(2,1)} %t0.1), channel_id=1, source_target_pairs={{0,1},{1,2},{2,3},{3,0},{4,5},{5,6},{6,7},{7,4},{8,9},{9,10},{10,1... | collective-permute-start | bytes 786440 | tf_op jit(solution)/shard_map/ppermute | solution.py:60
  2.8 14.8 %collective-permute-start.2 = (bf16[256,512]{1,0:T(8,128)(2,1)}, bf16[256,512]{1,0:T(8,128)(2,1)S(1)}, u32[]{:S(2)}, u32[]{:S(2)}) collective-permute-start(bf16[256,512]{1,0:T(8,128)(2,1)} %t0.1), channel_id=1, source_target_pairs={{0,2},{1,3},{2,0},{3,1},{4,6},{5,7},{6,4},{7,5},{8,10},{9,11},{10,... | collective-permute-start | bytes 786440 | tf_op jit(solution)/shard_map/ppermute | solution.py:60
  19.7 75.8 %copy-start.7 = (f32[256,128]{1,0:T(8,128)S(1)}, f32[256,128]{1,0:T(8,128)}, u32[]{:S(2)}) copy-start(f32[256,128]{1,0:T(8,128)} %get-tuple-element.50.inv_in) | copy-start | bytes 393220
  53.6 41.9 %copy-start.2 = (bf16[4,256,512]{2,1,0:T(8,128)(2,1)S(1)}, bf16[4,256,512]{2,1,0:T(8,128)(2,1)}, u32[]{:S(2)}) copy-start(bf16[4,256,512]{2,1,0:T(8,128)(2,1)} %get-tuple-element.49.scaled) | copy-start | bytes 3145732
  53.6 31.0 %collective-permute-start.6 = (bf16[8,512,128]{2,1,0:T(8,128)(2,1)S(1)}, bf16[8,512,128]{2,1,0:T(8,128)(2,1)S(1)}, u32[]{:S(2)}, u32[]{:S(2)}) collective-permute-start(bf16[8,512,128]{2,1,0:T(8,128)(2,1)S(1)} %all_to_all.5.own), channel_id=1, source_target_pairs={{0,4},{4,0},{8,12},{12,8},{16,20},{20,16},{24,28},{28,24},{32,36},... | collective-permute-start | bytes 3145736 | tf_op jit(solution)/shard_map/ppermute | solution.py:48
  53.6 34.2 %collective-permute-start.10 = (bf16[384,1024]{1,0:T(8,128)(2,1)S(1)}, bf16[384,1024]{1,0:T(8,128)(2,1)S(1)}, u32[]{:S(2)}, u32[]{:S(2)}) collective-permute-start(bf16[384,1024]{1,0:T(8,128)(2,1)S(1)} %fusion), channel_id=1, source_target_pairs={{0,2},{1,3},{2,0},{3,1},{4,6},{5,7},{6,4},{7,5},{8,10},{9,11},{10,... | collective-permute-start | bytes 2359304 | tf_op jit(solution)/shard_map/ppermute | solution.py:60
  55.4 35.4 %collective-permute-start.9 = (bf16[384,1024]{1,0:T(8,128)(2,1)S(1)}, bf16[384,1024]{1,0:T(8,128)(2,1)S(1)}, u32[]{:S(2)}, u32[]{:S(2)}) collective-permute-start(bf16[384,1024]{1,0:T(8,128)(2,1)S(1)} %fusion), channel_id=1, source_target_pairs={{0,3},{1,0},{2,1},{3,2},{4,7},{5,4},{6,5},{7,6},{8,11},{9,8},{10,9... | collective-permute-start | bytes 2359304 | tf_op jit(solution)/shard_map/ppermute | solution.py:60
  56.2 35.7 %collective-permute-start.8 = (bf16[384,1024]{1,0:T(8,128)(2,1)S(1)}, bf16[384,1024]{1,0:T(8,128)(2,1)S(1)}, u32[]{:S(2)}, u32[]{:S(2)}) collective-permute-start(bf16[384,1024]{1,0:T(8,128)(2,1)S(1)} %fusion), channel_id=1, source_target_pairs={{0,1},{1,2},{2,3},{3,0},{4,5},{5,6},{6,7},{7,4},{8,9},{9,10},{10,1... | collective-permute-start | bytes 2359304 | tf_op jit(solution)/shard_map/ppermute | solution.py:60
  57.5 1.6 %collective-permute-start.7 = (bf16[1,512,128]{2,1,0:T(8,128)(2,1)}, bf16[1,512,128]{2,1,0:T(8,128)(2,1)S(1)}, u32[]{:S(2)}, u32[]{:S(2)}) collective-permute-start(bf16[1,512,128]{2,1,0:T(8,128)(2,1)} %get-tuple-element.39.own), channel_id=1, source_target_pairs={{0,4},{4,0},{8,12},{12,8},{16,20},{20,16},{24,28},{28,24},{32,36},... | collective-permute-start | bytes 393224 | tf_op jit(solution)/shard_map/ppermute | solution.py:48
  59.0 7.3 %collective-permute-start.5 = (bf16[256,256]{1,0:T(8,128)(2,1)}, bf16[256,256]{1,0:T(8,128)(2,1)S(1)}, u32[]{:S(2)}, u32[]{:S(2)}) collective-permute-start(bf16[256,256]{1,0:T(8,128)(2,1)} %get-tuple-element.46.q3.q0), channel_id=1, source_target_pairs={{0,16},{4,20},{8,24},{12,28},{16,0},{20,4},{24,8},{28,12},{32,48},... | collective-permute-start | bytes 393224 | tf_op jit(solution)/shard_map/ppermute | solution.py:48
  66.3 5.9 %collective-permute-start.4 = (bf16[256,256]{1,0:T(8,128)(2,1)}, bf16[256,256]{1,0:T(8,128)(2,1)S(1)}, u32[]{:S(2)}, u32[]{:S(2)}) collective-permute-start(bf16[256,256]{1,0:T(8,128)(2,1)} %get-tuple-element.46.q3.q0), channel_id=1, source_target_pairs={{0,24},{4,28},{8,0},{12,4},{16,8},{20,12},{24,16},{28,20},{32,56},... | collective-permute-start | bytes 393224 | tf_op jit(solution)/shard_map/ppermute | solution.py:48
  72.1 6.7 %collective-permute-start.3 = (bf16[256,256]{1,0:T(8,128)(2,1)}, bf16[256,256]{1,0:T(8,128)(2,1)S(1)}, u32[]{:S(2)}, u32[]{:S(2)}) collective-permute-start(bf16[256,256]{1,0:T(8,128)(2,1)} %get-tuple-element.46.q3.q0), channel_id=1, source_target_pairs={{0,8},{4,12},{8,16},{12,20},{16,24},{20,28},{24,0},{28,4},{32,40},... | collective-permute-start | bytes 393224 | tf_op jit(solution)/shard_map/ppermute | solution.py:48
  87.8 31.9 %copy-start.4 = (bf16[256,256]{1,0:T(8,128)(2,1)S(1)}, bf16[256,256]{1,0:T(8,128)(2,1)}, u32[]{:S(2)}) copy-start(bf16[256,256]{1,0:T(8,128)(2,1)} %get-tuple-element.46.q3.q0) | copy-start | bytes 393220
  91.9 51.1 %collective-permute-start.21 = (bf16[384,1024]{1,0:T(8,128)(2,1)S(1)}, bf16[384,1024]{1,0:T(8,128)(2,1)S(1)}, u32[]{:S(2)}, u32[]{:S(2)}) collective-permute-start(bf16[384,1024]{1,0:T(8,128)(2,1)S(1)} %collective-permute-done.8.a1), channel_id=1, source_target_pairs={{0,4},{4,0},{8,12},{12,8},{16,20},{20,16},{24,28},{28,24},{32,36},... | collective-permute-start | bytes 2359304 | tf_op jit(solution)/shard_map/ppermute | solution.py:48
  92.0 51.1 %collective-permute-start.22 = (bf16[384,1024]{1,0:T(8,128)(2,1)S(1)}, bf16[384,1024]{1,0:T(8,128)(2,1)S(1)}, u32[]{:S(2)}, u32[]{:S(2)}) collective-permute-start(bf16[384,1024]{1,0:T(8,128)(2,1)S(1)} %collective-permute-done.9.a2), channel_id=1, source_target_pairs={{0,4},{4,0},{8,12},{12,8},{16,20},{20,16},{24,28},{28,24},{32,36},... | collective-permute-start | bytes 2359304 | tf_op jit(solution)/shard_map/ppermute | solution.py:48
  92.5 50.6 %collective-permute-start.23 = (bf16[384,1024]{1,0:T(8,128)(2,1)S(1)}, bf16[384,1024]{1,0:T(8,128)(2,1)S(1)}, u32[]{:S(2)}, u32[]{:S(2)}) collective-permute-start(bf16[384,1024]{1,0:T(8,128)(2,1)S(1)} %collective-permute-done.10.a3), channel_id=1, source_target_pairs={{0,4},{4,0},{8,12},{12,8},{16,20},{20,16},{24,28},{28,24},{32,36},... | collective-permute-start | bytes 2359304 | tf_op jit(solution)/shard_map/ppermute | solution.py:48
  92.5 27.0 %collective-permute-start.11 = (bf16[528,256]{1,0:T(8,128)(2,1)}, bf16[528,256]{1,0:T(8,128)(2,1)S(1)}, u32[]{:S(2)}, u32[]{:S(2)}) collective-permute-start(bf16[528,256]{1,0:T(8,128)(2,1)} %get-tuple-element.42), channel_id=1, source_target_pairs={{0,24},{4,28},{8,0},{12,4},{16,8},{20,12},{24,16},{28,20},{32,56},... | collective-permute-start | bytes 811016 | tf_op jit(solution)/shard_map/ppermute | solution.py:48
  95.5 34.5 %copy-start.9 = (f32[128]{0:T(128)S(1)}, f32[128]{0:T(128)}, u32[]{:S(2)}) copy-start(f32[128]{0:T(128)} %param.25) | copy-start | bytes 1540
  95.5 34.5 %copy-start.10 = (f32[2]{0:T(128)S(1)}, f32[2]{0:T(128)}, u32[]{:S(2)}) copy-start(f32[2]{0:T(128)} %lam.1) | copy-start | bytes 28
  95.5 34.5 %copy-start.11 = (f32[128]{0:T(128)S(1)}, f32[128]{0:T(128)}, u32[]{:S(2)}) copy-start(f32[128]{0:T(128)} %param.27) | copy-start | bytes 1540
  97.0 46.1 %copy-start = (bf16[256,2048]{1,0:T(8,128)(2,1)S(1)}, bf16[256,2048]{1,0:T(8,128)(2,1)}, u32[]{:S(2)}) copy-start(bf16[256,2048]{1,0:T(8,128)(2,1)} %w_attn.1) | copy-start | bytes 3145732
  97.0 46.1 %copy-start.1 = (bf16[128,2048]{1,0:T(8,128)(2,1)S(1)}, bf16[128,2048]{1,0:T(8,128)(2,1)}, u32[]{:S(2)}) copy-start(bf16[128,2048]{1,0:T(8,128)(2,1)} %w_conv.1) | copy-start | bytes 1572868
  97.0 7.4 %collective-permute-start.14 = (bf16[32,128]{1,0:T(8,128)(2,1)}, bf16[32,128]{1,0:T(8,128)(2,1)S(1)}, u32[]{:S(2)}, u32[]{:S(2)}) collective-permute-start(bf16[32,128]{1,0:T(8,128)(2,1)} %get-tuple-element.53), channel_id=1, source_target_pairs={{0,4},{4,8},{8,12},{12,16},{16,20},{20,24},{24,28},{28,32},{32,36}... | collective-permute-start | bytes 24584 | tf_op jit(solution)/shard_map/ppermute | solution.py:327
  105.4 5.3 %collective-permute-start.17 = (f32[1,256]{1,0:T(1,128)}, f32[1,256]{1,0:T(1,128)S(1)}, u32[]{:S(2)}, u32[]{:S(2)}) collective-permute-start(f32[1,256]{1,0:T(1,128)} %get-tuple-element.56), channel_id=1, source_target_pairs={{0,2},{1,3},{2,0},{3,1},{4,6},{5,7},{6,4},{7,5},{8,10},{9,11},{10,... | collective-permute-start | bytes 3080 | tf_op jit(solution)/shard_map/ppermute | solution.py:60
  110.6 3.8 %collective-permute-start.16 = (f32[1,256]{1,0:T(1,128)}, f32[1,256]{1,0:T(1,128)S(1)}, u32[]{:S(2)}, u32[]{:S(2)}) collective-permute-start(f32[1,256]{1,0:T(1,128)} %get-tuple-element.56), channel_id=1, source_target_pairs={{0,3},{1,0},{2,1},{3,2},{4,7},{5,4},{6,5},{7,6},{8,11},{9,8},{10,9... | collective-permute-start | bytes 3080 | tf_op jit(solution)/shard_map/ppermute | solution.py:60
  114.4 5.0 %collective-permute-start.15 = (f32[1,256]{1,0:T(1,128)}, f32[1,256]{1,0:T(1,128)S(1)}, u32[]{:S(2)}, u32[]{:S(2)}) collective-permute-start(f32[1,256]{1,0:T(1,128)} %get-tuple-element.56), channel_id=1, source_target_pairs={{0,1},{1,2},{2,3},{3,0},{4,5},{5,6},{6,7},{7,4},{8,9},{9,10},{10,1... | collective-permute-start | bytes 3080 | tf_op jit(solution)/shard_map/ppermute | solution.py:60
  119.4 10.6 %collective-permute-start.12 = (bf16[528,256]{1,0:T(8,128)(2,1)S(1)}, bf16[528,256]{1,0:T(8,128)(2,1)S(1)}, u32[]{:S(2)}, u32[]{:S(2)}) collective-permute-start(bf16[528,256]{1,0:T(8,128)(2,1)S(1)} %copy-done.19), channel_id=1, source_target_pairs={{0,8},{4,12},{8,16},{12,20},{16,24},{20,28},{24,0},{28,4},{32,40},... | collective-permute-start | bytes 811016 | tf_op jit(solution)/shard_map/ppermute | solution.py:48
  119.5 10.6 %collective-permute-start.13 = (bf16[528,256]{1,0:T(8,128)(2,1)S(1)}, bf16[528,256]{1,0:T(8,128)(2,1)S(1)}, u32[]{:S(2)}, u32[]{:S(2)}) collective-permute-start(bf16[528,256]{1,0:T(8,128)(2,1)S(1)} %copy-done.18), channel_id=1, source_target_pairs={{0,16},{4,20},{8,24},{12,28},{16,0},{20,4},{24,8},{28,12},{32,48},... | collective-permute-start | bytes 811016 | tf_op jit(solution)/shard_map/ppermute | solution.py:48
  131.8 5.5 %collective-permute-start.18 = (bf16[64,384]{1,0:T(8,128)(2,1)}, bf16[64,384]{1,0:T(8,128)(2,1)S(1)}, u32[]{:S(2)}, u32[]{:S(2)}) collective-permute-start(bf16[64,384]{1,0:T(8,128)(2,1)} %get-tuple-element.59), channel_id=1, source_target_pairs={{0,1},{1,2},{2,3},{3,0},{4,5},{5,6},{6,7},{7,4},{8,9},{9,10},{10,1... | collective-permute-start | bytes 147464 | tf_op jit(solution)/shard_map/ppermute | solution.py:60
  131.8 5.5 %collective-permute-start.19 = (bf16[64,384]{1,0:T(8,128)(2,1)}, bf16[64,384]{1,0:T(8,128)(2,1)S(1)}, u32[]{:S(2)}, u32[]{:S(2)}) collective-permute-start(bf16[64,384]{1,0:T(8,128)(2,1)} %get-tuple-element.60), channel_id=1, source_target_pairs={{0,3},{1,0},{2,1},{3,2},{4,7},{5,4},{6,5},{7,6},{8,11},{9,8},{10,9... | collective-permute-start | bytes 147464 | tf_op jit(solution)/shard_map/ppermute | solution.py:60
  137.3 5.8 %collective-permute-start.20 = (bf16[64,384]{1,0:T(8,128)(2,1)}, bf16[64,384]{1,0:T(8,128)(2,1)S(1)}, u32[]{:S(2)}, u32[]{:S(2)}) collective-permute-start(bf16[64,384]{1,0:T(8,128)(2,1)} %get-tuple-element.61), channel_id=1, source_target_pairs={{0,2},{1,3},{2,0},{3,1},{4,6},{5,7},{6,4},{7,5},{8,10},{9,11},{10,... | collective-permute-start | bytes 147464 | tf_op jit(solution)/shard_map/ppermute | solution.py:60
  (12 other events, 116.2 us)
